TPU v7x, 128 devices: a whole 4x4x4 slice. The times are simulated.
128 devices in a mesh: ep: 128 (over z, y, x, core).
Axes of the slice: x: 4, y: 4, z: 4, core: 2. Of those that a mesh axis runs over, the one named last changes fastest.
Arguments:
- tokens: bfloat16 [2048, 2048], P('ep'), may hold values from -6 to 6
- lengths: int32 [2048], P('ep'), may hold values from 1 to 1024, 1048576 in all
- cache_keys: bfloat16 [2048, 1024, 128], P('ep'), may hold values from -6 to 6
- cache_values: bfloat16 [2048, 1024, 128], P('ep'), may hold values from -6 to 6
- mix_gain: float32 [2048], replicated, may hold values from 0.1 to 1.9
- mix_out_gain: float32 [2048], replicated, may hold values from 0.1 to 1.9
- ffn_gain: float32 [2048], replicated, may hold values from 0.1 to 1.9
- ffn_out_gain: float32 [2048], replicated, may hold values from 0.1 to 1.9
- query_weight: bfloat16 [2048, 2048], P(None, 'ep'), may hold values from -0.125 to 0.125
- key_weight: bfloat16 [2048, 128], replicated, may hold values from -0.125 to 0.125
- value_weight: bfloat16 [2048, 128], replicated, may hold values from -0.125 to 0.125
- head_bias: float32 [32], replicated, may hold values from -8 to -2
- output_weight: bfloat16 [2048, 2048], P(None, 'ep'), may hold values from -0.125 to 0.125
- routes: int32 [2048, 6], P('ep'), may hold values from 0 to 127, all different within a row; in each aligned block of 16 rows (0 to 15, 16 to 31, ...) at most 2 rows name the same one
- route_weights: float32 [2048, 6], P('ep'), may hold values from 0.1 to 1
- expert_gate: bfloat16 [128, 2048, 512], P('ep'), may hold values from -0.125 to 0.125
- expert_up: bfloat16 [128, 2048, 512], P('ep'), may hold values from -0.125 to 0.125
- expert_down: bfloat16 [128, 512, 2048], P('ep'), may hold values from -0.25 to 0.25
- shared_gate: bfloat16 [2048, 512], replicated, may hold values from -0.125 to 0.125
- shared_up: bfloat16 [2048, 512], replicated, may hold values from -0.125 to 0.125
- shared_down: bfloat16 [512, 2048], replicated, may hold values from -0.25 to 0.25
Outputs:
- layer_out: bfloat16 [2048, 2048], P('ep')
- new_keys: bfloat16 [2048, 128], P('ep')
- new_values: bfloat16 [2048, 128], P('ep')
Inputs may be any that keep to these rules, and one draw needn't show every extreme that they name: `routes`: each row names 6 different experts. Among the rows of one device no expert is named more than 2 times, a bound that some block reaches in some device's rows. `lengths`: the new token stands at this position; cache entries at this position and after are unused. Some sequence has exactly 1024.
All inputs are finite; a program needn't handle non-finite values. No bound on the sum of `lengths` on one device may be relied on, other than what follows from the above.
Results may differ from a plain program's by a relative error of at most 0.013.
Values may be sent and summed in bfloat16 or wider, within the bound.
No kernel may reach another device: no remote copies, remote signals or barrier semaphores. Data moves between devices by JAX's collectives and lax.ppermute only.
A program may use at most 128 MiB of HBM per device.

v0:
```python
import math

import jax
import jax.numpy as jnp
from jax import lax
from jax.sharding import PartitionSpec as P

HD = 64


def rms_scale(rows, gain):
    return rows * lax.rsqrt(jnp.mean(rows * rows, axis=-1, keepdims=True) + 1e-06) * gain


def later_sums(values):
    seqs, kv_heads, group, span = values.shape
    width = math.gcd(span, 128)
    count = span // width
    blocked = values.reshape(seqs, kv_heads, group, count, width)
    inner_pos = jnp.arange(width)
    upper = (inner_pos[:, None] > inner_pos[None, :]).astype(jnp.float32)
    inside = jnp.einsum("skgbj,ji->skgbi", blocked, upper, precision=lax.Precision.HIGHEST)
    totals = jnp.sum(blocked, axis=4)
    block_pos = jnp.arange(count)
    beyond = (block_pos[:, None] > block_pos[None, :]).astype(jnp.float32)
    carried = jnp.einsum("skgc,cb->skgb", totals, beyond, precision=lax.Precision.HIGHEST)
    return (inside + carried[..., None]).reshape(seqs, kv_heads, group, span)


def body(
    tokens,
    lengths,
    cache_keys,
    cache_values,
    mix_gain,
    mix_out_gain,
    ffn_gain,
    ffn_out_gain,
    query_weight,
    key_weight,
    value_weight,
    head_bias,
    output_weight,
    routes,
    route_weights,
    expert_gate,
    expert_up,
    expert_down,
    shared_gate,
    shared_up,
    shared_down,
):
    resid = tokens.astype(jnp.float32)
    normed = rms_scale(resid, mix_gain).astype(jnp.bfloat16)
    new_keys = jnp.dot(normed, key_weight, preferred_element_type=jnp.float32).astype(jnp.bfloat16)
    new_values = jnp.dot(normed, value_weight, preferred_element_type=jnp.float32).astype(
        jnp.bfloat16
    )
    queries = jnp.dot(
        normed,
        lax.all_gather(query_weight, "ep", axis=1, tiled=True),
        preferred_element_type=jnp.float32,
    ).astype(jnp.bfloat16)
    seqs, span, width = cache_keys.shape
    kv_heads = width // HD
    heads = queries.shape[1] // HD
    group = heads // kv_heads
    q_heads = queries.reshape(seqs, kv_heads, group, HD)
    k_heads = cache_keys.reshape(seqs, span, kv_heads, HD)
    v_heads = cache_values.reshape(seqs, span, kv_heads, HD)
    scores = jnp.einsum(
        "skgd,slkd->skgl", q_heads, k_heads, preferred_element_type=jnp.float32
    ) * HD ** (-0.5)
    scores = scores + head_bias.reshape(kv_heads, group)[None, :, :, None]
    valid = (jnp.arange(span)[None, :] < lengths[:, None])[:, None, None, :]
    log_beta = jax.nn.log_sigmoid(scores)
    log_keep = jnp.where(valid, log_beta - scores, 0.0)
    after = later_sums(log_keep)
    stick = jnp.where(valid, jnp.exp(log_beta + after), 0.0).astype(jnp.bfloat16)
    attended = jnp.einsum("skgl,slkd->skgd", stick, v_heads, preferred_element_type=jnp.float32)
    attended = attended.astype(jnp.bfloat16).reshape(seqs, heads * HD)
    mixed = jnp.dot(
        attended,
        lax.all_gather(output_weight, "ep", axis=1, tiled=True),
        preferred_element_type=jnp.float32,
    ).astype(jnp.bfloat16)
    resid1 = resid + rms_scale(mixed.astype(jnp.float32), mix_out_gain)
    ffn_in = rms_scale(resid1, ffn_gain).astype(jnp.bfloat16)
    devices = lax.axis_size("ep")
    top = routes.shape[1]
    experts = devices * expert_gate.shape[0]
    capacity = 2 * ((seqs * top + devices - 1) // devices)
    flat = routes.reshape(-1)
    onehot = (flat[:, None] == jnp.arange(experts)[None, :]).astype(jnp.float32)
    assign_pos = jnp.arange(flat.shape[0])
    lower = (assign_pos[:, None] > assign_pos[None, :]).astype(jnp.float32)
    earlier = jnp.dot(lower, onehot, precision=lax.Precision.HIGHEST)
    rank = jnp.sum(earlier * onehot, axis=1).astype(jnp.int32)
    slot = flat * capacity + rank
    placed = slot.reshape(seqs, top)[:, :, None] == jnp.arange(experts * capacity)[None, None, :]
    dispatch = jnp.sum(placed.astype(jnp.float32), axis=1).astype(jnp.bfloat16)
    outgoing = jnp.einsum("sc,sd->cd", dispatch, ffn_in, preferred_element_type=jnp.float32)
    outgoing = outgoing.astype(jnp.bfloat16).reshape(experts, capacity, ffn_in.shape[1])
    shared_hidden = (
        jax.nn.silu(jnp.dot(ffn_in, shared_gate, preferred_element_type=jnp.float32))
        * jnp.dot(ffn_in, shared_up, preferred_element_type=jnp.float32)
    ).astype(jnp.bfloat16)
    shared_out = jnp.dot(shared_hidden, shared_down, preferred_element_type=jnp.float32)
    incoming = lax.all_to_all(outgoing, "ep", split_axis=0, concat_axis=0, tiled=True)
    sources, count, features = incoming.shape
    rows = incoming.reshape(sources * count, features)
    hidden = (
        jax.nn.silu(jnp.dot(rows, expert_gate[0], preferred_element_type=jnp.float32))
        * jnp.dot(rows, expert_up[0], preferred_element_type=jnp.float32)
    ).astype(jnp.bfloat16)
    result = jnp.dot(hidden, expert_down[0], preferred_element_type=jnp.float32).astype(
        jnp.bfloat16
    )
    returned = lax.all_to_all(
        result.reshape(sources, count, features), "ep", split_axis=0, concat_axis=0, tiled=True
    )
    picked = jnp.take(returned.reshape(experts * capacity, -1), slot, axis=0)
    routed = jnp.sum(
        picked.astype(jnp.float32).reshape(seqs, top, -1) * route_weights[:, :, None], axis=1
    )
    layer_out = (resid1 + rms_scale(routed + shared_out, ffn_out_gain)).astype(jnp.bfloat16)
    return (layer_out, new_keys, new_values)


def solution(mesh):
    in_specs = (
        P("ep", None),
        P("ep"),
        P("ep", None, None),
        P("ep", None, None),
        P(),
        P(),
        P(),
        P(),
        P(None, "ep"),
        P(),
        P(),
        P(),
        P(None, "ep"),
        P("ep", None),
        P("ep", None),
        P("ep", None, None),
        P("ep", None, None),
        P("ep", None, None),
        P(),
        P(),
        P(),
    )
    out_specs = (P("ep", None), P("ep", None), P("ep", None))
    return jax.shard_map(body, mesh=mesh, in_specs=in_specs, out_specs=out_specs, check_vma=False)
```

profile of v0, /device:TPU:1, one launch (start us, length us, event | category | flops | bytes accessed | tf_op | source)
XLA Modules:
  0.0 238.4 jit_solution(5669032476505502544)
XLA Ops:
  7.2 0.0 copy-start
  7.2 0.0 all-gather.3.cloned.1.call-start
  7.2 0.7 all-gather.3.cloned.1.call-update
  7.9 0.0 all-gather.5.cloned.1.call-start
  8.0 0.7 all-gather.5.cloned.1.call-update
  8.7 0.7 add.115
  9.4 6.4 %copy.43 = bf16[16,1024,128]{1,2,0:T(8,128)(2,1)} copy(bf16[16,1024,128]{2,1,0:T(8,128)(2,1)} %param.23) | data formatting | bytes 8388608 | tf_op args[2]
  15.8 6.5 %copy.46 = bf16[16,1024,128]{1,2,0:T(8,128)(2,1)} copy(bf16[16,1024,128]{2,1,0:T(8,128)(2,1)} %param.24) | data formatting | bytes 8388608 | tf_op args[3]
  22.3 0.0 copy-done.9
  22.3 0.1 copy.47
  22.4 0.1 reshape.156
  22.5 0.3 fusion.13
  22.8 0.1 convert_element_type.88
  22.9 0.1 copy.49
  23.0 0.1 convert_reduce_fusion
  23.1 0.0 copy-done.1
  23.1 0.1 fusion.26
  23.2 0.0 copy-done.11
  23.2 0.1 iota_compare_fusion.2
  23.3 61.0 %all-gather.3.cloned.1.call-done = bf16[2048,2048]{0,1:T(8,128)(2,1)} async-done(((bf16[2048,16]{0,1:T(8,128)(2,1)}), bf16[2048,2048]{0,1:T(8,128)(2,1)}) %all-gather.3.cloned.1.call-update) | async-done | bytes 8388624 | tf_op jit(solution)/shard_map/all_gather | solution.py:61
  84.3 0.0 copy-done.5
  84.3 5.6 %convolution_convert_fusion.3 = bf16[16,2048]{1,0:T(8,128)(2,1)S(1)} fusion(bf16[2048,2048]{0,1:T(8,128)(2,1)} %all-gather.3.cloned.1.call-done, bf16[16,2048]{1,0:T(8,128)(2,1)S(1)} %copy-done.1, f32[2048]{0:T(1024)S(1)} %copy-done.5, f32[16]{0:T(128)S(1)} %add_rsqrt_fusion.3), kind=kOutput, calls=%fused_computation.7 | convolution fusion | flops 134381568 | bytes 8527936 | tf_op jit(solution)/shard_map/dot_general | solution.py:59
  90.0 0.2 reshape.150
  90.2 5.3 %subtract_select_fusion = (f32[16,2,16,1024]{3,2,1,0:T(8,128)S(1)}, f32[16,2,16,1024]{3,2,1,0:T(8,128)}) fusion(f32[2,16]{1,0:T(2,128)S(1)} %add.115, pred[16,1024]{1,0:T(8,128)(4,1)S(1)} %iota_compare_fusion.2, bf16[16,2,16,64]{3,2,1,0:T(8,128)(2,1)S(1)} %reshape.150, bf16[16,1024,2,64]{1,3,2,0:T(8,128)(2,1)} %bitcast.64), kind=kOutput, calls=%fused_computation.15 | convolution fusion | flops 73400320 | bytes 8470656 | tf_op jit(solution)/shard_map/skgd,slkd->skgl/dot_general | solution.py:71
  95.5 1.8 copy.55
  97.2 2.2 reduce_sum.73
  99.4 0.2 fusion.40
  99.7 4.1 %convolution_add_fusion.1 = f32[16,2,16,8,128]{4,3,2,1,0:T(8,128)} fusion(f32[16,2,16,8,128]{4,3,2,1,0:T(8,128)} %bitcast.62, f32[16,2,16,8]{3,2,1,0:T(8,128)S(1)} %fusion.40), kind=kOutput, calls=%fused_computation.17 | convolution fusion | flops 805847040 | bytes 4210688 | tf_op jit(solution)/shard_map/skgbj,ji->skgbi/dot_general | solution.py:22
  103.8 2.7 %reshape.153 = f32[16,2,16,1024]{3,2,1,0:T(8,128)} reshape(f32[16,2,16,8,128]{4,3,2,1,0:T(8,128)} %convolution_add_fusion.1) | data formatting | bytes 4194304 | tf_op jit(solution)/shard_map/reshape | solution.py:27
  106.5 5.4 %convolution_convert_fusion.4 = bf16[16,2,16,64]{3,2,1,0:T(8,128)(2,1)S(1)} fusion(bf16[16,1024,2,64]{1,3,2,0:T(8,128)(2,1)} %bitcast.63, f32[16,2,16,1024]{3,2,1,0:T(8,128)} %reshape.153, f32[16,2,16,1024]{3,2,1,0:T(8,128)} %get-tuple-element.6, f32[2,16]{1,0:T(2,128)S(1)} %add.115, pred[16,1024]{1,0:T(8,128)(4,1)S(1)} %iota_compare_fusion.2), kind=kOutput, calls=%fused_computation.20 | convolution fusion | flops 73957376 | bytes 8470656 | tf_op jit(solution)/shard_map/skgl,slkd->skgd/dot_general | solution.py:80
  111.9 0.2 reshape.155
  112.1 0.0 copy-start.6
  112.1 0.0 copy-start.7
  112.1 42.4 %all-gather.5.cloned.1.call-done = bf16[2048,2048]{0,1:T(8,128)(2,1)} async-done(((bf16[2048,16]{0,1:T(8,128)(2,1)}), bf16[2048,2048]{0,1:T(8,128)(2,1)}) %all-gather.5.cloned.1.call-update) | async-done | bytes 8388624 | tf_op jit(solution)/shard_map/all_gather | solution.py:84
  154.5 5.8 %multiply_reduce_fusion.3 = (f32[16]{0:T(128)S(1)}, f32[16,2048]{1,0:T(8,128)S(1)}) fusion(bf16[16,2048]{1,0:T(8,128)(2,1)S(1)} %reshape.155, bf16[2048,2048]{0,1:T(8,128)(2,1)} %all-gather.5.cloned.1.call-done), kind=kOutput, calls=%fused_computation.47 | convolution fusion | flops 134348784 | bytes 8585280 | tf_op jit(solution)/shard_map/dot_general | solution.py:82
  160.3 0.0 copy-done.6
  160.3 0.2 multiply_reduce_fusion.2
  160.5 0.0 copy-done.7
  160.5 0.1 multiply_convert_fusion
  160.6 0.4 convolution_convert_fusion.1
  161.1 0.0 copy-start.10
  161.1 1.5 reshape.157
  162.6 5.4 %all-to-all-start = ((bf16[128,2,2048]{2,1,0:T(2,128)(2,1)}), bf16[128,2,2048]{2,1,0:T(2,128)(2,1)S(1)}, u32[]{:S(2)}, u32[]{:S(2)}) async-start(bf16[128,2,2048]{2,1,0:T(2,128)(2,1)} %reshape.157), calls=%async_computation | async-start | bytes 2097152 | tf_op jit(solution)/shard_map/all_to_all | solution.py:109
  168.0 0.1 mul.150
  168.1 0.0 copy-done.10
  168.1 0.1 copy.50
  168.2 19.0 %all-to-all-done = bf16[128,2,2048]{2,1,0:T(2,128)(2,1)S(1)} async-done(((bf16[128,2,2048]{2,1,0:T(2,128)(2,1)}), bf16[128,2,2048]{2,1,0:T(2,128)(2,1)S(1)}, u32[]{:S(2)}, u32[]{:S(2)}) %all-to-all-start) | async-done | bytes 1048608 | tf_op jit(solution)/shard_map/all_to_all | solution.py:109
  187.2 1.2 reshape.158
  188.4 3.5 %fusion.5 = f32[256,512]{1,0:T(8,128)} fusion(bf16[256,2048]{1,0:T(8,128)(2,1)} %reshape.158, bf16[1,2048,512]{2,1,0:T(8,128)(2,1)} %param.36), kind=kOutput, calls=%fused_computation.12 | convolution fusion | flops 536870912 | bytes 3670016 | tf_op jit(solution)/shard_map/dot_general | solution.py:113
  191.9 0.0 copy-done.2
  191.9 4.0 %convolution_convert_fusion = bf16[256,2048]{1,0:T(8,128)(2,1)} fusion(bf16[1,512,2048]{2,1,0:T(8,128)(2,1)S(1)} %copy-done, bf16[256,2048]{1,0:T(8,128)(2,1)S(1)} %copy-done.2, bf16[1,2048,512]{2,1,0:T(8,128)(2,1)} %param.37, f32[256,512]{1,0:T(8,128)} %fusion.5), kind=kOutput, calls=%fused_computation.2 | convolution fusion | flops 1075052544 | bytes 6815744 | tf_op jit(solution)/shard_map/dot_general | solution.py:116
  195.9 2.6 %reshape.159 = bf16[128,2,2048]{2,1,0:T(2,128)(2,1)} reshape(bf16[256,2048]{1,0:T(8,128)(2,1)} %convolution_convert_fusion) | data formatting | bytes 2097152 | tf_op jit(solution)/shard_map/reshape | solution.py:120
  198.5 5.4 %all-to-all-start.1 = ((bf16[128,2,2048]{2,1,0:T(2,128)(2,1)}), bf16[128,2,2048]{2,1,0:T(2,128)(2,1)}, u32[]{:S(2)}, u32[]{:S(2)}) async-start(bf16[128,2,2048]{2,1,0:T(2,128)(2,1)} %reshape.159), calls=%async_computation.1 | async-start | bytes 2097152 | tf_op jit(solution)/shard_map/all_to_all | solution.py:119
  204.0 0.8 convolution_convert_fusion.5
  204.9 0.8 convolution_convert_fusion.6
  205.7 2.0 fusion.52
  207.7 15.3 %all-to-all-done.1 = bf16[128,2,2048]{2,1,0:T(2,128)(2,1)} async-done(((bf16[128,2,2048]{2,1,0:T(2,128)(2,1)}), bf16[128,2,2048]{2,1,0:T(2,128)(2,1)}, u32[]{:S(2)}, u32[]{:S(2)}) %all-to-all-start.1) | async-done | bytes 1048608 | tf_op jit(solution)/shard_map/all_to_all | solution.py:119
  223.0 1.5 reshape.160
  224.5 1.6 gather_fusion
  226.1 1.1 gather.7
  227.2 0.6 multiply_reduce_fusion
  227.8 0.0 copy-start.8
  227.8 3.1 %multiply_reduce_fusion.1 = (f32[16]{0:T(128)S(1)}, f32[16,2048]{1,0:T(8,128)S(1)}) fusion(f32[16,2048]{1,0:T(8,128)S(1)} %multiply_reduce_fusion, bf16[512,2048]{1,0:T(8,128)(2,1)} %param.41, bf16[16,2048]{1,0:T(8,128)(2,1)S(1)} %multiply_convert_fusion, bf16[2048,512]{1,0:T(8,128)(2,1)} %param.40, f32[16,512]{1,0:T(8,128)S(1)} %fusion.52), kind=kOutput, calls=%fused_computation.44 | convolution fusion | flops 67256304 | bytes 4554816 | tf_op jit(solution)/shard_map/dot_general | solution.py:108
  230.9 0.7 add_convert_fusion
  (20 shorter events, 0.1 us)
Async XLA Ops:
  7.2 184.7 %copy-start = (bf16[1,512,2048]{2,1,0:T(8,128)(2,1)S(1)}, bf16[1,512,2048]{2,1,0:T(8,128)(2,1)}, u32[]{:S(2)}) copy-start(bf16[1,512,2048]{2,1,0:T(8,128)(2,1)} %param.38) | copy-start | bytes 6291460
  7.2 77.1 %all-gather.3.cloned.1.call-start = ((), (), s32[]{:S(2)}) async-start(), calls=%async_computation.2 | async-start | bytes 8454144 | tf_op jit(solution)/shard_map/all_gather | solution.py:61
  7.9 146.6 %all-gather.5.cloned.1.call-start = ((), (), s32[]{:S(2)}) async-start(), calls=%async_computation.3 | async-start | bytes 8454144 | tf_op jit(solution)/shard_map/all_gather | solution.py:84
  15.8 6.5 %copy-start.9 = (s32[16,6]{0,1:T(8,128)S(1)}, s32[16,6]{0,1:T(8,128)}, u32[]{:S(2)}) copy-start(s32[16,6]{0,1:T(8,128)} %param.34) | copy-start | bytes 1156
  15.8 7.3 %copy-start.1 = (bf16[16,2048]{1,0:T(8,128)(2,1)S(1)}, bf16[16,2048]{1,0:T(8,128)(2,1)}, u32[]{:S(2)}) copy-start(bf16[16,2048]{1,0:T(8,128)(2,1)} %param.21) | copy-start | bytes 196612
  15.8 7.4 %copy-start.11 = (s32[16]{0:T(128)S(1)}, s32[16]{0:T(128)}, u32[]{:S(2)}) copy-start(s32[16]{0:T(128)} %param.22) | copy-start | bytes 196
  15.8 68.5 %copy-start.5 = (f32[2048]{0:T(1024)S(1)}, f32[2048]{0:T(1024)}, u32[]{:S(2)}) copy-start(f32[2048]{0:T(1024)} %param.25) | copy-start | bytes 24580
  112.1 48.2 %copy-start.6 = (f32[2048]{0:T(1024)S(1)}, f32[2048]{0:T(1024)}, u32[]{:S(2)}) copy-start(f32[2048]{0:T(1024)} %param.26) | copy-start | bytes 24580
  112.1 48.4 %copy-start.7 = (f32[2048]{0:T(1024)S(1)}, f32[2048]{0:T(1024)}, u32[]{:S(2)}) copy-start(f32[2048]{0:T(1024)} %param.27) | copy-start | bytes 24580
  161.1 7.0 %copy-start.10 = (f32[16,6]{0,1:T(8,128)S(1)}, f32[16,6]{0,1:T(8,128)}, u32[]{:S(2)}) copy-start(f32[16,6]{0,1:T(8,128)} %param.35) | copy-start | bytes 1156
  162.6 24.6 %all-to-all-start = ((bf16[128,2,2048]{2,1,0:T(2,128)(2,1)}), bf16[128,2,2048]{2,1,0:T(2,128)(2,1)S(1)}, u32[]{:S(2)}, u32[]{:S(2)}) async-start(bf16[128,2,2048]{2,1,0:T(2,128)(2,1)} %reshape.157), calls=%async_computation | async-start | bytes 2097152 | tf_op jit(solution)/shard_map/all_to_all | solution.py:109
  188.4 3.5 %copy-start.2 = (bf16[256,2048]{1,0:T(8,128)(2,1)S(1)}, bf16[256,2048]{1,0:T(8,128)(2,1)}, u32[]{:S(2)}) copy-start(bf16[256,2048]{1,0:T(8,128)(2,1)} %reshape.158) | copy-start | bytes 3145732
  195.9 8.1 %copy-start.3 = (bf16[2048,128]{1,0:T(8,128)(2,1)S(1)}, bf16[2048,128]{1,0:T(8,128)(2,1)}, u32[]{:S(2)}) copy-start(bf16[2048,128]{1,0:T(8,128)(2,1)} %param.31) | copy-start | bytes 1572868
  195.9 9.0 %copy-start.4 = (bf16[2048,128]{1,0:T(8,128)(2,1)S(1)}, bf16[2048,128]{1,0:T(8,128)(2,1)}, u32[]{:S(2)}) copy-start(bf16[2048,128]{1,0:T(8,128)(2,1)} %param.30) | copy-start | bytes 1572868
  198.5 24.5 %all-to-all-start.1 = ((bf16[128,2,2048]{2,1,0:T(2,128)(2,1)}), bf16[128,2,2048]{2,1,0:T(2,128)(2,1)}, u32[]{:S(2)}, u32[]{:S(2)}) async-start(bf16[128,2,2048]{2,1,0:T(2,128)(2,1)} %reshape.159), calls=%async_computation.1 | async-start | bytes 2097152 | tf_op jit(solution)/shard_map/all_to_all | solution.py:119
  227.8 3.1 %copy-start.8 = (f32[2048]{0:T(1024)S(1)}, f32[2048]{0:T(1024)}, u32[]{:S(2)}) copy-start(f32[2048]{0:T(1024)} %param.28) | copy-start | bytes 24580
Sparse Core Ops, SparseCore 0:
  11.0 73.3 all-gather.2
  87.3 67.1 all-gather.4
where the time goes:
time: 239 us; the launch traced here: 238 us
  waiting for transfers between devices  139 us (58%)
  matrix products  41.4 us (17%)
  local copies, waits for them, and re-layouts  28.5 us (12%)
  between operations  14.3 us (6%)
  starting transfers between devices  10.9 us (5%)
  other arithmetic  4.18 us (2%)
    all_gather x1, waiting for transfers between devices, body(): lax.all_gather(query_weight, 'ep', axis=1, tiled=True)  61 us
    all_gather x1, waiting for transfers between devices, body(): lax.all_gather(output_weight, 'ep', axis=1, tiled=True)  42.4 us
    all_to_all x1, waiting for transfers between devices, body(): lax.all_to_all(outgoing, 'ep', split_axis=0, concat_axis=0, tiled=True)  19 us
    all_to_all x1, waiting for transfers between devices, body(): lax.all_to_all(result.reshape(sources, count, features), 'ep', split_axis...  15.3 us
    unnamed x29, local copies, waits for them, and re-layouts  14.9 us
    dot_general x1, matrix products, body(): jnp.dot(attended, lax.all_gather(output_weight, 'ep', axis=1, tiled=True)...  5.76 us
    dot_general x1, matrix products, body(): jnp.dot(normed, lax.all_gather(query_weight, 'ep', axis=1, tiled=True), p...  5.65 us
    all_to_all x1, starting transfers between devices, body(): lax.all_to_all(result.reshape(sources, count, features), 'ep', split_axis...  5.44 us
  transfers between devices with their start and end apart: 4, of which 4 were waited for; matrix products, arithmetic and copies ran while one was open for 19% of the time, Pallas kernels for 0%

commit v1 on v0

v1 whole, which is shorter than its diff:
```python
import jax
import jax.numpy as jnp
from jax import lax
from jax.experimental import pallas as pl
from jax.experimental.pallas import tpu as pltpu
from jax.sharding import PartitionSpec as P


D = 2048
HD = 64
H = 32
FF = 512
TOP = 6
SEQ = 16
LEN = 1024
EP = 128
GRP = 4
XS = 2
PLANE = 16
COLS = D // GRP
SHARD = D // EP
CAP = 2
CH = CAP * D // 16
NJ = D // CH
EPS = 1e-06
F32 = jnp.float32
BF16 = jnp.bfloat16

VMEM = pl.BlockSpec(memory_space=pltpu.VMEM)
HBM = pl.BlockSpec(memory_space=pltpu.HBM)
SMEM = pl.BlockSpec(memory_space=pltpu.SMEM)
PARAMS = pltpu.CompilerParams(vmem_limit_bytes=40 * 1024 * 1024)


def rms(rows, gain):
    return rows * lax.rsqrt(jnp.mean(rows * rows, axis=-1, keepdims=True) + EPS) * gain


def iota(shape, dim):
    return lax.broadcasted_iota(jnp.int32, shape, dim)


def dot(a, b):
    return jnp.dot(a, b, preferred_element_type=F32)


def dot_nt(a, b):
    return lax.dot_general(a, b, (((1,), (1,)), ((), ())), preferred_element_type=F32)


def start_columns(own, other, core, full, sems):
    copies = [
        pltpu.make_async_copy(own, full.at[:, core], sems.at[0]),
        pltpu.make_async_copy(other, full.at[:, 1 - core], sems.at[1]),
    ]
    for c in copies:
        c.start()
    return copies


def columns(copies, full):
    for c in copies:
        c.wait()
    return full[...].reshape(COLS, D)


def norm_kernel(t0, t1, t2, t3, gain, wk, wv, rows, nk, nv):
    for i, t in enumerate((t0, t1, t2, t3)):
        rows[i * SEQ : (i + 1) * SEQ] = rms(t[...].astype(F32), gain[...]).astype(BF16)
    mine = rows[:SEQ]
    nk[...] = dot(mine, wk[...]).astype(BF16)
    nv[...] = dot(mine, wv[...]).astype(BF16)


def query_kernel(place, rows, own, other, q0, q1, q2, q3, full, sems):
    copies = start_columns(own, other, place[1], full, sems)
    out = dot_nt(rows[...], columns(copies, full)).astype(BF16)
    for i, q in enumerate((q0, q1, q2, q3)):
        q[...] = out[i * SEQ : (i + 1) * SEQ]


SUB = 4
BLK = 256


def attend_kernel(place, lens, q0, q1, q2, q3, bias, keys, values, out, qf, sel, upper, att):
    step = pl.program_id(0)

    @pl.when(step == 0)
    def _():
        for i, q in enumerate((q0, q1, q2, q3)):
            qf[i] = q[...].astype(F32) * HD ** (-0.5)
        row, col = iota((D, 2 * HD), 0), iota((D, 2 * HD), 1)
        x, plane, k = row >> 9, (row >> 5) & (PLANE - 1), row & 31
        sel[...] = (col == (plane >> 3) * HD + (x & 1) * 32 + k).astype(F32).astype(BF16)
        upper[...] = (iota((BLK, BLK), 0) > iota((BLK, BLK), 1)).astype(F32).astype(BF16)

    own = place[0]
    plane = (iota((H, COLS), 1) >> 5) * 2
    masks = [plane + half == iota((H, COLS), 0) for half in range(2)]
    spread = []
    for u in range(SUB):
        parts = []
        for m in range(GRP):
            row = qf[own ^ m, pl.ds(step * SUB + u, 1), :]
            parts.append(jnp.where(masks[m >> 1], jnp.broadcast_to(row, (H, COLS)), 0.0).astype(BF16))
        spread.append(jnp.concatenate(parts, axis=1))
    placed = dot(jnp.concatenate(spread, axis=0), sel[...]).astype(BF16)
    for u in range(SUB):
        z = dot_nt(placed[u * H : (u + 1) * H], keys[u]) + bias[...]
        n = lens[step * SUB + u]
        valid = iota((H, LEN), 1) < n
        soft = jnp.log(1.0 + jnp.exp(-jnp.abs(z)))
        log_beta = jnp.minimum(z, 0.0) - soft
        log_keep = jnp.where(valid, log_beta - z, 0.0)
        high = log_keep.astype(BF16)
        low = (log_keep - high.astype(F32)).astype(BF16)
        carry = jnp.zeros((H, 1), F32)
        blocks = []
        for b in range(LEN // BLK - 1, -1, -1):
            s = slice(b * BLK, (b + 1) * BLK)
            both = dot(jnp.concatenate([high[:, s], low[:, s]], axis=0), upper[...])
            after = both[:H] + both[H:]
            blocks.append(after + carry)
            carry = carry + after[:, :1] + log_keep[:, s][:, :1]
        after = jnp.concatenate(blocks[::-1], axis=1)
        weights = jnp.where(valid, jnp.exp(log_beta + after), 0.0).astype(BF16)
        att[pl.ds((step * SUB + u) * H, H), :] = dot(weights, values[u])

    @pl.when(step == SEQ // SUB - 1)
    def _():
        left = iota((SEQ, 2 * HD), 1) < HD
        for i in range(H // 2):
            even = att[pl.ds(2 * i, SEQ, stride=H), :]
            odd = att[pl.ds(2 * i + 1, SEQ, stride=H), :]
            if 2 * i < H // 2:
                odd = pltpu.roll(odd, HD, 1)
            else:
                even = pltpu.roll(even, HD, 1)
            out[:, i * 2 * HD : (i + 1) * 2 * HD] = jnp.where(left, even, odd).astype(BF16)


def output_kernel(place, a0, a1, a2, a3, own, other, m0, m1, m2, m3, full, sems):
    copies = start_columns(own, other, place[1], full, sems)
    rows = jnp.concatenate([a[...] for a in (a0, a1, a2, a3)], axis=0)
    out = dot_nt(rows, columns(copies, full)).astype(BF16)
    for i, m in enumerate((m0, m1, m2, m3)):
        m[...] = out[i * SEQ : (i + 1) * SEQ]


def places(routes, weights):
    shape = (EP * CAP, NJ * SEQ)
    row = iota(shape, 0)
    named = jnp.zeros(shape, F32)
    weight = jnp.zeros(shape, F32)
    for k in range(TOP):
        hit = jnp.broadcast_to(routes[k : k + 1, :], shape) == row >> 1
        named = named + hit.astype(F32)
        if weights is not None:
            weight = weight + jnp.where(hit, jnp.broadcast_to(weights[k : k + 1, :], shape), 0.0)
    a, b = iota((NJ * SEQ, NJ * SEQ), 0), iota((NJ * SEQ, NJ * SEQ), 1)
    earlier = (((a >> 4) == (b >> 4)) & (a < b)).astype(F32).astype(BF16)
    rank = dot(named.astype(BF16), earlier)
    here = jnp.where((rank == (row & 1).astype(F32)) & (named > 0.0), 1.0, 0.0)
    return here if weights is None else here * weight


def expand(x):
    block = (iota((NJ, NJ * SEQ), 0) == (iota((NJ, NJ * SEQ), 1) >> 4)).astype(F32)
    return (x[:, None, :] * block[None, :, :]).reshape(EP * CAP * NJ, NJ * SEQ)


def route_kernel(routes, send):
    send[...] = expand(places(routes, None)).astype(BF16)


def mix_kernel(place, m0, m1, m2, m3, tokens, mix_gain, ffn_gain, send, resid1, ffn_in, outgoing, pieces):
    for i, m in enumerate((m0, m1, m2, m3)):
        pieces[i] = m[...]
    own = place[0]
    got = [pieces[own ^ m] for m in range(GRP)]
    n = GRP * 128
    col = iota((n, n), 1)
    source = ((col >> 5) & 3) * 128 + (col >> 7) * 32 + (col & 31)
    order = (iota((n, n), 0) == source).astype(F32).astype(BF16)
    parts = []
    for i in range(COLS // 128):
        block = jnp.concatenate([g[:, i * 128 : (i + 1) * 128] for g in got], axis=1)
        parts.append(dot(block, order))
    mixed = jnp.concatenate(parts, axis=1)
    r1 = tokens[...].astype(F32) + rms(mixed, mix_gain[...])
    resid1[...] = r1
    x = rms(r1, ffn_gain[...]).astype(BF16)
    ffn_in[...] = x
    blocks = jnp.concatenate([x[:, j * CH : (j + 1) * CH] for j in range(NJ)], axis=0)
    outgoing[...] = dot(send[...], blocks).astype(BF16)


def expert_kernel(incoming, gate, up, down, outgoing, rows, result, wg, wu, wd, sems):
    copies = [
        pltpu.make_async_copy(w.at[0], v, sems.at[i])
        for i, (w, v) in enumerate(((gate, wg), (up, wu), (down, wd)))
    ]
    for c in copies:
        c.start()
    n = 256
    a, b = iota((n, n), 0), iota((n, n), 1)
    order = (b == (a & 31) * NJ + (a >> 5)).astype(F32).astype(BF16)
    back = (a == (b & 31) * NJ + (b >> 5)).astype(F32).astype(BF16)
    for g in range(EP * 16 // n):
        block = dot(order, incoming[g * n : (g + 1) * n, :]).astype(BF16)
        for j in range(NJ):
            rows[g * 32 : (g + 1) * 32, j * CH : (j + 1) * CH] = block[j * 32 : (j + 1) * 32]
    x = rows[...]
    copies[0].wait()
    gated = jax.nn.silu(dot(x, wg[...]))
    copies[1].wait()
    hidden = (gated * dot(x, wu[...])).astype(BF16)
    copies[2].wait()
    result[...] = dot(hidden, wd[...]).astype(BF16)
    for g in range(EP * 16 // n):
        block = jnp.concatenate(
            [result[g * 32 : (g + 1) * 32, j * CH : (j + 1) * CH] for j in range(NJ)], axis=0
        )
        outgoing[g * n : (g + 1) * n, :] = dot(back, block).astype(BF16)


def final_kernel(returned, routes, weights, resid1, shared, gain, out):
    scaled = expand(places(routes, weights))
    top = scaled.astype(BF16)
    rest = (scaled - top.astype(F32)).astype(BF16)
    got = returned[...]
    total = dot(top.T, got) + dot(rest.T, got)
    routed = jnp.concatenate([total[j * SEQ : (j + 1) * SEQ] for j in range(NJ)], axis=1)
    out[...] = (resid1[...] + rms(routed + shared[...], gain[...])).astype(BF16)


def call(kernel, ins, outs, smem=0, hbm=0, scratch=()):
    return pl.pallas_call(
        kernel,
        in_specs=[SMEM] * smem + [VMEM] * (ins - smem - hbm) + [HBM] * hbm,
        out_specs=[VMEM] * len(outs),
        out_shape=[jax.ShapeDtypeStruct(s, d) for s, d in outs],
        scratch_shapes=list(scratch),
        compiler_params=PARAMS,
    )


def in_hbm(x):
    return pltpu.with_memory_space_constraint(x, pltpu.HBM)


def swap(x, d):
    return lax.ppermute(x, "ep", [(i, i ^ d) for i in range(EP)])


def share(x):
    return [x] + [swap(x, XS * d) for d in range(1, GRP)]


def trade(parts):
    return [parts[0]] + [swap(parts[d], XS * d) for d in range(1, GRP)]


def copies_kernel(x, *refs):
    for i in range(PLANE):
        refs[-1][i] = x[...]


def gather_columns(weight, after=()):
    mine = weight.T
    line = EP // PLANE
    groups = [[g + line * i for i in range(PLANE)] for g in range(line)]
    copies = pl.pallas_call(
        copies_kernel,
        in_specs=[VMEM] + [pl.BlockSpec(memory_space=pl.ANY)] * len(after),
        out_specs=VMEM,
        out_shape=jax.ShapeDtypeStruct((PLANE, SHARD, D), BF16),
        compiler_params=pltpu.CompilerParams(vmem_limit_bytes=4 * 1024 * 1024),
        name="copies",
    )(mine, *after)
    own = lax.all_to_all(copies, "ep", 0, 0, tiled=True, axis_index_groups=groups)
    return own, swap(own, 1)


def body(
    tokens, lengths, cache_keys, cache_values, mix_gain, mix_out_gain, ffn_gain, ffn_out_gain,
    query_weight, key_weight, value_weight, head_bias, output_weight, routes, route_weights,
    expert_gate, expert_up, expert_down, shared_gate, shared_up, shared_down,
):
    here = lax.axis_index("ep")
    place = jnp.stack([here // XS % GRP, here % 2]).astype(jnp.int32)
    group_tokens = share(tokens)
    own_q, other_q = gather_columns(query_weight)
    route_rows = jnp.tile(routes.T, (1, NJ))
    weight_rows = jnp.tile(route_weights.T, (1, NJ))
    (send,) = call(route_kernel, 1, [((EP * 16, NJ * SEQ), BF16)])(route_rows)
    rows, new_keys, new_values = call(
        norm_kernel, 7, [((GRP * SEQ, D), BF16)] + [((SEQ, 2 * HD), BF16)] * 2
    )(*group_tokens, mix_gain[None], key_weight, value_weight)
    piece = ((SEQ, COLS), BF16)
    load = [pltpu.VMEM((PLANE, 2, SHARD, D), BF16), pltpu.SemaphoreType.DMA((2,))]
    queries = call(
        query_kernel, 4, [piece] * GRP, smem=1, hbm=2, scratch=load
    )(place, rows, in_hbm(own_q), in_hbm(other_q))
    own_o, other_o = gather_columns(output_weight, after=(queries[0],))
    queries = trade(queries)

    whole = lambda *shape: pl.BlockSpec(shape, lambda i: (0,) * len(shape))
    cache_spec = pl.BlockSpec((SUB, LEN, 2 * HD), lambda i: (i, 0, 0))
    attend = pl.pallas_call(
        attend_kernel,
        grid=(SEQ // SUB,),
        in_specs=[SMEM, SMEM] + [whole(SEQ, COLS)] * GRP + [whole(H, 1), cache_spec, cache_spec],
        out_specs=whole(SEQ, D),
        out_shape=jax.ShapeDtypeStruct((SEQ, D), BF16),
        scratch_shapes=[
            pltpu.VMEM((GRP, SEQ, COLS), F32),
            pltpu.VMEM((D, 2 * HD), BF16),
            pltpu.VMEM((BLK, BLK), BF16),
            pltpu.VMEM((SEQ * H, 2 * HD), F32),
        ],
        compiler_params=PARAMS,
        name="attend",
    )
    attended = attend(
        place, lengths, *queries, head_bias[:, None], in_hbm(cache_keys), in_hbm(cache_values)
    )

    mixed = trade(
        call(output_kernel, 7, [piece] * GRP, smem=1, hbm=2, scratch=load)(
            place, *share(attended), in_hbm(own_o), in_hbm(other_o)
        )
    )
    resid1, ffn_in, outgoing = call(
        mix_kernel, 9,
        [((SEQ, D), F32), ((SEQ, D), BF16), ((EP * 16, CH), BF16)],
        smem=1, scratch=[pltpu.VMEM((GRP, SEQ, COLS), BF16)],
    )(place, *mixed, tokens, mix_out_gain[None], ffn_gain[None], send)

    incoming = lax.all_to_all(outgoing.reshape(EP, 16, CH), "ep", 0, 0, tiled=True)
    shared_hidden = (
        jax.nn.silu(dot(ffn_in, shared_gate)) * dot(ffn_in, shared_up)
    ).astype(BF16)
    shared_out = dot(shared_hidden, shared_down)
    (result,) = call(
        expert_kernel, 4, [((EP * 16, CH), BF16)], hbm=3,
        scratch=[
            pltpu.VMEM((EP * CAP, D), BF16),
            pltpu.VMEM((EP * CAP, D), BF16),
            pltpu.VMEM((D, FF), BF16),
            pltpu.VMEM((D, FF), BF16),
            pltpu.VMEM((FF, D), BF16),
            pltpu.SemaphoreType.DMA((3,)),
        ],
    )(incoming.reshape(EP * 16, CH), in_hbm(expert_gate), in_hbm(expert_up), in_hbm(expert_down))
    returned = lax.all_to_all(result.reshape(EP, 16, CH), "ep", 0, 0, tiled=True)
    (layer_out,) = call(final_kernel, 6, [((SEQ, D), BF16)])(
        returned.reshape(EP * 16, CH), route_rows, weight_rows, resid1, shared_out,
        ffn_out_gain[None],
    )
    return (layer_out, new_keys, new_values)


def solution(mesh):
    row, full = P("ep", None), P()
    cube, col = P("ep", None, None), P(None, "ep")
    in_specs = (
        row, P("ep"), cube, cube, full, full, full, full, col, full, full, full, col, row, row,
        cube, cube, cube, full, full, full,
    )

    return jax.shard_map(body, mesh=mesh, in_specs=in_specs, out_specs=(row, row, row), check_vma=False)
```

time: 239 us -> 156 us (0.65)
  waiting for transfers between devices: 139 us -> 27.5 us
  blocking collectives: 0 us -> 70.4 us
  matrix products: 41.4 us -> 4.32 us
  local copies, waits for them, and re-layouts: 28.5 us -> 2.28 us
  Pallas kernels: 0 us -> 25.6 us
  starting transfers between devices: 10.9 us -> 24.6 us
  between operations: 14.3 us -> 0.87 us
  other arithmetic: 4.18 us -> 0.07 us
    all_gather x2 -> x0, waiting for transfers between devices: 103 us -> none  [the longest x1 61 us: body(): lax.all_gather(query_weight, 'ep', axis=1, tiled=True)]
    all_to_all x0 -> x3, blocking collectives: none -> 70.4 us  [the longest x2 43.6 us: gather_columns(): lax.all_to_all(copies, 'ep', 0, 0, tiled=True, axis_index_groups=groups)]
    dot_general x14 -> x2, matrix products: 41.4 us -> 4.32 us  [dot(): return jnp.dot(a, b, preferred_element_type=F32)]
    pallas_call x0 -> x10, Pallas kernels: none -> 25.6 us  [the longest x1 11.1 us: body(): attend(place, lengths, *queries, head_bias[:, None], in_hbm(cache_keys),...]
    ppermute x0 -> x14, starting transfers between devices: none -> 20 us  [swap(): return lax.ppermute(x, 'ep', [(i, i ^ d) for i in range(EP)])]
    all_to_all x2 -> x1, waiting for transfers between devices: 34.4 us -> 14.9 us  [body(): lax.all_to_all(result.reshape(EP, 16, CH), 'ep', 0, 0, tiled=True)]
    unnamed x29 -> x30, local copies, waits for them, and re-layouts: 14.9 us -> 2.03 us
    ppermute x0 -> x14, waiting for transfers between devices: none -> 12.6 us  [swap(): return lax.ppermute(x, 'ep', [(i, i ^ d) for i in range(EP)])]
  transfers between devices with their start and end apart: 4 -> 15, of which waited for: 4 -> 8; matrix products, arithmetic and copies ran while one was open for 19% -> 3% of each run, Pallas kernels for 0% -> 8%
where the time goes in v1:
time: 156 us
  blocking collectives  70.4 us (45%)
  waiting for transfers between devices  27.5 us (18%)
  Pallas kernels  25.6 us (16%)
  starting transfers between devices  24.6 us (16%)
  matrix products  4.32 us (3%)
  local copies, waits for them, and re-layouts  2.28 us (1%)
    all_to_all x2, blocking collectives, gather_columns(): lax.all_to_all(copies, 'ep', 0, 0, tiled=True, axis_index_groups=groups)  43.6 us
    all_to_all x1, blocking collectives, body(): lax.all_to_all(outgoing.reshape(EP, 16, CH), 'ep', 0, 0, tiled=True)  26.8 us
    ppermute x14, starting transfers between devices, swap(): return lax.ppermute(x, 'ep', [(i, i ^ d) for i in range(EP)])  20 us
    all_to_all x1, waiting for transfers between devices, body(): lax.all_to_all(result.reshape(EP, 16, CH), 'ep', 0, 0, tiled=True)  14.9 us
    ppermute x14, waiting for transfers between devices, swap(): return lax.ppermute(x, 'ep', [(i, i ^ d) for i in range(EP)])  12.6 us
    pallas_call x1, Pallas kernels, body(): attend(place, lengths, *queries, head_bias[:, None], in_hbm(cache_keys),...  11.1 us
    all_to_all x1, starting transfers between devices, body(): lax.all_to_all(result.reshape(EP, 16, CH), 'ep', 0, 0, tiled=True)  4.52 us
    pallas_call x1, Pallas kernels, body(): call(expert_kernel, 4, [((EP * 16, CH), BF16)], hbm=3, scratch=[pltpu.VME...  4.35 us
  transfers between devices with their start and end apart: 15, of which 8 were waited for; matrix products, arithmetic and copies ran while one was open for 3% of the time, Pallas kernels for 8%

profile of v1, /device:TPU:1, one launch (start us, length us, event | category | flops | bytes accessed | tf_op | source)
XLA Modules:
  0.0 155.6 jit_solution(5452261549440142144)
XLA Ops:
  0.6 0.0 copy-start
  0.6 0.0 copy-start.4
  0.7 0.0 copy-start.2
  0.7 0.0 copy-start.3
  0.7 1.0 copy-done.5
  1.7 0.1 copies.2
  1.7 24.5 %all_to_all.20.own = bf16[16,16,2048]{2,1,0:T(8,128)(2,1)} all-to-all(bf16[16,16,2048]{2,1,0:T(8,128)(2,1)S(1)} %copies.2), channel_id=1, replica_groups={{0,8,16,24,32,40,48,56,64,72,80,88,96,104,112,120},{1,9,17,25,33,41,49,..., dimensions={0} | all-to-all | bytes 2097152 | tf_op jit(solution)/shard_map/all_to_all | solution.py:282
  26.3 2.1 %collective-permute-start.3 = (bf16[16,16,2048]{2,1,0:T(8,128)(2,1)}, bf16[16,16,2048]{2,1,0:T(8,128)(2,1)}, u32[]{:S(2)}, u32[]{:S(2)}) collective-permute-start(bf16[16,16,2048]{2,1,0:T(8,128)(2,1)} %all_to_all.20.own), channel_id=1, source_target_pairs={{0,1},{1,0},{2,3},{3,2},{4,5},{5,4},{6,7},{7,6},{8,9},{9,8},{10,11... | collective-permute-start | bytes 3145736 | tf_op jit(solution)/shard_map/ppermute | solution.py:254
  28.3 1.2 collective-permute-start
  29.6 2.5 %collective-permute-start.1 = (bf16[16,2048]{1,0:T(8,128)(2,1)S(1)}, bf16[16,2048]{1,0:T(8,128)(2,1)S(1)}, u32[]{:S(2)}, u32[]{:S(2)}) collective-permute-start(bf16[16,2048]{1,0:T(8,128)(2,1)S(1)} %copy-done.4), channel_id=1, source_target_pairs={{0,4},{1,5},{2,6},{3,7},{4,0},{5,1},{6,2},{7,3},{8,12},{9,13},{10,... | collective-permute-start | bytes 196616 | tf_op jit(solution)/shard_map/ppermute | solution.py:254
  32.0 0.2 collective-permute-start.2
  32.2 0.1 pad_add_fusion.place
  32.3 0.0 collective-permute-done.t1
  32.3 3.2 %collective-permute-done.1.t2 = bf16[16,2048]{1,0:T(8,128)(2,1)S(1)} collective-permute-done((bf16[16,2048]{1,0:T(8,128)(2,1)S(1)}, bf16[16,2048]{1,0:T(8,128)(2,1)S(1)}, u32[]{:S(2)}, u32[]{:S(2)}) %collective-permute-start.1) | collective-permute-done | bytes 65568 | tf_op jit(solution)/shard_map/ppermute | solution.py:254
  35.5 1.0 collective-permute-done.2.t3
  36.5 0.0 copy-done.3
  36.5 0.9 shard_map.220
  37.4 0.0 collective-permute-done.3.other
  37.4 2.9 %shard_map.221 = (bf16[16,512]{1,0:T(8,128)(2,1)S(1)}, bf16[16,512]{1,0:T(8,128)(2,1)S(1)}, bf16[16,512]{1,0:T(8,128)(2,1)S(1)}, bf16[16,512]{1,0:T(8,128)(2,1)S(1)}) custom-call(s32[2]{0:T(128)S(1)} %pad_add_fusion.place, bf16[64,2048]{1,0:T(8,128)(2,1)S(1)} %get-tuple-element.17.rows, bf16[16,16,2048]{2,1,0:T(8,128)(2,1)} %all_to_all.20.own, ...), custom_call_target="tpu_custom_call" | custom-call | tf_op jit(solution)/shard_map/pallas_call | solution.py:303
  40.3 0.0 copy-start.14
  40.3 0.0 copy-start.11
  40.3 0.1 copies.3
  40.4 19.1 %all_to_all.21.own = bf16[16,16,2048]{2,1,0:T(8,128)(2,1)} all-to-all(bf16[16,16,2048]{2,1,0:T(8,128)(2,1)S(1)} %copies.3), channel_id=1, replica_groups={{0,8,16,24,32,40,48,56,64,72,80,88,96,104,112,120},{1,9,17,25,33,41,49,..., dimensions={0} | all-to-all | bytes 2097152 | tf_op jit(solution)/shard_map/all_to_all | solution.py:282
  59.5 2.4 %collective-permute-start.10 = (bf16[16,16,2048]{2,1,0:T(8,128)(2,1)}, bf16[16,16,2048]{2,1,0:T(8,128)(2,1)}, u32[]{:S(2)}, u32[]{:S(2)}) collective-permute-start(bf16[16,16,2048]{2,1,0:T(8,128)(2,1)} %all_to_all.21.own), channel_id=1, source_target_pairs={{0,1},{1,0},{2,3},{3,2},{4,5},{5,4},{6,7},{7,6},{8,9},{9,8},{10,11... | collective-permute-start | bytes 3145736 | tf_op jit(solution)/shard_map/ppermute | solution.py:254
  61.9 0.3 collective-permute-start.4
  62.2 2.5 %collective-permute-start.5 = (bf16[16,512]{1,0:T(8,128)(2,1)S(1)}, bf16[16,512]{1,0:T(8,128)(2,1)S(1)}, u32[]{:S(2)}, u32[]{:S(2)}) collective-permute-start(bf16[16,512]{1,0:T(8,128)(2,1)S(1)} %get-tuple-element.20), channel_id=1, source_target_pairs={{0,4},{1,5},{2,6},{3,7},{4,0},{5,1},{6,2},{7,3},{8,12},{9,13},{10,... | collective-permute-start | bytes 49160 | tf_op jit(solution)/shard_map/ppermute | solution.py:254
  64.7 1.0 collective-permute-start.6
  65.7 0.1 copy.24.bias
  65.8 0.0 collective-permute-done.4.q1
  65.8 0.6 collective-permute-done.5.q2
  66.4 2.0 %collective-permute-done.6.q3 = bf16[16,512]{1,0:T(8,128)(2,1)S(1)} collective-permute-done((bf16[16,512]{1,0:T(8,128)(2,1)S(1)}, bf16[16,512]{1,0:T(8,128)(2,1)S(1)}, u32[]{:S(2)}, u32[]{:S(2)}) %collective-permute-start.6) | collective-permute-done | bytes 16416 | tf_op jit(solution)/shard_map/ppermute | solution.py:254
  68.5 11.1 %attend.1.a0 = bf16[16,2048]{1,0:T(8,128)(2,1)S(1)} custom-call(s32[2]{0:T(128)S(1)} %pad_add_fusion.place, s32[16]{0:T(128)S(1)} %copy-done.11, bf16[16,512]{1,0:T(8,128)(2,1)S(1)} %get-tuple-element.18.q0.refs_0_, bf16[16,512]{1,0:T(8,128)(2,1)S(1)} %collective-permute-done.4.q1, bf16[16,512]{1,0:T(8,128)(2,1)S(1)} %collective-permute-done.5.q2, ...), custom_call_target="tpu_custom_call" | custom-call | tf_op jit(solution)/shard_map/attend/pallas_call | solution.py:326
  79.6 0.0 copy-start.12
  79.6 0.0 copy-start.8
  79.6 0.0 copy-start.9
  79.6 0.1 collective-permute-start.7
  79.7 2.2 %collective-permute-start.8 = (bf16[16,2048]{1,0:T(8,128)(2,1)S(1)}, bf16[16,2048]{1,0:T(8,128)(2,1)S(1)}, u32[]{:S(2)}, u32[]{:S(2)}) collective-permute-start(bf16[16,2048]{1,0:T(8,128)(2,1)S(1)} %attend.1.a0), channel_id=1, source_target_pairs={{0,4},{1,5},{2,6},{3,7},{4,0},{5,1},{6,2},{7,3},{8,12},{9,13},{10,... | collective-permute-start | bytes 196616 | tf_op jit(solution)/shard_map/ppermute | solution.py:254
  81.9 1.6 %collective-permute-start.9 = (bf16[16,2048]{1,0:T(8,128)(2,1)S(1)}, bf16[16,2048]{1,0:T(8,128)(2,1)S(1)}, u32[]{:S(2)}, u32[]{:S(2)}) collective-permute-start(bf16[16,2048]{1,0:T(8,128)(2,1)S(1)} %attend.1.a0), channel_id=1, source_target_pairs={{0,6},{1,7},{2,4},{3,5},{4,2},{5,3},{6,0},{7,1},{8,14},{9,15},{10,... | collective-permute-start | bytes 196616 | tf_op jit(solution)/shard_map/ppermute | solution.py:254
  83.6 0.0 collective-permute-done.7.a1
  83.6 0.9 collective-permute-done.8.a2
  84.4 2.5 %collective-permute-done.9.a3 = bf16[16,2048]{1,0:T(8,128)(2,1)S(1)} collective-permute-done((bf16[16,2048]{1,0:T(8,128)(2,1)S(1)}, bf16[16,2048]{1,0:T(8,128)(2,1)S(1)}, u32[]{:S(2)}, u32[]{:S(2)}) %collective-permute-start.9) | collective-permute-done | bytes 65568 | tf_op jit(solution)/shard_map/ppermute | solution.py:254
  87.0 0.0 collective-permute-done.10.other
  87.0 2.9 %shard_map.222 = (bf16[16,512]{1,0:T(8,128)(2,1)S(1)}, bf16[16,512]{1,0:T(8,128)(2,1)S(1)}, bf16[16,512]{1,0:T(8,128)(2,1)S(1)}, bf16[16,512]{1,0:T(8,128)(2,1)S(1)}) custom-call(s32[2]{0:T(128)S(1)} %pad_add_fusion.place, bf16[16,2048]{1,0:T(8,128)(2,1)S(1)} %attend.1.a0, bf16[16,2048]{1,0:T(8,128)(2,1)S(1)} %collective-permute-done.7.a1, ...), custom_call_target="tpu_custom_call" | custom-call | tf_op jit(solution)/shard_map/pallas_call | solution.py:331
  89.8 0.1 collective-permute-start.11
  89.9 2.8 %collective-permute-start.12 = (bf16[16,512]{1,0:T(8,128)(2,1)S(1)}, bf16[16,512]{1,0:T(8,128)(2,1)S(1)}, u32[]{:S(2)}, u32[]{:S(2)}) collective-permute-start(bf16[16,512]{1,0:T(8,128)(2,1)S(1)} %get-tuple-element.24), channel_id=1, source_target_pairs={{0,4},{1,5},{2,6},{3,7},{4,0},{5,1},{6,2},{7,3},{8,12},{9,13},{10,... | collective-permute-start | bytes 49160 | tf_op jit(solution)/shard_map/ppermute | solution.py:254
  92.7 1.0 collective-permute-start.13
  93.8 0.1 tile.9.routes
  93.9 0.3 shard_map.223.send
  94.2 0.0 collective-permute-done.11.m1
  94.2 0.0 collective-permute-done.12.m2
  94.2 2.3 %collective-permute-done.13.m3 = bf16[16,512]{1,0:T(8,128)(2,1)S(1)} collective-permute-done((bf16[16,512]{1,0:T(8,128)(2,1)S(1)}, bf16[16,512]{1,0:T(8,128)(2,1)S(1)}, u32[]{:S(2)}, u32[]{:S(2)}) %collective-permute-start.13) | collective-permute-done | bytes 16416 | tf_op jit(solution)/shard_map/ppermute | solution.py:254
  96.6 1.6 %shard_map.224 = (f32[16,2048]{1,0:T(8,128)S(1)}, bf16[16,2048]{1,0:T(8,128)(2,1)S(1)}, bf16[2048,256]{1,0:T(8,128)(2,1)S(1)}) custom-call(s32[2]{0:T(128)S(1)} %pad_add_fusion.place, bf16[16,512]{1,0:T(8,128)(2,1)S(1)} %get-tuple-element.22.m0, bf16[16,512]{1,0:T(8,128)(2,1)S(1)} %collective-permute-done.11.m1, ...), custom_call_target="tpu_custom_call" | custom-call | tf_op jit(solution)/shard_map/pallas_call | solution.py:335
  98.1 26.8 %all_to_all.22 = bf16[128,16,256]{2,1,0:T(8,128)(2,1)S(1)} all-to-all(bf16[128,16,256]{2,1,0:T(8,128)(2,1)S(1)} %bitcast.23), channel_id=1, replica_groups=mesh['ep'=128] {'ep'}, dimensions={0} | all-to-all | bytes 2097152 | tf_op jit(solution)/shard_map/all_to_all | solution.py:341
  124.9 4.3 %shard_map.225 = bf16[2048,256]{1,0:T(8,128)(2,1)S(1)} custom-call(bf16[2048,256]{1,0:T(8,128)(2,1)S(1)} %bitcast.22, bf16[1,2048,512]{2,1,0:T(8,128)(2,1)} %gate.1, bf16[1,2048,512]{2,1,0:T(8,128)(2,1)} %up.1, bf16[1,512,2048]{2,1,0:T(8,128)(2,1)} %down.1), custom_call_target="tpu_custom_call" | custom-call | tf_op jit(solution)/shard_map/pallas_call | solution.py:346
  129.3 0.0 copy-start.1
  129.3 1.0 copy-done.1
  130.3 4.5 %all-to-all-start.3 = ((bf16[128,16,256]{2,1,0:T(8,128)(2,1)}), bf16[128,16,256]{2,1,0:T(8,128)(2,1)S(1)}, u32[]{:S(2)}, u32[]{:S(2)}) async-start(bf16[128,16,256]{2,1,0:T(8,128)(2,1)} %bitcast.21), calls=%async_computation.3 | async-start | bytes 2097152 | tf_op jit(solution)/shard_map/all_to_all | solution.py:357
  134.8 0.1 tile.21.weights
  134.9 2.0 %fusion.5 = f32[16,512]{1,0:T(8,128)S(1)} fusion(bf16[16,2048]{1,0:T(8,128)(2,1)S(1)} %get-tuple-element.28, bf16[2048,512]{1,0:T(8,128)(2,1)} %param.39), kind=kOutput, calls=%fused_computation.6 | convolution fusion | flops 33554432 | bytes 2195456 | tf_op jit(solution)/shard_map/dot_general | solution.py:44
  136.9 0.0 copy-done
  136.9 2.4 %fusion.shared = f32[16,2048]{1,0:T(8,128)S(1)} fusion(bf16[512,2048]{1,0:T(8,128)(2,1)S(1)} %copy-done, f32[16,512]{1,0:T(8,128)S(1)} %fusion.5, bf16[16,2048]{1,0:T(8,128)(2,1)S(1)} %get-tuple-element.28, bf16[2048,512]{1,0:T(8,128)(2,1)} %param.40), kind=kOutput, calls=%fused_computation.1 | convolution fusion | flops 67158016 | bytes 4423680 | tf_op jit(solution)/shard_map/dot_general | solution.py:44
  139.2 14.9 %all-to-all-done.3 = bf16[128,16,256]{2,1,0:T(8,128)(2,1)S(1)} async-done(((bf16[128,16,256]{2,1,0:T(8,128)(2,1)}), bf16[128,16,256]{2,1,0:T(8,128)(2,1)S(1)}, u32[]{:S(2)}, u32[]{:S(2)}) %all-to-all-start.3) | async-done | bytes 1048608 | tf_op jit(solution)/shard_map/all_to_all | solution.py:357
  154.2 0.0 copy-done.10
  154.2 1.5 shard_map.226
  (17 shorter events, 0.0 us)
Async XLA Ops:
  0.6 136.2 %copy-start = (bf16[512,2048]{1,0:T(8,128)(2,1)S(1)}, bf16[512,2048]{1,0:T(8,128)(2,1)}, u32[]{:S(2)}) copy-start(bf16[512,2048]{1,0:T(8,128)(2,1)} %param.41) | copy-start | bytes 6291460
  0.6 27.7 %copy-start.4 = (bf16[16,2048]{1,0:T(8,128)(2,1)S(1)}, bf16[16,2048]{1,0:T(8,128)(2,1)}, u32[]{:S(2)}) copy-start(bf16[16,2048]{1,0:T(8,128)(2,1)} %tokens.1) | copy-start | bytes 196612
  0.7 35.8 %copy-start.2 = (bf16[2048,128]{1,0:T(8,128)(2,1)S(1)}, bf16[2048,128]{1,0:T(8,128)(2,1)}, u32[]{:S(2)}) copy-start(bf16[2048,128]{1,0:T(8,128)(2,1)} %wk.1) | copy-start | bytes 1572868
  0.7 35.8 %copy-start.3 = (bf16[2048,128]{1,0:T(8,128)(2,1)S(1)}, bf16[2048,128]{1,0:T(8,128)(2,1)}, u32[]{:S(2)}) copy-start(bf16[2048,128]{1,0:T(8,128)(2,1)} %wv.1) | copy-start | bytes 1572868
  0.7 1.0 copy-start.5
  1.7 34.8 %copy-start.7 = (f32[2048]{0:T(1024)S(1)}, f32[2048]{0:T(1024)}, u32[]{:S(2)}) copy-start(f32[2048]{0:T(1024)} %param.25) | copy-start | bytes 24580
  26.3 14.0 %copy-start.6 = (bf16[2048,16]{0,1:T(8,128)(2,1)S(1)}, bf16[2048,16]{0,1:T(8,128)(2,1)}, u32[]{:S(2)}) copy-start(bf16[2048,16]{0,1:T(8,128)(2,1)} %param.33) | copy-start | bytes 196612
  26.3 11.1 %collective-permute-start.3 = (bf16[16,16,2048]{2,1,0:T(8,128)(2,1)}, bf16[16,16,2048]{2,1,0:T(8,128)(2,1)}, u32[]{:S(2)}, u32[]{:S(2)}) collective-permute-start(bf16[16,16,2048]{2,1,0:T(8,128)(2,1)} %all_to_all.20.own), channel_id=1, source_target_pairs={{0,1},{1,0},{2,3},{3,2},{4,5},{5,4},{6,7},{7,6},{8,9},{9,8},{10,11... | collective-permute-start | bytes 3145736 | tf_op jit(solution)/shard_map/ppermute | solution.py:254
  28.3 3.9 %collective-permute-start = (bf16[16,2048]{1,0:T(8,128)(2,1)S(1)}, bf16[16,2048]{1,0:T(8,128)(2,1)S(1)}, u32[]{:S(2)}, u32[]{:S(2)}) collective-permute-start(bf16[16,2048]{1,0:T(8,128)(2,1)S(1)} %copy-done.4), channel_id=1, source_target_pairs={{0,2},{1,3},{2,0},{3,1},{4,6},{5,7},{6,4},{7,5},{8,10},{9,11},{10,... | collective-permute-start | bytes 196616 | tf_op jit(solution)/shard_map/ppermute | solution.py:254
  29.6 6.0 %collective-permute-start.1 = (bf16[16,2048]{1,0:T(8,128)(2,1)S(1)}, bf16[16,2048]{1,0:T(8,128)(2,1)S(1)}, u32[]{:S(2)}, u32[]{:S(2)}) collective-permute-start(bf16[16,2048]{1,0:T(8,128)(2,1)S(1)} %copy-done.4), channel_id=1, source_target_pairs={{0,4},{1,5},{2,6},{3,7},{4,0},{5,1},{6,2},{7,3},{8,12},{9,13},{10,... | collective-permute-start | bytes 196616 | tf_op jit(solution)/shard_map/ppermute | solution.py:254
  32.0 4.5 %collective-permute-start.2 = (bf16[16,2048]{1,0:T(8,128)(2,1)S(1)}, bf16[16,2048]{1,0:T(8,128)(2,1)S(1)}, u32[]{:S(2)}, u32[]{:S(2)}) collective-permute-start(bf16[16,2048]{1,0:T(8,128)(2,1)S(1)} %copy-done.4), channel_id=1, source_target_pairs={{0,6},{1,7},{2,4},{3,5},{4,2},{5,3},{6,0},{7,1},{8,14},{9,15},{10,... | collective-permute-start | bytes 196616 | tf_op jit(solution)/shard_map/ppermute | solution.py:254
  40.3 25.4 %copy-start.14 = (f32[32]{0:T(128)S(1)}, f32[32]{0:T(128)}, u32[]{:S(2)}) copy-start(f32[32]{0:T(128)} %param.32) | copy-start | bytes 388
  40.3 28.2 %copy-start.11 = (s32[16]{0:T(128)S(1)}, s32[16]{0:T(128)}, u32[]{:S(2)}) copy-start(s32[16]{0:T(128)} %lens.1) | copy-start | bytes 196
  59.5 27.5 %collective-permute-start.10 = (bf16[16,16,2048]{2,1,0:T(8,128)(2,1)}, bf16[16,16,2048]{2,1,0:T(8,128)(2,1)}, u32[]{:S(2)}, u32[]{:S(2)}) collective-permute-start(bf16[16,16,2048]{2,1,0:T(8,128)(2,1)} %all_to_all.21.own), channel_id=1, source_target_pairs={{0,1},{1,0},{2,3},{3,2},{4,5},{5,4},{6,7},{7,6},{8,9},{9,8},{10,11... | collective-permute-start | bytes 3145736 | tf_op jit(solution)/shard_map/ppermute | solution.py:254
  61.9 4.0 %collective-permute-start.4 = (bf16[16,512]{1,0:T(8,128)(2,1)S(1)}, bf16[16,512]{1,0:T(8,128)(2,1)S(1)}, u32[]{:S(2)}, u32[]{:S(2)}) collective-permute-start(bf16[16,512]{1,0:T(8,128)(2,1)S(1)} %get-tuple-element.19), channel_id=1, source_target_pairs={{0,2},{1,3},{2,0},{3,1},{4,6},{5,7},{6,4},{7,5},{8,10},{9,11},{10,... | collective-permute-start | bytes 49160 | tf_op jit(solution)/shard_map/ppermute | solution.py:254
  62.2 4.3 %collective-permute-start.5 = (bf16[16,512]{1,0:T(8,128)(2,1)S(1)}, bf16[16,512]{1,0:T(8,128)(2,1)S(1)}, u32[]{:S(2)}, u32[]{:S(2)}) collective-permute-start(bf16[16,512]{1,0:T(8,128)(2,1)S(1)} %get-tuple-element.20), channel_id=1, source_target_pairs={{0,4},{1,5},{2,6},{3,7},{4,0},{5,1},{6,2},{7,3},{8,12},{9,13},{10,... | collective-permute-start | bytes 49160 | tf_op jit(solution)/shard_map/ppermute | solution.py:254
  64.7 3.8 %collective-permute-start.6 = (bf16[16,512]{1,0:T(8,128)(2,1)S(1)}, bf16[16,512]{1,0:T(8,128)(2,1)S(1)}, u32[]{:S(2)}, u32[]{:S(2)}) collective-permute-start(bf16[16,512]{1,0:T(8,128)(2,1)S(1)} %get-tuple-element.21), channel_id=1, source_target_pairs={{0,6},{1,7},{2,4},{3,5},{4,2},{5,3},{6,0},{7,1},{8,14},{9,15},{10,... | collective-permute-start | bytes 49160 | tf_op jit(solution)/shard_map/ppermute | solution.py:254
  79.6 14.2 %copy-start.12 = (s32[16,6]{0,1:T(8,128)S(1)}, s32[16,6]{0,1:T(8,128)}, u32[]{:S(2)}) copy-start(s32[16,6]{0,1:T(8,128)} %param.34) | copy-start | bytes 1156
  79.6 16.9 %copy-start.8 = (f32[2048]{0:T(1024)S(1)}, f32[2048]{0:T(1024)}, u32[]{:S(2)}) copy-start(f32[2048]{0:T(1024)} %param.26) | copy-start | bytes 24580
  79.6 16.9 %copy-start.9 = (f32[2048]{0:T(1024)S(1)}, f32[2048]{0:T(1024)}, u32[]{:S(2)}) copy-start(f32[2048]{0:T(1024)} %param.27) | copy-start | bytes 24580
  79.6 3.9 %collective-permute-start.7 = (bf16[16,2048]{1,0:T(8,128)(2,1)S(1)}, bf16[16,2048]{1,0:T(8,128)(2,1)S(1)}, u32[]{:S(2)}, u32[]{:S(2)}) collective-permute-start(bf16[16,2048]{1,0:T(8,128)(2,1)S(1)} %attend.1.a0), channel_id=1, source_target_pairs={{0,2},{1,3},{2,0},{3,1},{4,6},{5,7},{6,4},{7,5},{8,10},{9,11},{10,... | collective-permute-start | bytes 196616 | tf_op jit(solution)/shard_map/ppermute | solution.py:254
  79.7 4.7 %collective-permute-start.8 = (bf16[16,2048]{1,0:T(8,128)(2,1)S(1)}, bf16[16,2048]{1,0:T(8,128)(2,1)S(1)}, u32[]{:S(2)}, u32[]{:S(2)}) collective-permute-start(bf16[16,2048]{1,0:T(8,128)(2,1)S(1)} %attend.1.a0), channel_id=1, source_target_pairs={{0,4},{1,5},{2,6},{3,7},{4,0},{5,1},{6,2},{7,3},{8,12},{9,13},{10,... | collective-permute-start | bytes 196616 | tf_op jit(solution)/shard_map/ppermute | solution.py:254
  81.9 5.0 %collective-permute-start.9 = (bf16[16,2048]{1,0:T(8,128)(2,1)S(1)}, bf16[16,2048]{1,0:T(8,128)(2,1)S(1)}, u32[]{:S(2)}, u32[]{:S(2)}) collective-permute-start(bf16[16,2048]{1,0:T(8,128)(2,1)S(1)} %attend.1.a0), channel_id=1, source_target_pairs={{0,6},{1,7},{2,4},{3,5},{4,2},{5,3},{6,0},{7,1},{8,14},{9,15},{10,... | collective-permute-start | bytes 196616 | tf_op jit(solution)/shard_map/ppermute | solution.py:254
  89.8 4.3 %collective-permute-start.11 = (bf16[16,512]{1,0:T(8,128)(2,1)S(1)}, bf16[16,512]{1,0:T(8,128)(2,1)S(1)}, u32[]{:S(2)}, u32[]{:S(2)}) collective-permute-start(bf16[16,512]{1,0:T(8,128)(2,1)S(1)} %get-tuple-element.23), channel_id=1, source_target_pairs={{0,2},{1,3},{2,0},{3,1},{4,6},{5,7},{6,4},{7,5},{8,10},{9,11},{10,... | collective-permute-start | bytes 49160 | tf_op jit(solution)/shard_map/ppermute | solution.py:254
  89.9 4.3 %collective-permute-start.12 = (bf16[16,512]{1,0:T(8,128)(2,1)S(1)}, bf16[16,512]{1,0:T(8,128)(2,1)S(1)}, u32[]{:S(2)}, u32[]{:S(2)}) collective-permute-start(bf16[16,512]{1,0:T(8,128)(2,1)S(1)} %get-tuple-element.24), channel_id=1, source_target_pairs={{0,4},{1,5},{2,6},{3,7},{4,0},{5,1},{6,2},{7,3},{8,12},{9,13},{10,... | collective-permute-start | bytes 49160 | tf_op jit(solution)/shard_map/ppermute | solution.py:254
  92.7 3.8 %collective-permute-start.13 = (bf16[16,512]{1,0:T(8,128)(2,1)S(1)}, bf16[16,512]{1,0:T(8,128)(2,1)S(1)}, u32[]{:S(2)}, u32[]{:S(2)}) collective-permute-start(bf16[16,512]{1,0:T(8,128)(2,1)S(1)} %get-tuple-element.25), channel_id=1, source_target_pairs={{0,6},{1,7},{2,4},{3,5},{4,2},{5,3},{6,0},{7,1},{8,14},{9,15},{10,... | collective-permute-start | bytes 49160 | tf_op jit(solution)/shard_map/ppermute | solution.py:254
  129.3 1.0 copy-start.1
  130.3 4.5 %copy-start.13 = (f32[16,6]{0,1:T(8,128)S(1)}, f32[16,6]{0,1:T(8,128)}, u32[]{:S(2)}) copy-start(f32[16,6]{0,1:T(8,128)} %param.35) | copy-start | bytes 1156
  130.3 23.9 %all-to-all-start.3 = ((bf16[128,16,256]{2,1,0:T(8,128)(2,1)}), bf16[128,16,256]{2,1,0:T(8,128)(2,1)S(1)}, u32[]{:S(2)}, u32[]{:S(2)}) async-start(bf16[128,16,256]{2,1,0:T(8,128)(2,1)} %bitcast.21), calls=%async_computation.3 | async-start | bytes 2097152 | tf_op jit(solution)/shard_map/all_to_all | solution.py:357
  136.9 17.3 %copy-start.10 = (f32[2048]{0:T(1024)S(1)}, f32[2048]{0:T(1024)}, u32[]{:S(2)}) copy-start(f32[2048]{0:T(1024)} %param.28) | copy-start | bytes 24580

commit v2 on v1

--- a/solution.py
+++ b/solution.py
@@ -48,20 +48,16 @@
     return lax.dot_general(a, b, (((1,), (1,)), ((), ())), preferred_element_type=F32)
 
 
-def start_columns(own, other, core, full, sems):
-    copies = [
-        pltpu.make_async_copy(own, full.at[:, core], sems.at[0]),
-        pltpu.make_async_copy(other, full.at[:, 1 - core], sems.at[1]),
-    ]
-    for c in copies:
-        c.start()
-    return copies
-
-
-def columns(copies, full):
-    for c in copies:
-        c.wait()
-    return full[...].reshape(COLS, D)
+def project(place, rows, own, other, outs):
+    for core in range(2):
+
+        @pl.when(place[1] == core)
+        def _():
+            pair = (own, other) if core == 0 else (other, own)
+            weight = jnp.concatenate([pair[c][p] for p in range(PLANE) for c in range(2)], axis=0)
+            out = dot_nt(rows, weight).astype(BF16)
+            for i, o in enumerate(outs):
+                o[...] = out[i * SEQ : (i + 1) * SEQ]
 
 
 def norm_kernel(t0, t1, t2, t3, gain, wk, wv, rows, nk, nv):
@@ -72,60 +68,62 @@
     nv[...] = dot(mine, wv[...]).astype(BF16)
 
 
-def query_kernel(place, rows, own, other, q0, q1, q2, q3, full, sems):
-    copies = start_columns(own, other, place[1], full, sems)
-    out = dot_nt(rows[...], columns(copies, full)).astype(BF16)
-    for i, q in enumerate((q0, q1, q2, q3)):
-        q[...] = out[i * SEQ : (i + 1) * SEQ]
-
-
-SUB = 4
+def query_kernel(place, rows, own, other, *outs):
+    project(place, rows[...], own, other, outs)
+
+
+SUB = 8
 BLK = 256
 
 
-def attend_kernel(place, lens, q0, q1, q2, q3, bias, keys, values, out, qf, sel, upper, att):
+def attend_kernel(place, lens, q0, q1, q2, q3, bias, keys, values, out, qf, placed, upper, att):
     step = pl.program_id(0)
 
     @pl.when(step == 0)
     def _():
+        upper[...] = (iota((BLK, BLK), 0) > iota((BLK, BLK), 1)).astype(F32).astype(BF16)
         for i, q in enumerate((q0, q1, q2, q3)):
             qf[i] = q[...].astype(F32) * HD ** (-0.5)
-        row, col = iota((D, 2 * HD), 0), iota((D, 2 * HD), 1)
-        x, plane, k = row >> 9, (row >> 5) & (PLANE - 1), row & 31
-        sel[...] = (col == (plane >> 3) * HD + (x & 1) * 32 + k).astype(F32).astype(BF16)
-        upper[...] = (iota((BLK, BLK), 0) > iota((BLK, BLK), 1)).astype(F32).astype(BF16)
-
-    own = place[0]
-    plane = (iota((H, COLS), 1) >> 5) * 2
-    masks = [plane + half == iota((H, COLS), 0) for half in range(2)]
-    spread = []
+        row, col = iota((COLS, 2 * HD), 0), iota((COLS, 2 * HD), 1)
+        plane = iota((H, COLS), 1) >> 5
+        spread = [[] for _ in range(SEQ)]
+        select = []
+        for m in range(GRP):
+            target = (row >> 8) * HD + (m & 1) * 32 + (row & 31)
+            select.append((col == target).astype(F32).astype(BF16))
+            mask = plane * 2 + (m >> 1) == iota((H, COLS), 0)
+            part = qf[place[0] ^ m]
+            for u in range(SEQ):
+                rows = jnp.broadcast_to(part[u : u + 1], (H, COLS))
+                spread[u].append(jnp.where(mask, rows, 0.0).astype(BF16))
+        spread = jnp.concatenate([jnp.concatenate(p, axis=1) for p in spread], axis=0)
+        placed[...] = dot(spread, jnp.concatenate(select, axis=0)).astype(BF16)
+
+    count = LEN // BLK
+    first = pl.multiple_of(step * SUB * H, SUB * H)
+    valid, beta, keep, stacked = [], [], [], []
     for u in range(SUB):
-        parts = []
-        for m in range(GRP):
-            row = qf[own ^ m, pl.ds(step * SUB + u, 1), :]
-            parts.append(jnp.where(masks[m >> 1], jnp.broadcast_to(row, (H, COLS)), 0.0).astype(BF16))
-        spread.append(jnp.concatenate(parts, axis=1))
-    placed = dot(jnp.concatenate(spread, axis=0), sel[...]).astype(BF16)
+        z = dot_nt(placed[pl.ds(first + u * H, H), :], keys[u]) + bias[...]
+        valid.append(iota((H, LEN), 1) < lens[step * SUB + u])
+        soft = jnp.log(1.0 + jnp.exp(-jnp.abs(z)))
+        beta.append(jnp.minimum(z, 0.0) - soft)
+        keep.append(jnp.where(valid[u], beta[u] - z, 0.0))
+        high = keep[u].astype(BF16)
+        low = (keep[u] - high.astype(F32)).astype(BF16)
+        for b in range(count):
+            stacked += [high[:, b * BLK : (b + 1) * BLK], low[:, b * BLK : (b + 1) * BLK]]
+    later = dot(jnp.concatenate(stacked, axis=0), upper[...])
     for u in range(SUB):
-        z = dot_nt(placed[u * H : (u + 1) * H], keys[u]) + bias[...]
-        n = lens[step * SUB + u]
-        valid = iota((H, LEN), 1) < n
-        soft = jnp.log(1.0 + jnp.exp(-jnp.abs(z)))
-        log_beta = jnp.minimum(z, 0.0) - soft
-        log_keep = jnp.where(valid, log_beta - z, 0.0)
-        high = log_keep.astype(BF16)
-        low = (log_keep - high.astype(F32)).astype(BF16)
         carry = jnp.zeros((H, 1), F32)
         blocks = []
-        for b in range(LEN // BLK - 1, -1, -1):
-            s = slice(b * BLK, (b + 1) * BLK)
-            both = dot(jnp.concatenate([high[:, s], low[:, s]], axis=0), upper[...])
-            after = both[:H] + both[H:]
+        for b in range(count - 1, -1, -1):
+            at = (u * count + b) * 2 * H
+            after = later[at : at + H] + later[at + H : at + 2 * H]
             blocks.append(after + carry)
-            carry = carry + after[:, :1] + log_keep[:, s][:, :1]
+            carry = carry + after[:, :1] + keep[u][:, b * BLK : b * BLK + 1]
         after = jnp.concatenate(blocks[::-1], axis=1)
-        weights = jnp.where(valid, jnp.exp(log_beta + after), 0.0).astype(BF16)
-        att[pl.ds((step * SUB + u) * H, H), :] = dot(weights, values[u])
+        weights = jnp.where(valid[u], jnp.exp(beta[u] + after), 0.0).astype(BF16)
+        att[pl.ds(first + u * H, H), :] = dot(weights, values[u])
 
     @pl.when(step == SEQ // SUB - 1)
     def _():
@@ -140,12 +138,9 @@
             out[:, i * 2 * HD : (i + 1) * 2 * HD] = jnp.where(left, even, odd).astype(BF16)
 
 
-def output_kernel(place, a0, a1, a2, a3, own, other, m0, m1, m2, m3, full, sems):
-    copies = start_columns(own, other, place[1], full, sems)
+def output_kernel(place, a0, a1, a2, a3, own, other, *outs):
     rows = jnp.concatenate([a[...] for a in (a0, a1, a2, a3)], axis=0)
-    out = dot_nt(rows, columns(copies, full)).astype(BF16)
-    for i, m in enumerate((m0, m1, m2, m3)):
-        m[...] = out[i * SEQ : (i + 1) * SEQ]
+    project(place, rows, own, other, outs)
 
 
 def places(routes, weights):
@@ -170,11 +165,7 @@
     return (x[:, None, :] * block[None, :, :]).reshape(EP * CAP * NJ, NJ * SEQ)
 
 
-def route_kernel(routes, send):
-    send[...] = expand(places(routes, None)).astype(BF16)
-
-
-def mix_kernel(place, m0, m1, m2, m3, tokens, mix_gain, ffn_gain, send, resid1, ffn_in, outgoing, pieces):
+def mix_kernel(place, m0, m1, m2, m3, tokens, mix_gain, ffn_gain, routes, resid1, ffn_in, outgoing, pieces):
     for i, m in enumerate((m0, m1, m2, m3)):
         pieces[i] = m[...]
     own = place[0]
@@ -193,13 +184,14 @@
     x = rms(r1, ffn_gain[...]).astype(BF16)
     ffn_in[...] = x
     blocks = jnp.concatenate([x[:, j * CH : (j + 1) * CH] for j in range(NJ)], axis=0)
-    outgoing[...] = dot(send[...], blocks).astype(BF16)
-
-
-def expert_kernel(incoming, gate, up, down, outgoing, rows, result, wg, wu, wd, sems):
+    send = expand(places(routes, None)).astype(BF16)
+    outgoing[...] = dot(send, blocks).astype(BF16)
+
+
+def expert_kernel(incoming, gate, up, down, outgoing, rows, result, wu, wd, sems):
     copies = [
         pltpu.make_async_copy(w.at[0], v, sems.at[i])
-        for i, (w, v) in enumerate(((gate, wg), (up, wu), (down, wd)))
+        for i, (w, v) in enumerate(((up, wu), (down, wd)))
     ]
     for c in copies:
         c.start()
@@ -212,11 +204,10 @@
         for j in range(NJ):
             rows[g * 32 : (g + 1) * 32, j * CH : (j + 1) * CH] = block[j * 32 : (j + 1) * 32]
     x = rows[...]
+    gated = jax.nn.silu(dot(x, gate[0]))
     copies[0].wait()
-    gated = jax.nn.silu(dot(x, wg[...]))
+    hidden = (gated * dot(x, wu[...])).astype(BF16)
     copies[1].wait()
-    hidden = (gated * dot(x, wu[...])).astype(BF16)
-    copies[2].wait()
     result[...] = dot(hidden, wd[...]).astype(BF16)
     for g in range(EP * 16 // n):
         block = jnp.concatenate(
@@ -262,23 +253,22 @@
     return [parts[0]] + [swap(parts[d], XS * d) for d in range(1, GRP)]
 
 
-def copies_kernel(x, *refs):
+def copies_kernel(x, out):
     for i in range(PLANE):
-        refs[-1][i] = x[...]
-
-
-def gather_columns(weight, after=()):
-    mine = weight.T
+        out[i] = x[...]
+
+
+def gather_columns(weight):
     line = EP // PLANE
     groups = [[g + line * i for i in range(PLANE)] for g in range(line)]
     copies = pl.pallas_call(
         copies_kernel,
-        in_specs=[VMEM] + [pl.BlockSpec(memory_space=pl.ANY)] * len(after),
+        in_specs=[VMEM],
         out_specs=VMEM,
         out_shape=jax.ShapeDtypeStruct((PLANE, SHARD, D), BF16),
         compiler_params=pltpu.CompilerParams(vmem_limit_bytes=4 * 1024 * 1024),
         name="copies",
-    )(mine, *after)
+    )(weight.T)
     own = lax.all_to_all(copies, "ep", 0, 0, tiled=True, axis_index_groups=groups)
     return own, swap(own, 1)
 
@@ -294,16 +284,12 @@
     own_q, other_q = gather_columns(query_weight)
     route_rows = jnp.tile(routes.T, (1, NJ))
     weight_rows = jnp.tile(route_weights.T, (1, NJ))
-    (send,) = call(route_kernel, 1, [((EP * 16, NJ * SEQ), BF16)])(route_rows)
     rows, new_keys, new_values = call(
         norm_kernel, 7, [((GRP * SEQ, D), BF16)] + [((SEQ, 2 * HD), BF16)] * 2
     )(*group_tokens, mix_gain[None], key_weight, value_weight)
     piece = ((SEQ, COLS), BF16)
-    load = [pltpu.VMEM((PLANE, 2, SHARD, D), BF16), pltpu.SemaphoreType.DMA((2,))]
-    queries = call(
-        query_kernel, 4, [piece] * GRP, smem=1, hbm=2, scratch=load
-    )(place, rows, in_hbm(own_q), in_hbm(other_q))
-    own_o, other_o = gather_columns(output_weight, after=(queries[0],))
+    queries = call(query_kernel, 4, [piece] * GRP, smem=1)(place, rows, own_q, other_q)
+    own_o, other_o = gather_columns(output_weight)
     queries = trade(queries)
 
     whole = lambda *shape: pl.BlockSpec(shape, lambda i: (0,) * len(shape))
@@ -316,7 +302,7 @@
         out_shape=jax.ShapeDtypeStruct((SEQ, D), BF16),
         scratch_shapes=[
             pltpu.VMEM((GRP, SEQ, COLS), F32),
-            pltpu.VMEM((D, 2 * HD), BF16),
+            pltpu.VMEM((SEQ * H, 2 * HD), BF16),
             pltpu.VMEM((BLK, BLK), BF16),
             pltpu.VMEM((SEQ * H, 2 * HD), F32),
         ],
@@ -328,32 +314,34 @@
     )
 
     mixed = trade(
-        call(output_kernel, 7, [piece] * GRP, smem=1, hbm=2, scratch=load)(
-            place, *share(attended), in_hbm(own_o), in_hbm(other_o)
-        )
+        call(output_kernel, 7, [piece] * GRP, smem=1)(place, *share(attended), own_o, other_o)
     )
     resid1, ffn_in, outgoing = call(
         mix_kernel, 9,
         [((SEQ, D), F32), ((SEQ, D), BF16), ((EP * 16, CH), BF16)],
         smem=1, scratch=[pltpu.VMEM((GRP, SEQ, COLS), BF16)],
-    )(place, *mixed, tokens, mix_out_gain[None], ffn_gain[None], send)
+    )(place, *mixed, tokens, mix_out_gain[None], ffn_gain[None], route_rows)
 
     incoming = lax.all_to_all(outgoing.reshape(EP, 16, CH), "ep", 0, 0, tiled=True)
     shared_hidden = (
         jax.nn.silu(dot(ffn_in, shared_gate)) * dot(ffn_in, shared_up)
     ).astype(BF16)
     shared_out = dot(shared_hidden, shared_down)
-    (result,) = call(
-        expert_kernel, 4, [((EP * 16, CH), BF16)], hbm=3,
-        scratch=[
+    result = pl.pallas_call(
+        expert_kernel,
+        in_specs=[VMEM, VMEM, HBM, HBM],
+        out_specs=VMEM,
+        out_shape=jax.ShapeDtypeStruct((EP * 16, CH), BF16),
+        scratch_shapes=[
             pltpu.VMEM((EP * CAP, D), BF16),
             pltpu.VMEM((EP * CAP, D), BF16),
             pltpu.VMEM((D, FF), BF16),
-            pltpu.VMEM((D, FF), BF16),
             pltpu.VMEM((FF, D), BF16),
-            pltpu.SemaphoreType.DMA((3,)),
+            pltpu.SemaphoreType.DMA((2,)),
         ],
-    )(incoming.reshape(EP * 16, CH), in_hbm(expert_gate), in_hbm(expert_up), in_hbm(expert_down))
+        compiler_params=PARAMS,
+        name="expert",
+    )(incoming.reshape(EP * 16, CH), expert_gate, in_hbm(expert_up), in_hbm(expert_down))
     returned = lax.all_to_all(result.reshape(EP, 16, CH), "ep", 0, 0, tiled=True)
     (layer_out,) = call(final_kernel, 6, [((SEQ, D), BF16)])(
         returned.reshape(EP * 16, CH), route_rows, weight_rows, resid1, shared_out,

time: 156 us -> 156 us (level)
  blocking collectives: 70.4 us -> 29 us
  waiting for transfers between devices: 27.5 us -> 55.2 us
  starting transfers between devices: 24.6 us -> 38.3 us
  Pallas kernels: 25.6 us -> 19 us
  local copies, waits for them, and re-layouts: 2.28 us -> 8.55 us
    all_to_all x2 -> x0, blocking collectives: 43.6 us -> none  [gather_columns(): lax.all_to_all(copies, 'ep', 0, 0, tiled=True, axis_index_groups=groups)]
    all_to_all x0 -> x2, waiting for transfers between devices: none -> 27.9 us  [gather_columns(): lax.all_to_all(copies, 'ep', 0, 0, tiled=True, axis_index_groups=groups)]
    all_to_all x0 -> x2, starting transfers between devices: none -> 12.8 us  [gather_columns(): lax.all_to_all(copies, 'ep', 0, 0, tiled=True, axis_index_groups=groups)]
    unnamed x30 -> x40, local copies, waits for them, and re-layouts: 2.03 us -> 8.31 us
    pallas_call x1, Pallas kernels: 11.1 us -> 6.63 us  [body(): attend(place, lengths, *queries, head_bias[:, None], in_hbm(cache_keys),...]
    all_to_all x1, blocking collectives: 26.8 us -> 29 us  [body(): lax.all_to_all(outgoing.reshape(EP, 16, CH), 'ep', 0, 0, tiled=True)]
    pallas_call x6 -> x5, Pallas kernels: 10.5 us -> 8.32 us  [the longest x1 4.17 us: body(): pl.pallas_call(expert_kernel, in_specs=[VMEM, VMEM, HBM, HBM], out_specs=...]
  transfers between devices with their start and end apart: 15 -> 17, of which waited for: 8 -> 11; matrix products, arithmetic and copies ran while one was open for 3% -> 3% of each run, Pallas kernels for 8% -> 6%
where the time goes in v2:
time: 156 us; the launch traced here: 155 us
  waiting for transfers between devices  55.2 us (35%)
  starting transfers between devices  38.3 us (25%)
  blocking collectives  29 us (19%)
  Pallas kernels  19 us (12%)
  local copies, waits for them, and re-layouts  8.55 us (5%)
  matrix products  4.32 us (3%)
    all_to_all x1, blocking collectives, body(): lax.all_to_all(outgoing.reshape(EP, 16, CH), 'ep', 0, 0, tiled=True)  29 us
    all_to_all x2, waiting for transfers between devices, gather_columns(): lax.all_to_all(copies, 'ep', 0, 0, tiled=True, axis_index_groups=groups)  27.9 us
    ppermute x14, starting transfers between devices, swap(): return lax.ppermute(x, 'ep', [(i, i ^ d) for i in range(EP)])  21 us
    all_to_all x1, waiting for transfers between devices, body(): lax.all_to_all(result.reshape(EP, 16, CH), 'ep', 0, 0, tiled=True)  14.9 us
    all_to_all x2, starting transfers between devices, gather_columns(): lax.all_to_all(copies, 'ep', 0, 0, tiled=True, axis_index_groups=groups)  12.8 us
    ppermute x14, waiting for transfers between devices, swap(): return lax.ppermute(x, 'ep', [(i, i ^ d) for i in range(EP)])  12.3 us
    unnamed x40, local copies, waits for them, and re-layouts  8.31 us
    pallas_call x1, Pallas kernels, body(): attend(place, lengths, *queries, head_bias[:, None], in_hbm(cache_keys),...  6.63 us
  transfers between devices with their start and end apart: 17, of which 11 were waited for; matrix products, arithmetic and copies ran while one was open for 3% of the time, Pallas kernels for 6%

profile of v2, /device:TPU:1, one launch (start us, length us, event | category | flops | bytes accessed | tf_op | source)
XLA Modules:
  0.0 155.3 jit_solution(5627958623943868651)
XLA Ops:
  0.6 0.0 copy-start
  0.7 1.0 copy-done.10
  1.6 0.1 copies.2
  1.7 1.0 copy-done.4
  2.7 8.6 %all-to-all-start = ((bf16[16,16,2048]{2,1,0:T(8,128)(2,1)}), bf16[16,16,2048]{2,1,0:T(8,128)(2,1)S(1)}, u32[]{:S(2)}, u32[]{:S(2)}) async-start(bf16[16,16,2048]{2,1,0:T(8,128)(2,1)} %copy-done.4), calls=%async_computation | async-start | bytes 2097152 | tf_op jit(solution)/shard_map/all_to_all | solution.py:272
  11.3 0.0 copy-start.9
  11.3 0.0 copy-start.12
  11.3 0.1 copies.3
  11.4 1.0 copy-done.3
  12.4 14.9 %all-to-all-done.own = bf16[16,16,2048]{2,1,0:T(8,128)(2,1)S(1)} async-done(((bf16[16,16,2048]{2,1,0:T(8,128)(2,1)}), bf16[16,16,2048]{2,1,0:T(8,128)(2,1)S(1)}, u32[]{:S(2)}, u32[]{:S(2)}) %all-to-all-start) | async-done | bytes 1048608 | tf_op jit(solution)/shard_map/all_to_all | solution.py:272
  27.3 1.0 copy-done.1
  28.3 4.2 %all-to-all-start.1 = ((bf16[16,16,2048]{2,1,0:T(8,128)(2,1)}), bf16[16,16,2048]{2,1,0:T(8,128)(2,1)S(1)}, u32[]{:S(2)}, u32[]{:S(2)}) async-start(bf16[16,16,2048]{2,1,0:T(8,128)(2,1)} %copy-done.3), calls=%async_computation.1 | async-start | bytes 2097152 | tf_op jit(solution)/shard_map/all_to_all | solution.py:272
  32.5 0.0 copy-start.19
  32.5 0.0 copy-start.16
  32.6 2.1 %collective-permute-start.3 = (bf16[16,16,2048]{2,1,0:T(8,128)(2,1)}, bf16[16,16,2048]{2,1,0:T(8,128)(2,1)}, u32[]{:S(2)}, u32[]{:S(2)}) collective-permute-start(bf16[16,16,2048]{2,1,0:T(8,128)(2,1)} %copy-done.1), channel_id=1, source_target_pairs={{0,1},{1,0},{2,3},{3,2},{4,5},{5,4},{6,7},{7,6},{8,9},{9,8},{10,11... | collective-permute-start | bytes 3145736 | tf_op jit(solution)/shard_map/ppermute | solution.py:245
  34.7 13.0 %all-to-all-done.1.own = bf16[16,16,2048]{2,1,0:T(8,128)(2,1)S(1)} async-done(((bf16[16,16,2048]{2,1,0:T(8,128)(2,1)}), bf16[16,16,2048]{2,1,0:T(8,128)(2,1)S(1)}, u32[]{:S(2)}, u32[]{:S(2)}) %all-to-all-start.1) | async-done | bytes 1048608 | tf_op jit(solution)/shard_map/all_to_all | solution.py:272
  47.7 3.2 %collective-permute-start.10 = (bf16[16,16,2048]{2,1,0:T(8,128)(2,1)S(1)}, bf16[16,16,2048]{2,1,0:T(8,128)(2,1)}, u32[]{:S(2)}, u32[]{:S(2)}) collective-permute-start(bf16[16,16,2048]{2,1,0:T(8,128)(2,1)S(1)} %all-to-all-done.1.own), channel_id=1, source_target_pairs={{0,1},{1,0},{2,3},{3,2},{4,5},{5,4},{6,7},{7,6},{8,9},{9,8},{10,11... | collective-permute-start | bytes 3145736 | tf_op jit(solution)/shard_map/ppermute | solution.py:245
  50.9 1.2 collective-permute-start
  52.1 2.5 %collective-permute-start.1 = (bf16[16,2048]{1,0:T(8,128)(2,1)S(1)}, bf16[16,2048]{1,0:T(8,128)(2,1)S(1)}, u32[]{:S(2)}, u32[]{:S(2)}) collective-permute-start(bf16[16,2048]{1,0:T(8,128)(2,1)S(1)} %copy-done.9), channel_id=1, source_target_pairs={{0,4},{1,5},{2,6},{3,7},{4,0},{5,1},{6,2},{7,3},{8,12},{9,13},{10,... | collective-permute-start | bytes 196616 | tf_op jit(solution)/shard_map/ppermute | solution.py:245
  54.5 0.2 collective-permute-start.2
  54.7 0.1 pad_add_fusion.place
  54.8 0.0 collective-permute-done.t1
  54.8 3.3 %collective-permute-done.1.t2 = bf16[16,2048]{1,0:T(8,128)(2,1)S(1)} collective-permute-done((bf16[16,2048]{1,0:T(8,128)(2,1)S(1)}, bf16[16,2048]{1,0:T(8,128)(2,1)S(1)}, u32[]{:S(2)}, u32[]{:S(2)}) %collective-permute-start.1) | collective-permute-done | bytes 65568 | tf_op jit(solution)/shard_map/ppermute | solution.py:245
  58.1 0.9 collective-permute-done.2.t3
  59.0 1.0 copy-done.7
  60.1 1.0 copy-done.8
  61.1 0.9 shard_map.220
  62.0 0.0 collective-permute-done.3.other
  62.0 1.2 copy-done.2
  63.3 2.0 %shard_map.221 = (bf16[16,512]{1,0:T(8,128)(2,1)S(1)}, bf16[16,512]{1,0:T(8,128)(2,1)S(1)}, bf16[16,512]{1,0:T(8,128)(2,1)S(1)}, bf16[16,512]{1,0:T(8,128)(2,1)S(1)}) custom-call(s32[2]{0:T(128)S(1)} %pad_add_fusion.place, bf16[64,2048]{1,0:T(8,128)(2,1)S(1)} %get-tuple-element.17.rows, bf16[16,16,2048]{2,1,0:T(8,128)(2,1)S(1)} %copy-done.2, ...), custom_call_target="tpu_custom_call" | custom-call | tf_op jit(solution)/shard_map/pallas_call | solution.py:291
  65.3 0.5 collective-permute-start.4
  65.8 2.5 %collective-permute-start.5 = (bf16[16,512]{1,0:T(8,128)(2,1)S(1)}, bf16[16,512]{1,0:T(8,128)(2,1)S(1)}, u32[]{:S(2)}, u32[]{:S(2)}) collective-permute-start(bf16[16,512]{1,0:T(8,128)(2,1)S(1)} %get-tuple-element.20), channel_id=1, source_target_pairs={{0,4},{1,5},{2,6},{3,7},{4,0},{5,1},{6,2},{7,3},{8,12},{9,13},{10,... | collective-permute-start | bytes 49160 | tf_op jit(solution)/shard_map/ppermute | solution.py:245
  68.3 0.9 collective-permute-start.6
  69.2 0.1 copy.24.bias
  69.3 0.0 collective-permute-done.4.q1
  69.3 0.6 collective-permute-done.5.q2
  69.9 2.2 %collective-permute-done.6.q3 = bf16[16,512]{1,0:T(8,128)(2,1)S(1)} collective-permute-done((bf16[16,512]{1,0:T(8,128)(2,1)S(1)}, bf16[16,512]{1,0:T(8,128)(2,1)S(1)}, u32[]{:S(2)}, u32[]{:S(2)}) %collective-permute-start.6) | collective-permute-done | bytes 16416 | tf_op jit(solution)/shard_map/ppermute | solution.py:245
  72.1 6.6 %attend.1.a0 = bf16[16,2048]{1,0:T(8,128)(2,1)S(1)} custom-call(s32[2]{0:T(128)S(1)} %pad_add_fusion.place, s32[16]{0:T(128)S(1)} %copy-done.16, bf16[16,512]{1,0:T(8,128)(2,1)S(1)} %get-tuple-element.18.q0, bf16[16,512]{1,0:T(8,128)(2,1)S(1)} %collective-permute-done.4.q1, bf16[16,512]{1,0:T(8,128)(2,1)S(1)} %collective-permute-done.5.q2, ...), custom_call_target="tpu_custom_call" | custom-call | tf_op jit(solution)/shard_map/attend/pallas_call | solution.py:312
  78.7 0.0 copy-start.17
  78.8 0.0 copy-start.14
  78.8 0.0 copy-start.15
  78.8 0.1 collective-permute-start.7
  78.9 2.1 %collective-permute-start.8 = (bf16[16,2048]{1,0:T(8,128)(2,1)S(1)}, bf16[16,2048]{1,0:T(8,128)(2,1)S(1)}, u32[]{:S(2)}, u32[]{:S(2)}) collective-permute-start(bf16[16,2048]{1,0:T(8,128)(2,1)S(1)} %attend.1.a0), channel_id=1, source_target_pairs={{0,4},{1,5},{2,6},{3,7},{4,0},{5,1},{6,2},{7,3},{8,12},{9,13},{10,... | collective-permute-start | bytes 196616 | tf_op jit(solution)/shard_map/ppermute | solution.py:245
  81.0 1.8 %collective-permute-start.9 = (bf16[16,2048]{1,0:T(8,128)(2,1)S(1)}, bf16[16,2048]{1,0:T(8,128)(2,1)S(1)}, u32[]{:S(2)}, u32[]{:S(2)}) collective-permute-start(bf16[16,2048]{1,0:T(8,128)(2,1)S(1)} %attend.1.a0), channel_id=1, source_target_pairs={{0,6},{1,7},{2,4},{3,5},{4,2},{5,3},{6,0},{7,1},{8,14},{9,15},{10,... | collective-permute-start | bytes 196616 | tf_op jit(solution)/shard_map/ppermute | solution.py:245
  82.7 0.0 collective-permute-done.10.other
  82.7 0.8 collective-permute-done.8.a2
  83.6 1.7 %collective-permute-done.9.a3 = bf16[16,2048]{1,0:T(8,128)(2,1)S(1)} collective-permute-done((bf16[16,2048]{1,0:T(8,128)(2,1)S(1)}, bf16[16,2048]{1,0:T(8,128)(2,1)S(1)}, u32[]{:S(2)}, u32[]{:S(2)}) %collective-permute-start.9) | collective-permute-done | bytes 65568 | tf_op jit(solution)/shard_map/ppermute | solution.py:245
  85.3 2.0 %shard_map.222 = (bf16[16,512]{1,0:T(8,128)(2,1)S(1)}, bf16[16,512]{1,0:T(8,128)(2,1)S(1)}, bf16[16,512]{1,0:T(8,128)(2,1)S(1)}, bf16[16,512]{1,0:T(8,128)(2,1)S(1)}) custom-call(s32[2]{0:T(128)S(1)} %pad_add_fusion.place, bf16[16,2048]{1,0:T(8,128)(2,1)S(1)} %attend.1.a0, bf16[16,2048]{1,0:T(8,128)(2,1)S(1)} %collective-permute-done.7.a1, ...), custom_call_target="tpu_custom_call" | custom-call | tf_op jit(solution)/shard_map/pallas_call | solution.py:317
  87.3 0.1 collective-permute-start.11
  87.4 2.9 %collective-permute-start.12 = (bf16[16,512]{1,0:T(8,128)(2,1)S(1)}, bf16[16,512]{1,0:T(8,128)(2,1)S(1)}, u32[]{:S(2)}, u32[]{:S(2)}) collective-permute-start(bf16[16,512]{1,0:T(8,128)(2,1)S(1)} %get-tuple-element.24), channel_id=1, source_target_pairs={{0,4},{1,5},{2,6},{3,7},{4,0},{5,1},{6,2},{7,3},{8,12},{9,13},{10,... | collective-permute-start | bytes 49160 | tf_op jit(solution)/shard_map/ppermute | solution.py:245
  90.3 0.9 collective-permute-start.13
  91.2 0.1 tile.9.routes
  91.3 0.3 collective-permute-done.12.m2
  91.6 2.5 %collective-permute-done.13.m3 = bf16[16,512]{1,0:T(8,128)(2,1)S(1)} collective-permute-done((bf16[16,512]{1,0:T(8,128)(2,1)S(1)}, bf16[16,512]{1,0:T(8,128)(2,1)S(1)}, u32[]{:S(2)}, u32[]{:S(2)}) %collective-permute-start.13) | collective-permute-done | bytes 16416 | tf_op jit(solution)/shard_map/ppermute | solution.py:245
  94.1 1.6 %shard_map.223 = (f32[16,2048]{1,0:T(8,128)S(1)}, bf16[16,2048]{1,0:T(8,128)(2,1)S(1)}, bf16[2048,256]{1,0:T(8,128)(2,1)S(1)}) custom-call(s32[2]{0:T(128)S(1)} %pad_add_fusion.place, bf16[16,512]{1,0:T(8,128)(2,1)S(1)} %get-tuple-element.22.m0, bf16[16,512]{1,0:T(8,128)(2,1)S(1)} %collective-permute-done.11.m1, ...), custom_call_target="tpu_custom_call" | custom-call | tf_op jit(solution)/shard_map/pallas_call | solution.py:319
  95.7 29.0 %all_to_all.20 = bf16[128,16,256]{2,1,0:T(8,128)(2,1)S(1)} all-to-all(bf16[128,16,256]{2,1,0:T(8,128)(2,1)S(1)} %bitcast.23), channel_id=1, replica_groups=mesh['ep'=128] {'ep'}, dimensions={0} | all-to-all | bytes 2097152 | tf_op jit(solution)/shard_map/all_to_all | solution.py:325
  124.8 4.2 %expert.1 = bf16[2048,256]{1,0:T(8,128)(2,1)S(1)} custom-call(bf16[2048,256]{1,0:T(8,128)(2,1)S(1)} %bitcast.22, bf16[1,2048,512]{2,1,0:T(8,128)(2,1)S(1)} %copy-done.6, bf16[1,2048,512]{2,1,0:T(8,128)(2,1)} %up.1, bf16[1,512,2048]{2,1,0:T(8,128)(2,1)} %down.1), custom_call_target="tpu_custom_call" | custom-call | tf_op jit(solution)/shard_map/expert/pallas_call | solution.py:330
  129.0 1.0 copy-done.5
  129.9 4.5 %all-to-all-start.3 = ((bf16[128,16,256]{2,1,0:T(8,128)(2,1)}), bf16[128,16,256]{2,1,0:T(8,128)(2,1)S(1)}, u32[]{:S(2)}, u32[]{:S(2)}) async-start(bf16[128,16,256]{2,1,0:T(8,128)(2,1)} %bitcast.21), calls=%async_computation.3 | async-start | bytes 2097152 | tf_op jit(solution)/shard_map/all_to_all | solution.py:345
  134.5 0.1 tile.21.weights
  134.6 2.0 %fusion.5 = f32[16,512]{1,0:T(8,128)S(1)} fusion(bf16[16,2048]{1,0:T(8,128)(2,1)S(1)} %get-tuple-element.28, bf16[2048,512]{1,0:T(8,128)(2,1)} %param.39), kind=kOutput, calls=%fused_computation.6 | convolution fusion | flops 33554432 | bytes 2195456 | tf_op jit(solution)/shard_map/dot_general | solution.py:44
  136.5 2.4 %fusion.shared = f32[16,2048]{1,0:T(8,128)S(1)} fusion(bf16[512,2048]{1,0:T(8,128)(2,1)S(1)} %copy-done, f32[16,512]{1,0:T(8,128)S(1)} %fusion.5, bf16[16,2048]{1,0:T(8,128)(2,1)S(1)} %get-tuple-element.28, bf16[2048,512]{1,0:T(8,128)(2,1)} %param.40), kind=kOutput, calls=%fused_computation.1 | convolution fusion | flops 67158016 | bytes 4423680 | tf_op jit(solution)/shard_map/dot_general | solution.py:44
  138.9 14.9 %all-to-all-done.3 = bf16[128,16,256]{2,1,0:T(8,128)(2,1)S(1)} async-done(((bf16[128,16,256]{2,1,0:T(8,128)(2,1)}), bf16[128,16,256]{2,1,0:T(8,128)(2,1)S(1)}, u32[]{:S(2)}, u32[]{:S(2)}) %all-to-all-start.3) | async-done | bytes 1048608 | tf_op jit(solution)/shard_map/all_to_all | solution.py:345
  153.8 1.5 shard_map.224
  (28 shorter events, 0.1 us)
Async XLA Ops:
  0.6 135.9 %copy-start = (bf16[512,2048]{1,0:T(8,128)(2,1)S(1)}, bf16[512,2048]{1,0:T(8,128)(2,1)}, u32[]{:S(2)}) copy-start(bf16[512,2048]{1,0:T(8,128)(2,1)} %param.41) | copy-start | bytes 6291460
  0.6 1.0 copy-start.10
  1.6 9.7 %copy-start.11 = (bf16[2048,16]{0,1:T(8,128)(2,1)S(1)}, bf16[2048,16]{0,1:T(8,128)(2,1)}, u32[]{:S(2)}) copy-start(bf16[2048,16]{0,1:T(8,128)(2,1)} %param.33) | copy-start | bytes 196612
  1.7 1.0 copy-start.4
  2.7 24.6 %all-to-all-start = ((bf16[16,16,2048]{2,1,0:T(8,128)(2,1)}), bf16[16,16,2048]{2,1,0:T(8,128)(2,1)S(1)}, u32[]{:S(2)}, u32[]{:S(2)}) async-start(bf16[16,16,2048]{2,1,0:T(8,128)(2,1)} %copy-done.4), calls=%async_computation | async-start | bytes 2097152 | tf_op jit(solution)/shard_map/all_to_all | solution.py:272
  11.3 39.6 %copy-start.9 = (bf16[16,2048]{1,0:T(8,128)(2,1)S(1)}, bf16[16,2048]{1,0:T(8,128)(2,1)}, u32[]{:S(2)}) copy-start(bf16[16,2048]{1,0:T(8,128)(2,1)} %tokens.1) | copy-start | bytes 196612
  11.3 47.7 %copy-start.12 = (f32[2048]{0:T(1024)S(1)}, f32[2048]{0:T(1024)}, u32[]{:S(2)}) copy-start(f32[2048]{0:T(1024)} %param.25) | copy-start | bytes 24580
  11.4 1.0 copy-start.3
  27.3 1.0 copy-start.1
  28.3 19.4 %all-to-all-start.1 = ((bf16[16,16,2048]{2,1,0:T(8,128)(2,1)}), bf16[16,16,2048]{2,1,0:T(8,128)(2,1)S(1)}, u32[]{:S(2)}, u32[]{:S(2)}) async-start(bf16[16,16,2048]{2,1,0:T(8,128)(2,1)} %copy-done.3), calls=%async_computation.1 | async-start | bytes 2097152 | tf_op jit(solution)/shard_map/all_to_all | solution.py:272
  32.5 36.7 %copy-start.19 = (f32[32]{0:T(128)S(1)}, f32[32]{0:T(128)}, u32[]{:S(2)}) copy-start(f32[32]{0:T(128)} %param.32) | copy-start | bytes 388
  32.5 39.6 %copy-start.16 = (s32[16]{0:T(128)S(1)}, s32[16]{0:T(128)}, u32[]{:S(2)}) copy-start(s32[16]{0:T(128)} %lens.1) | copy-start | bytes 196
  32.6 29.5 %collective-permute-start.3 = (bf16[16,16,2048]{2,1,0:T(8,128)(2,1)}, bf16[16,16,2048]{2,1,0:T(8,128)(2,1)}, u32[]{:S(2)}, u32[]{:S(2)}) collective-permute-start(bf16[16,16,2048]{2,1,0:T(8,128)(2,1)} %copy-done.1), channel_id=1, source_target_pairs={{0,1},{1,0},{2,3},{3,2},{4,5},{5,4},{6,7},{7,6},{8,9},{9,8},{10,11... | collective-permute-start | bytes 3145736 | tf_op jit(solution)/shard_map/ppermute | solution.py:245
  47.7 35.0 %collective-permute-start.10 = (bf16[16,16,2048]{2,1,0:T(8,128)(2,1)S(1)}, bf16[16,16,2048]{2,1,0:T(8,128)(2,1)}, u32[]{:S(2)}, u32[]{:S(2)}) collective-permute-start(bf16[16,16,2048]{2,1,0:T(8,128)(2,1)S(1)} %all-to-all-done.1.own), channel_id=1, source_target_pairs={{0,1},{1,0},{2,3},{3,2},{4,5},{5,4},{6,7},{7,6},{8,9},{9,8},{10,11... | collective-permute-start | bytes 3145736 | tf_op jit(solution)/shard_map/ppermute | solution.py:245
  50.9 3.9 %collective-permute-start = (bf16[16,2048]{1,0:T(8,128)(2,1)S(1)}, bf16[16,2048]{1,0:T(8,128)(2,1)S(1)}, u32[]{:S(2)}, u32[]{:S(2)}) collective-permute-start(bf16[16,2048]{1,0:T(8,128)(2,1)S(1)} %copy-done.9), channel_id=1, source_target_pairs={{0,2},{1,3},{2,0},{3,1},{4,6},{5,7},{6,4},{7,5},{8,10},{9,11},{10,... | collective-permute-start | bytes 196616 | tf_op jit(solution)/shard_map/ppermute | solution.py:245
  52.1 6.0 %collective-permute-start.1 = (bf16[16,2048]{1,0:T(8,128)(2,1)S(1)}, bf16[16,2048]{1,0:T(8,128)(2,1)S(1)}, u32[]{:S(2)}, u32[]{:S(2)}) collective-permute-start(bf16[16,2048]{1,0:T(8,128)(2,1)S(1)} %copy-done.9), channel_id=1, source_target_pairs={{0,4},{1,5},{2,6},{3,7},{4,0},{5,1},{6,2},{7,3},{8,12},{9,13},{10,... | collective-permute-start | bytes 196616 | tf_op jit(solution)/shard_map/ppermute | solution.py:245
  54.5 4.5 %collective-permute-start.2 = (bf16[16,2048]{1,0:T(8,128)(2,1)S(1)}, bf16[16,2048]{1,0:T(8,128)(2,1)S(1)}, u32[]{:S(2)}, u32[]{:S(2)}) collective-permute-start(bf16[16,2048]{1,0:T(8,128)(2,1)S(1)} %copy-done.9), channel_id=1, source_target_pairs={{0,6},{1,7},{2,4},{3,5},{4,2},{5,3},{6,0},{7,1},{8,14},{9,15},{10,... | collective-permute-start | bytes 196616 | tf_op jit(solution)/shard_map/ppermute | solution.py:245
  59.0 1.0 copy-start.7
  60.1 1.0 copy-start.8
  62.0 1.2 copy-start.2
  65.3 4.0 %collective-permute-start.4 = (bf16[16,512]{1,0:T(8,128)(2,1)S(1)}, bf16[16,512]{1,0:T(8,128)(2,1)S(1)}, u32[]{:S(2)}, u32[]{:S(2)}) collective-permute-start(bf16[16,512]{1,0:T(8,128)(2,1)S(1)} %get-tuple-element.19), channel_id=1, source_target_pairs={{0,2},{1,3},{2,0},{3,1},{4,6},{5,7},{6,4},{7,5},{8,10},{9,11},{10,... | collective-permute-start | bytes 49160 | tf_op jit(solution)/shard_map/ppermute | solution.py:245
  65.8 4.1 %collective-permute-start.5 = (bf16[16,512]{1,0:T(8,128)(2,1)S(1)}, bf16[16,512]{1,0:T(8,128)(2,1)S(1)}, u32[]{:S(2)}, u32[]{:S(2)}) collective-permute-start(bf16[16,512]{1,0:T(8,128)(2,1)S(1)} %get-tuple-element.20), channel_id=1, source_target_pairs={{0,4},{1,5},{2,6},{3,7},{4,0},{5,1},{6,2},{7,3},{8,12},{9,13},{10,... | collective-permute-start | bytes 49160 | tf_op jit(solution)/shard_map/ppermute | solution.py:245
  68.3 3.8 %collective-permute-start.6 = (bf16[16,512]{1,0:T(8,128)(2,1)S(1)}, bf16[16,512]{1,0:T(8,128)(2,1)S(1)}, u32[]{:S(2)}, u32[]{:S(2)}) collective-permute-start(bf16[16,512]{1,0:T(8,128)(2,1)S(1)} %get-tuple-element.21), channel_id=1, source_target_pairs={{0,6},{1,7},{2,4},{3,5},{4,2},{5,3},{6,0},{7,1},{8,14},{9,15},{10,... | collective-permute-start | bytes 49160 | tf_op jit(solution)/shard_map/ppermute | solution.py:245
  78.7 12.5 %copy-start.17 = (s32[16,6]{0,1:T(8,128)S(1)}, s32[16,6]{0,1:T(8,128)}, u32[]{:S(2)}) copy-start(s32[16,6]{0,1:T(8,128)} %param.34) | copy-start | bytes 1156
  78.8 15.4 %copy-start.14 = (f32[2048]{0:T(1024)S(1)}, f32[2048]{0:T(1024)}, u32[]{:S(2)}) copy-start(f32[2048]{0:T(1024)} %param.26) | copy-start | bytes 24580
  78.8 15.4 %copy-start.15 = (f32[2048]{0:T(1024)S(1)}, f32[2048]{0:T(1024)}, u32[]{:S(2)}) copy-start(f32[2048]{0:T(1024)} %param.27) | copy-start | bytes 24580
  78.8 3.9 %collective-permute-start.7 = (bf16[16,2048]{1,0:T(8,128)(2,1)S(1)}, bf16[16,2048]{1,0:T(8,128)(2,1)S(1)}, u32[]{:S(2)}, u32[]{:S(2)}) collective-permute-start(bf16[16,2048]{1,0:T(8,128)(2,1)S(1)} %attend.1.a0), channel_id=1, source_target_pairs={{0,2},{1,3},{2,0},{3,1},{4,6},{5,7},{6,4},{7,5},{8,10},{9,11},{10,... | collective-permute-start | bytes 196616 | tf_op jit(solution)/shard_map/ppermute | solution.py:245
  78.9 4.7 %collective-permute-start.8 = (bf16[16,2048]{1,0:T(8,128)(2,1)S(1)}, bf16[16,2048]{1,0:T(8,128)(2,1)S(1)}, u32[]{:S(2)}, u32[]{:S(2)}) collective-permute-start(bf16[16,2048]{1,0:T(8,128)(2,1)S(1)} %attend.1.a0), channel_id=1, source_target_pairs={{0,4},{1,5},{2,6},{3,7},{4,0},{5,1},{6,2},{7,3},{8,12},{9,13},{10,... | collective-permute-start | bytes 196616 | tf_op jit(solution)/shard_map/ppermute | solution.py:245
  81.0 4.3 %collective-permute-start.9 = (bf16[16,2048]{1,0:T(8,128)(2,1)S(1)}, bf16[16,2048]{1,0:T(8,128)(2,1)S(1)}, u32[]{:S(2)}, u32[]{:S(2)}) collective-permute-start(bf16[16,2048]{1,0:T(8,128)(2,1)S(1)} %attend.1.a0), channel_id=1, source_target_pairs={{0,6},{1,7},{2,4},{3,5},{4,2},{5,3},{6,0},{7,1},{8,14},{9,15},{10,... | collective-permute-start | bytes 196616 | tf_op jit(solution)/shard_map/ppermute | solution.py:245
  87.3 4.0 %collective-permute-start.11 = (bf16[16,512]{1,0:T(8,128)(2,1)S(1)}, bf16[16,512]{1,0:T(8,128)(2,1)S(1)}, u32[]{:S(2)}, u32[]{:S(2)}) collective-permute-start(bf16[16,512]{1,0:T(8,128)(2,1)S(1)} %get-tuple-element.23), channel_id=1, source_target_pairs={{0,2},{1,3},{2,0},{3,1},{4,6},{5,7},{6,4},{7,5},{8,10},{9,11},{10,... | collective-permute-start | bytes 49160 | tf_op jit(solution)/shard_map/ppermute | solution.py:245
  87.4 4.2 %collective-permute-start.12 = (bf16[16,512]{1,0:T(8,128)(2,1)S(1)}, bf16[16,512]{1,0:T(8,128)(2,1)S(1)}, u32[]{:S(2)}, u32[]{:S(2)}) collective-permute-start(bf16[16,512]{1,0:T(8,128)(2,1)S(1)} %get-tuple-element.24), channel_id=1, source_target_pairs={{0,4},{1,5},{2,6},{3,7},{4,0},{5,1},{6,2},{7,3},{8,12},{9,13},{10,... | collective-permute-start | bytes 49160 | tf_op jit(solution)/shard_map/ppermute | solution.py:245
  90.3 3.8 %collective-permute-start.13 = (bf16[16,512]{1,0:T(8,128)(2,1)S(1)}, bf16[16,512]{1,0:T(8,128)(2,1)S(1)}, u32[]{:S(2)}, u32[]{:S(2)}) collective-permute-start(bf16[16,512]{1,0:T(8,128)(2,1)S(1)} %get-tuple-element.25), channel_id=1, source_target_pairs={{0,6},{1,7},{2,4},{3,5},{4,2},{5,3},{6,0},{7,1},{8,14},{9,15},{10,... | collective-permute-start | bytes 49160 | tf_op jit(solution)/shard_map/ppermute | solution.py:245
  91.3 33.4 %copy-start.6 = (bf16[1,2048,512]{2,1,0:T(8,128)(2,1)S(1)}, bf16[1,2048,512]{2,1,0:T(8,128)(2,1)}, u32[]{:S(2)}) copy-start(bf16[1,2048,512]{2,1,0:T(8,128)(2,1)} %gate.1) | copy-start | bytes 6291460
  128.9 1.0 copy-start.5
  129.9 4.5 %copy-start.18 = (f32[16,6]{0,1:T(8,128)S(1)}, f32[16,6]{0,1:T(8,128)}, u32[]{:S(2)}) copy-start(f32[16,6]{0,1:T(8,128)} %param.35) | copy-start | bytes 1156
  129.9 23.9 %all-to-all-start.3 = ((bf16[128,16,256]{2,1,0:T(8,128)(2,1)}), bf16[128,16,256]{2,1,0:T(8,128)(2,1)S(1)}, u32[]{:S(2)}, u32[]{:S(2)}) async-start(bf16[128,16,256]{2,1,0:T(8,128)(2,1)} %bitcast.21), calls=%async_computation.3 | async-start | bytes 2097152 | tf_op jit(solution)/shard_map/all_to_all | solution.py:345
  136.5 17.3 %copy-start.13 = (f32[2048]{0:T(1024)S(1)}, f32[2048]{0:T(1024)}, u32[]{:S(2)}) copy-start(f32[2048]{0:T(1024)} %param.28) | copy-start | bytes 24580

commit v3 on v2

--- a/solution.py
+++ b/solution.py
@@ -60,82 +60,126 @@
                 o[...] = out[i * SEQ : (i + 1) * SEQ]
 
 
-def norm_kernel(t0, t1, t2, t3, gain, wk, wv, rows, nk, nv):
+def fetch(sources, targets, sems):
+    copies = [pltpu.make_async_copy(s, t, sems.at[i]) for i, (s, t) in enumerate(zip(sources, targets))]
+    for c in copies:
+        c.start()
+    return copies
+
+
+def norm_kernel(t0, t1, t2, t3, others, gain, rows):
     for i, t in enumerate((t0, t1, t2, t3)):
         rows[i * SEQ : (i + 1) * SEQ] = rms(t[...].astype(F32), gain[...]).astype(BF16)
-    mine = rows[:SEQ]
-    nk[...] = dot(mine, wk[...]).astype(BF16)
-    nv[...] = dot(mine, wv[...]).astype(BF16)
-
-
-def query_kernel(place, rows, own, other, *outs):
-    project(place, rows[...], own, other, outs)
+    rows[GRP * SEQ :] = rms(others[...].astype(F32), gain[...]).astype(BF16)
+
+
+def query_kernel(rows, own, mine, others):
+    weight = jnp.concatenate([own[p] for p in range(PLANE)], axis=0)
+    out = dot_nt(rows[...], weight).astype(BF16)
+    mine[...] = out[: GRP * SEQ]
+    others[...] = out[GRP * SEQ :]
+
+
+def join_kernel(mine, got, *outs):
+    for i, o in enumerate(outs):
+        o[...] = jnp.concatenate([mine[i * SEQ : (i + 1) * SEQ], got[i * SEQ : (i + 1) * SEQ]], axis=1)
 
 
 SUB = 8
 BLK = 256
 
 
-def attend_kernel(place, lens, q0, q1, q2, q3, bias, keys, values, out, qf, placed, upper, att):
-    step = pl.program_id(0)
-
-    @pl.when(step == 0)
-    def _():
-        upper[...] = (iota((BLK, BLK), 0) > iota((BLK, BLK), 1)).astype(F32).astype(BF16)
-        for i, q in enumerate((q0, q1, q2, q3)):
-            qf[i] = q[...].astype(F32) * HD ** (-0.5)
-        row, col = iota((COLS, 2 * HD), 0), iota((COLS, 2 * HD), 1)
-        plane = iota((H, COLS), 1) >> 5
-        spread = [[] for _ in range(SEQ)]
-        select = []
-        for m in range(GRP):
-            target = (row >> 8) * HD + (m & 1) * 32 + (row & 31)
-            select.append((col == target).astype(F32).astype(BF16))
-            mask = plane * 2 + (m >> 1) == iota((H, COLS), 0)
-            part = qf[place[0] ^ m]
-            for u in range(SEQ):
-                rows = jnp.broadcast_to(part[u : u + 1], (H, COLS))
-                spread[u].append(jnp.where(mask, rows, 0.0).astype(BF16))
-        spread = jnp.concatenate([jnp.concatenate(p, axis=1) for p in spread], axis=0)
-        placed[...] = dot(spread, jnp.concatenate(select, axis=0)).astype(BF16)
+def attend_kernel(place, lens, q0, q1, q2, q3, bias, keys, values, out, qf, placed, upper, att, kbuf, vbuf, sems):
+    copies = []
+    for g in range(SEQ // SUB):
+        part = pl.ds(g * SUB, SUB)
+        copies.append(
+            [
+                pltpu.make_async_copy(keys.at[part], kbuf.at[part], sems.at[0, g]),
+                pltpu.make_async_copy(values.at[part], vbuf.at[part], sems.at[1, g]),
+            ]
+        )
+        for c in copies[g]:
+            c.start()
+
+    upper[...] = (iota((BLK, BLK), 0) > iota((BLK, BLK), 1)).astype(F32).astype(BF16)
+    for i, q in enumerate((q0, q1, q2, q3)):
+        qf[i] = q[...].astype(F32) * HD ** (-0.5)
+    row, col = iota((COLS, 2 * HD), 0), iota((COLS, 2 * HD), 1)
+    plane, shard = (row >> 4) & (PLANE - 1), ((row >> 8) ^ place[1]) * SHARD + (row & 15)
+    head = ((iota((H, COLS), 1) >> 4) & (PLANE - 1)) * 2
+    spread = [[] for _ in range(SEQ)]
+    select = []
+    for m in range(GRP):
+        target = (plane >> 3) * HD + (m & 1) * 32 + shard
+        select.append((col == target).astype(F32).astype(BF16))
+        mask = head + (m >> 1) == iota((H, COLS), 0)
+        part = qf[place[0] ^ m]
+        for u in range(SEQ):
+            rows = jnp.broadcast_to(part[u : u + 1], (H, COLS))
+            spread[u].append(jnp.where(mask, rows, 0.0).astype(BF16))
+    spread = jnp.concatenate([jnp.concatenate(p, axis=1) for p in spread], axis=0)
+    placed[...] = dot(spread, jnp.concatenate(select, axis=0)).astype(BF16)
 
     count = LEN // BLK
-    first = pl.multiple_of(step * SUB * H, SUB * H)
-    valid, beta, keep, stacked = [], [], [], []
-    for u in range(SUB):
-        z = dot_nt(placed[pl.ds(first + u * H, H), :], keys[u]) + bias[...]
-        valid.append(iota((H, LEN), 1) < lens[step * SUB + u])
-        soft = jnp.log(1.0 + jnp.exp(-jnp.abs(z)))
-        beta.append(jnp.minimum(z, 0.0) - soft)
-        keep.append(jnp.where(valid[u], beta[u] - z, 0.0))
-        high = keep[u].astype(BF16)
-        low = (keep[u] - high.astype(F32)).astype(BF16)
-        for b in range(count):
-            stacked += [high[:, b * BLK : (b + 1) * BLK], low[:, b * BLK : (b + 1) * BLK]]
-    later = dot(jnp.concatenate(stacked, axis=0), upper[...])
-    for u in range(SUB):
-        carry = jnp.zeros((H, 1), F32)
-        blocks = []
-        for b in range(count - 1, -1, -1):
-            at = (u * count + b) * 2 * H
-            after = later[at : at + H] + later[at + H : at + 2 * H]
-            blocks.append(after + carry)
-            carry = carry + after[:, :1] + keep[u][:, b * BLK : b * BLK + 1]
-        after = jnp.concatenate(blocks[::-1], axis=1)
-        weights = jnp.where(valid[u], jnp.exp(beta[u] + after), 0.0).astype(BF16)
-        att[pl.ds(first + u * H, H), :] = dot(weights, values[u])
-
-    @pl.when(step == SEQ // SUB - 1)
-    def _():
-        left = iota((SEQ, 2 * HD), 1) < HD
-        for i in range(H // 2):
-            even = att[pl.ds(2 * i, SEQ, stride=H), :]
-            odd = att[pl.ds(2 * i + 1, SEQ, stride=H), :]
-            if 2 * i < H // 2:
-                odd = pltpu.roll(odd, HD, 1)
-            else:
-                even = pltpu.roll(even, HD, 1)
-            out[:, i * 2 * HD : (i + 1) * 2 * HD] = jnp.where(left, even, odd).astype(BF16)
+    for g in range(SEQ // SUB):
+        copies[g][0].wait()
+        valid, beta, keep, stacked = [], [], [], []
+        for u in range(SUB):
+            s = g * SUB + u
+            z = dot_nt(placed[s * H : (s + 1) * H], kbuf[s]) + bias[...]
+            valid.append(iota((H, LEN), 1) < lens[s])
+            soft = jnp.log(1.0 + jnp.exp(-jnp.abs(z)))
+            beta.append(jnp.minimum(z, 0.0) - soft)
+            keep.append(jnp.where(valid[u], beta[u] - z, 0.0))
+            high = keep[u].astype(BF16)
+            low = (keep[u] - high.astype(F32)).astype(BF16)
+            for b in range(count):
+                stacked += [high[:, b * BLK : (b + 1) * BLK], low[:, b * BLK : (b + 1) * BLK]]
+        later = dot(jnp.concatenate(stacked, axis=0), upper[...])
+        copies[g][1].wait()
+        for u in range(SUB):
+            s = g * SUB + u
+            carry = jnp.zeros((H, 1), F32)
+            blocks = []
+            for b in range(count - 1, -1, -1):
+                at = (u * count + b) * 2 * H
+                after = later[at : at + H] + later[at + H : at + 2 * H]
+                blocks.append(after + carry)
+                carry = carry + after[:, :1] + keep[u][:, b * BLK : b * BLK + 1]
+            after = jnp.concatenate(blocks[::-1], axis=1)
+            weights = jnp.where(valid[u], jnp.exp(beta[u] + after), 0.0).astype(BF16)
+            att[s * H : (s + 1) * H, :] = dot(weights, vbuf[s])
+
+    left = iota((SEQ, 2 * HD), 1) < HD
+    for i in range(H // 2):
+        even = att[pl.ds(2 * i, SEQ, stride=H), :]
+        odd = att[pl.ds(2 * i + 1, SEQ, stride=H), :]
+        if 2 * i < H // 2:
+            odd = pltpu.roll(odd, HD, 1)
+        else:
+            even = pltpu.roll(even, HD, 1)
+        out[:, i * 2 * HD : (i + 1) * 2 * HD] = jnp.where(left, even, odd).astype(BF16)
+
+
+def attend(place, lengths, queries, bias, keys, values):
+    return pl.pallas_call(
+        attend_kernel,
+        in_specs=[SMEM, SMEM] + [VMEM] * (GRP + 1) + [HBM, HBM],
+        out_specs=VMEM,
+        out_shape=jax.ShapeDtypeStruct((SEQ, D), BF16),
+        scratch_shapes=[
+            pltpu.VMEM((GRP, SEQ, COLS), F32),
+            pltpu.VMEM((SEQ * H, 2 * HD), BF16),
+            pltpu.VMEM((BLK, BLK), BF16),
+            pltpu.VMEM((SEQ * H, 2 * HD), F32),
+            pltpu.VMEM((SEQ, LEN, 2 * HD), BF16),
+            pltpu.VMEM((SEQ, LEN, 2 * HD), BF16),
+            pltpu.SemaphoreType.DMA((2, SEQ // SUB)),
+        ],
+        compiler_params=PARAMS,
+        name="attend",
+    )(place, lengths, *queries, bias, in_hbm(keys), in_hbm(values))
 
 
 def output_kernel(place, a0, a1, a2, a3, own, other, *outs):
@@ -188,7 +232,7 @@
     outgoing[...] = dot(send, blocks).astype(BF16)
 
 
-def expert_kernel(incoming, gate, up, down, outgoing, rows, result, wu, wd, sems):
+def expert_kernel(incoming, gate, up, down, outgoing, rows, result, wu, wd, back_rows, sems):
     copies = [
         pltpu.make_async_copy(w.at[0], v, sems.at[i])
         for i, (w, v) in enumerate(((up, wu), (down, wd)))
@@ -213,7 +257,29 @@
         block = jnp.concatenate(
             [result[g * 32 : (g + 1) * 32, j * CH : (j + 1) * CH] for j in range(NJ)], axis=0
         )
-        outgoing[g * n : (g + 1) * n, :] = dot(back, block).astype(BF16)
+        span = pl.ds(g * n, n)
+        back_rows[span, :] = dot(back, block).astype(BF16)
+        out = pltpu.make_async_copy(back_rows.at[span], outgoing.at[span], sems.at[2 + g])
+        out.start()
+        copies.append(out)
+    for c in copies[2:]:
+        c.wait()
+
+
+def shared_kernel(x, tokens, mix_far, *refs):
+    far, (out, nk, nv), (gain, wk, wv, gate, up, down, sems) = refs[:5], refs[5:8], refs[8:]
+    copies = fetch((mix_far, *far), (gain, wk, wv, gate, up, down), sems)
+    for c in copies[:3]:
+        c.wait()
+    mine = rms(tokens[...].astype(F32), gain[...]).astype(BF16)
+    nk[...] = dot(mine, wk[...]).astype(BF16)
+    nv[...] = dot(mine, wv[...]).astype(BF16)
+    copies[3].wait()
+    gated = jax.nn.silu(dot(x[...], gate[...]))
+    copies[4].wait()
+    hidden = (gated * dot(x[...], up[...])).astype(BF16)
+    copies[5].wait()
+    out[...] = dot(hidden, down[...])
 
 
 def final_kernel(returned, routes, weights, resid1, shared, gain, out):
@@ -253,24 +319,11 @@
     return [parts[0]] + [swap(parts[d], XS * d) for d in range(1, GRP)]
 
 
-def copies_kernel(x, out):
-    for i in range(PLANE):
-        out[i] = x[...]
-
-
 def gather_columns(weight):
     line = EP // PLANE
     groups = [[g + line * i for i in range(PLANE)] for g in range(line)]
-    copies = pl.pallas_call(
-        copies_kernel,
-        in_specs=[VMEM],
-        out_specs=VMEM,
-        out_shape=jax.ShapeDtypeStruct((PLANE, SHARD, D), BF16),
-        compiler_params=pltpu.CompilerParams(vmem_limit_bytes=4 * 1024 * 1024),
-        name="copies",
-    )(weight.T)
-    own = lax.all_to_all(copies, "ep", 0, 0, tiled=True, axis_index_groups=groups)
-    return own, swap(own, 1)
+    copies = jnp.broadcast_to(weight.T[None], (PLANE, SHARD, D))
+    return lax.all_to_all(copies, "ep", 0, 0, tiled=True, axis_index_groups=groups)
 
 
 def body(
@@ -281,37 +334,23 @@
     here = lax.axis_index("ep")
     place = jnp.stack([here // XS % GRP, here % 2]).astype(jnp.int32)
     group_tokens = share(tokens)
-    own_q, other_q = gather_columns(query_weight)
+    own_q = gather_columns(query_weight)
+    own_o = gather_columns(output_weight)
     route_rows = jnp.tile(routes.T, (1, NJ))
     weight_rows = jnp.tile(route_weights.T, (1, NJ))
-    rows, new_keys, new_values = call(
-        norm_kernel, 7, [((GRP * SEQ, D), BF16)] + [((SEQ, 2 * HD), BF16)] * 2
-    )(*group_tokens, mix_gain[None], key_weight, value_weight)
+    others = swap(jnp.concatenate(group_tokens, axis=0), 1)
+    (rows,) = call(norm_kernel, 6, [((2 * GRP * SEQ, D), BF16)])(
+        *group_tokens, others, mix_gain[None]
+    )
     piece = ((SEQ, COLS), BF16)
-    queries = call(query_kernel, 4, [piece] * GRP, smem=1)(place, rows, own_q, other_q)
-    own_o, other_o = gather_columns(output_weight)
+    mine, others = call(query_kernel, 2, [((GRP * SEQ, COLS // 2), BF16)] * 2)(rows, own_q)
+    got = swap(others, 1)
+    queries = call(join_kernel, 2, [piece] * GRP)(mine, got)
     queries = trade(queries)
-
-    whole = lambda *shape: pl.BlockSpec(shape, lambda i: (0,) * len(shape))
-    cache_spec = pl.BlockSpec((SUB, LEN, 2 * HD), lambda i: (i, 0, 0))
-    attend = pl.pallas_call(
-        attend_kernel,
-        grid=(SEQ // SUB,),
-        in_specs=[SMEM, SMEM] + [whole(SEQ, COLS)] * GRP + [whole(H, 1), cache_spec, cache_spec],
-        out_specs=whole(SEQ, D),
-        out_shape=jax.ShapeDtypeStruct((SEQ, D), BF16),
-        scratch_shapes=[
-            pltpu.VMEM((GRP, SEQ, COLS), F32),
-            pltpu.VMEM((SEQ * H, 2 * HD), BF16),
-            pltpu.VMEM((BLK, BLK), BF16),
-            pltpu.VMEM((SEQ * H, 2 * HD), F32),
-        ],
-        compiler_params=PARAMS,
-        name="attend",
-    )
     attended = attend(
-        place, lengths, *queries, head_bias[:, None], in_hbm(cache_keys), in_hbm(cache_values)
-    )
+        place, lengths, queries, head_bias[:, None], cache_keys, cache_values
+    )
+    other_o = swap(own_o, 1)
 
     mixed = trade(
         call(output_kernel, 7, [piece] * GRP, smem=1)(place, *share(attended), own_o, other_o)
@@ -323,26 +362,44 @@
     )(place, *mixed, tokens, mix_out_gain[None], ffn_gain[None], route_rows)
 
     incoming = lax.all_to_all(outgoing.reshape(EP, 16, CH), "ep", 0, 0, tiled=True)
-    shared_hidden = (
-        jax.nn.silu(dot(ffn_in, shared_gate)) * dot(ffn_in, shared_up)
-    ).astype(BF16)
-    shared_out = dot(shared_hidden, shared_down)
     result = pl.pallas_call(
         expert_kernel,
         in_specs=[VMEM, VMEM, HBM, HBM],
-        out_specs=VMEM,
+        out_specs=HBM,
         out_shape=jax.ShapeDtypeStruct((EP * 16, CH), BF16),
         scratch_shapes=[
             pltpu.VMEM((EP * CAP, D), BF16),
             pltpu.VMEM((EP * CAP, D), BF16),
             pltpu.VMEM((D, FF), BF16),
             pltpu.VMEM((FF, D), BF16),
-            pltpu.SemaphoreType.DMA((2,)),
+            pltpu.VMEM((EP * 16, CH), BF16),
+            pltpu.SemaphoreType.DMA((10,)),
         ],
         compiler_params=PARAMS,
         name="expert",
     )(incoming.reshape(EP * 16, CH), expert_gate, in_hbm(expert_up), in_hbm(expert_down))
     returned = lax.all_to_all(result.reshape(EP, 16, CH), "ep", 0, 0, tiled=True)
+    shared_out, new_keys, new_values = pl.pallas_call(
+        shared_kernel,
+        in_specs=[VMEM, VMEM] + [HBM] * 6,
+        out_specs=[VMEM] * 3,
+        out_shape=[jax.ShapeDtypeStruct((SEQ, D), F32)]
+        + [jax.ShapeDtypeStruct((SEQ, 2 * HD), BF16)] * 2,
+        scratch_shapes=[
+            pltpu.VMEM((1, D), F32),
+            pltpu.VMEM((D, 2 * HD), BF16),
+            pltpu.VMEM((D, 2 * HD), BF16),
+            pltpu.VMEM((D, FF), BF16),
+            pltpu.VMEM((D, FF), BF16),
+            pltpu.VMEM((FF, D), BF16),
+            pltpu.SemaphoreType.DMA((6,)),
+        ],
+        compiler_params=PARAMS,
+        name="shared",
+    )(
+        ffn_in, tokens, in_hbm(mix_gain[None]), in_hbm(key_weight), in_hbm(value_weight),
+        in_hbm(shared_gate), in_hbm(shared_up), in_hbm(shared_down),
+    )
     (layer_out,) = call(final_kernel, 6, [((SEQ, D), BF16)])(
         returned.reshape(EP * 16, CH), route_rows, weight_rows, resid1, shared_out,
         ffn_out_gain[None],

time: 156 us -> 140 us (0.90)
  waiting for transfers between devices: 55.2 us -> 31.5 us
  blocking collectives: 29 us -> 52.6 us
  starting transfers between devices: 38.3 us -> 30.7 us
  local copies, waits for them, and re-layouts: 8.55 us -> 2.39 us
  matrix products: 4.32 us -> 0 us
  Pallas kernels: 19 us -> 21.6 us
    all_to_all x2 -> x1, waiting for transfers between devices: 27.9 us -> 1.56 us  [gather_columns(): lax.all_to_all(copies, 'ep', 0, 0, tiled=True, axis_index_groups=groups)]
    all_to_all x0 -> x1, blocking collectives: none -> 24.4 us  [gather_columns(): lax.all_to_all(copies, 'ep', 0, 0, tiled=True, axis_index_groups=groups)]
    all_to_all x2 -> x1, starting transfers between devices: 12.8 us -> 3.65 us  [gather_columns(): lax.all_to_all(copies, 'ep', 0, 0, tiled=True, axis_index_groups=groups)]
    unnamed x40 -> x22, local copies, waits for them, and re-layouts: 8.31 us -> 0.06 us
    dot_general x2 -> x0, matrix products: 4.32 us -> none  [dot(): return jnp.dot(a, b, preferred_element_type=F32)]
    ppermute x14 -> x15, waiting for transfers between devices: 12.3 us -> 14.6 us  [swap(): return lax.ppermute(x, 'ep', [(i, i ^ d) for i in range(EP)])]
    broadcast_in_dim x0 -> x2, local copies, waits for them, and re-layouts: none -> 2.08 us  [gather_columns(): copies = jnp.broadcast_to(weight.T[None], (PLANE, SHARD, D))]
    pallas_call x5, Pallas kernels: 9.71 us -> 11.5 us  [the longest x1 6.98 us: attend(): pl.pallas_call(attend_kernel, in_specs=[SMEM, SMEM] + [VMEM] * (GRP + 1)...]
  transfers between devices with their start and end apart: 17 -> 17, of which waited for: 11 -> 12; matrix products, arithmetic and copies ran while one was open for 3% -> 0% of each run, Pallas kernels for 6% -> 8%
where the time goes in v3:
time: 140 us
  blocking collectives  52.6 us (38%)
  waiting for transfers between devices  31.5 us (22%)
  starting transfers between devices  30.7 us (22%)
  Pallas kernels  21.6 us (15%)
  local copies, waits for them, and re-layouts  2.39 us (2%)
    all_to_all x1, blocking collectives, body(): lax.all_to_all(outgoing.reshape(EP, 16, CH), 'ep', 0, 0, tiled=True)  28.1 us
    all_to_all x1, blocking collectives, gather_columns(): lax.all_to_all(copies, 'ep', 0, 0, tiled=True, axis_index_groups=groups)  24.4 us
    ppermute x15, starting transfers between devices, swap(): return lax.ppermute(x, 'ep', [(i, i ^ d) for i in range(EP)])  22.6 us
    all_to_all x1, waiting for transfers between devices, body(): lax.all_to_all(result.reshape(EP, 16, CH), 'ep', 0, 0, tiled=True)  15.4 us
    ppermute x15, waiting for transfers between devices, swap(): return lax.ppermute(x, 'ep', [(i, i ^ d) for i in range(EP)])  14.6 us
    pallas_call x1, Pallas kernels, attend(): pl.pallas_call(attend_kernel, in_specs=[SMEM, SMEM] + [VMEM] * (GRP + 1)...  6.98 us
    pallas_call x1, Pallas kernels, body(): pl.pallas_call(expert_kernel, in_specs=[VMEM, VMEM, HBM, HBM], out_specs=...  5.02 us
    all_to_all x1, starting transfers between devices, body(): lax.all_to_all(result.reshape(EP, 16, CH), 'ep', 0, 0, tiled=True)  4.43 us
  transfers between devices with their start and end apart: 17, of which 12 were waited for; matrix products, arithmetic and copies ran while one was open for 0% of the time, Pallas kernels for 8%

profile of v3, /device:TPU:1, one launch (start us, length us, event | category | flops | bytes accessed | tf_op | source)
XLA Modules:
  0.0 139.7 jit_solution(7664642818874701503)
XLA Ops:
  0.6 0.0 copy-start.7
  0.6 1.0 broadcast_in_dim.31
  1.6 24.4 %all_to_all.20.own = bf16[16,16,2048]{2,1,0:T(8,128)(2,1)S(1)} all-to-all(bf16[16,16,2048]{2,1,0:T(8,128)(2,1)S(1)} %broadcast_in_dim.31), channel_id=1, replica_groups={{0,8,16,24,32,40,48,56,64,72,80,88,96,104,112,120},{1,9,17,25,33,41,49,..., dimensions={0} | all-to-all | bytes 2097152 | tf_op jit(solution)/shard_map/all_to_all | solution.py:326
  26.1 0.0 copy-done.7
  26.1 1.1 broadcast_in_dim.29
  27.2 3.7 %all-to-all-start = ((bf16[16,16,2048]{2,1,0:T(8,128)(2,1)}), bf16[16,16,2048]{2,1,0:T(8,128)(2,1)S(1)}, u32[]{:S(2)}, u32[]{:S(2)}) async-start(bf16[16,16,2048]{2,1,0:T(8,128)(2,1)} %broadcast_in_dim.29), calls=%async_computation | async-start | bytes 2097152 | tf_op jit(solution)/shard_map/all_to_all | solution.py:326
  30.8 0.0 copy-start.10
  30.8 0.0 copy-start.6
  30.9 2.1 %collective-permute-start.11 = (bf16[16,16,2048]{2,1,0:T(8,128)(2,1)S(1)}, bf16[16,16,2048]{2,1,0:T(8,128)(2,1)}, u32[]{:S(2)}, u32[]{:S(2)}) collective-permute-start(bf16[16,16,2048]{2,1,0:T(8,128)(2,1)S(1)} %all_to_all.20.own), channel_id=1, source_target_pairs={{0,1},{1,0},{2,3},{3,2},{4,5},{5,4},{6,7},{7,6},{8,9},{9,8},{10,11... | collective-permute-start | bytes 3145736 | tf_op jit(solution)/shard_map/ppermute | solution.py:311
  33.0 0.0 copy-done.1
  33.0 1.2 collective-permute-start
  34.2 2.5 %collective-permute-start.1 = (bf16[16,2048]{1,0:T(8,128)(2,1)S(1)}, bf16[16,2048]{1,0:T(8,128)(2,1)S(1)}, u32[]{:S(2)}, u32[]{:S(2)}) collective-permute-start(bf16[16,2048]{1,0:T(8,128)(2,1)S(1)} %copy-done.1), channel_id=1, source_target_pairs={{0,4},{1,5},{2,6},{3,7},{4,0},{5,1},{6,2},{7,3},{8,12},{9,13},{10,... | collective-permute-start | bytes 196616 | tf_op jit(solution)/shard_map/ppermute | solution.py:311
  36.7 0.2 collective-permute-start.2
  36.9 0.0 collective-permute-done.t1
  36.9 3.3 %collective-permute-done.1.t2 = bf16[16,2048]{1,0:T(8,128)(2,1)S(1)} collective-permute-done((bf16[16,2048]{1,0:T(8,128)(2,1)S(1)}, bf16[16,2048]{1,0:T(8,128)(2,1)S(1)}, u32[]{:S(2)}, u32[]{:S(2)}) %collective-permute-start.1) | collective-permute-done | bytes 65568 | tf_op jit(solution)/shard_map/ppermute | solution.py:311
  40.1 1.3 collective-permute-done.2.t3
  41.4 1.5 %collective-permute-start.3 = (bf16[64,2048]{1,0:T(8,128)(2,1)S(1)}, bf16[64,2048]{1,0:T(8,128)(2,1)S(1)}, u32[]{:S(2)}, u32[]{:S(2)}) collective-permute-start(bf16[64,2048]{1,0:T(8,128)(2,1)S(1)} %pad_maximum_fusion), channel_id=1, source_target_pairs={{0,1},{1,0},{2,3},{3,2},{4,5},{5,4},{6,7},{7,6},{8,9},{9,8},{10,11... | collective-permute-start | bytes 786440 | tf_op jit(solution)/shard_map/ppermute | solution.py:311
  42.9 1.2 collective-permute-done.3.others
  44.1 0.0 copy-done.2
  44.1 0.2 shard_map.220.rows
  44.3 1.6 %all-to-all-done.own = bf16[16,16,2048]{2,1,0:T(8,128)(2,1)S(1)} async-done(((bf16[16,16,2048]{2,1,0:T(8,128)(2,1)}), bf16[16,16,2048]{2,1,0:T(8,128)(2,1)S(1)}, u32[]{:S(2)}, u32[]{:S(2)}) %all-to-all-start) | async-done | bytes 1048608 | tf_op jit(solution)/shard_map/all_to_all | solution.py:326
  45.9 0.5 shard_map.221
  46.3 3.4 %collective-permute-start.4 = (bf16[64,256]{1,0:T(8,128)(2,1)S(1)}, bf16[64,256]{1,0:T(8,128)(2,1)S(1)}, u32[]{:S(2)}, u32[]{:S(2)}) collective-permute-start(bf16[64,256]{1,0:T(8,128)(2,1)S(1)} %get-tuple-element.20), channel_id=1, source_target_pairs={{0,1},{1,0},{2,3},{3,2},{4,5},{5,4},{6,7},{7,6},{8,9},{9,8},{10,11... | collective-permute-start | bytes 98312 | tf_op jit(solution)/shard_map/ppermute | solution.py:311
  49.7 0.9 collective-permute-done.4.got
  50.6 1.2 collective-permute-start.5
  51.8 2.5 %collective-permute-start.6 = (bf16[16,512]{1,0:T(8,128)(2,1)S(1)}, bf16[16,512]{1,0:T(8,128)(2,1)S(1)}, u32[]{:S(2)}, u32[]{:S(2)}) collective-permute-start(bf16[16,512]{1,0:T(8,128)(2,1)S(1)} %get-tuple-element.23), channel_id=1, source_target_pairs={{0,4},{1,5},{2,6},{3,7},{4,0},{5,1},{6,2},{7,3},{8,12},{9,13},{10,... | collective-permute-start | bytes 49160 | tf_op jit(solution)/shard_map/ppermute | solution.py:311
  54.3 0.2 collective-permute-start.7
  54.5 0.1 pad_add_fusion.place
  54.5 0.0 copy-done.10
  54.5 0.1 copy.24.bias
  54.6 0.0 collective-permute-done.5.q1
  54.6 1.3 collective-permute-done.6.q2
  55.9 2.2 %collective-permute-done.7.q3 = bf16[16,512]{1,0:T(8,128)(2,1)S(1)} collective-permute-done((bf16[16,512]{1,0:T(8,128)(2,1)S(1)}, bf16[16,512]{1,0:T(8,128)(2,1)S(1)}, u32[]{:S(2)}, u32[]{:S(2)}) %collective-permute-start.7) | collective-permute-done | bytes 16416 | tf_op jit(solution)/shard_map/ppermute | solution.py:311
  58.1 0.0 copy-done.6
  58.1 7.0 %attend.1.a0 = bf16[16,2048]{1,0:T(8,128)(2,1)S(1)} custom-call(s32[2]{0:T(128)S(1)} %pad_add_fusion.place, s32[16]{0:T(128)S(1)} %copy-done.6, bf16[16,512]{1,0:T(8,128)(2,1)S(1)} %get-tuple-element.21.q0, bf16[16,512]{1,0:T(8,128)(2,1)S(1)} %collective-permute-done.5.q1, bf16[16,512]{1,0:T(8,128)(2,1)S(1)} %collective-permute-done.6.q2, ...), custom_call_target="tpu_custom_call" | custom-call | tf_op jit(solution)/shard_map/attend/pallas_call | solution.py:166
  65.1 0.0 copy-start.8
  65.1 0.0 copy-start.4
  65.1 0.0 copy-start.5
  65.1 0.0 copy-start
  65.1 0.3 collective-permute-start.10
  65.4 0.0 collective-permute-start.8
  65.4 3.7 %collective-permute-start.9 = (bf16[16,2048]{1,0:T(8,128)(2,1)S(1)}, bf16[16,2048]{1,0:T(8,128)(2,1)S(1)}, u32[]{:S(2)}, u32[]{:S(2)}) collective-permute-start(bf16[16,2048]{1,0:T(8,128)(2,1)S(1)} %attend.1.a0), channel_id=1, source_target_pairs={{0,4},{1,5},{2,6},{3,7},{4,0},{5,1},{6,2},{7,3},{8,12},{9,13},{10,... | collective-permute-start | bytes 196616 | tf_op jit(solution)/shard_map/ppermute | solution.py:311
  69.0 0.5 collective-permute-done.10.a3
  69.5 0.0 collective-permute-done.8.a1
  69.5 1.9 %collective-permute-done.9.a2 = bf16[16,2048]{1,0:T(8,128)(2,1)S(1)} collective-permute-done((bf16[16,2048]{1,0:T(8,128)(2,1)S(1)}, bf16[16,2048]{1,0:T(8,128)(2,1)S(1)}, u32[]{:S(2)}, u32[]{:S(2)}) %collective-permute-start.9) | collective-permute-done | bytes 65568 | tf_op jit(solution)/shard_map/ppermute | solution.py:311
  71.4 0.0 collective-permute-done.11.other
  71.4 2.0 %shard_map.223 = (bf16[16,512]{1,0:T(8,128)(2,1)S(1)}, bf16[16,512]{1,0:T(8,128)(2,1)S(1)}, bf16[16,512]{1,0:T(8,128)(2,1)S(1)}, bf16[16,512]{1,0:T(8,128)(2,1)S(1)}) custom-call(s32[2]{0:T(128)S(1)} %pad_add_fusion.place, bf16[16,2048]{1,0:T(8,128)(2,1)S(1)} %attend.1.a0, bf16[16,2048]{1,0:T(8,128)(2,1)S(1)} %collective-permute-done.8.a1, ...), custom_call_target="tpu_custom_call" | custom-call | tf_op jit(solution)/shard_map/pallas_call | solution.py:356
  73.4 0.1 collective-permute-start.12
  73.6 2.3 %collective-permute-start.13 = (bf16[16,512]{1,0:T(8,128)(2,1)S(1)}, bf16[16,512]{1,0:T(8,128)(2,1)S(1)}, u32[]{:S(2)}, u32[]{:S(2)}) collective-permute-start(bf16[16,512]{1,0:T(8,128)(2,1)S(1)} %get-tuple-element.27), channel_id=1, source_target_pairs={{0,4},{1,5},{2,6},{3,7},{4,0},{5,1},{6,2},{7,3},{8,12},{9,13},{10,... | collective-permute-start | bytes 49160 | tf_op jit(solution)/shard_map/ppermute | solution.py:311
  75.9 1.5 %collective-permute-start.14 = (bf16[16,512]{1,0:T(8,128)(2,1)S(1)}, bf16[16,512]{1,0:T(8,128)(2,1)S(1)}, u32[]{:S(2)}, u32[]{:S(2)}) collective-permute-start(bf16[16,512]{1,0:T(8,128)(2,1)S(1)} %get-tuple-element.28), channel_id=1, source_target_pairs={{0,6},{1,7},{2,4},{3,5},{4,2},{5,3},{6,0},{7,1},{8,14},{9,15},{10,... | collective-permute-start | bytes 49160 | tf_op jit(solution)/shard_map/ppermute | solution.py:311
  77.4 0.1 tile.9.routes
  77.4 0.0 collective-permute-done.12.m1
  77.4 0.2 collective-permute-done.13.m2
  77.7 2.0 %collective-permute-done.14.m3 = bf16[16,512]{1,0:T(8,128)(2,1)S(1)} collective-permute-done((bf16[16,512]{1,0:T(8,128)(2,1)S(1)}, bf16[16,512]{1,0:T(8,128)(2,1)S(1)}, u32[]{:S(2)}, u32[]{:S(2)}) %collective-permute-start.14) | collective-permute-done | bytes 16416 | tf_op jit(solution)/shard_map/ppermute | solution.py:311
  79.7 0.0 copy-done.5
  79.7 1.6 %shard_map.224 = (f32[16,2048]{1,0:T(8,128)S(1)}, bf16[16,2048]{1,0:T(8,128)(2,1)S(1)}, bf16[2048,256]{1,0:T(8,128)(2,1)S(1)}) custom-call(s32[2]{0:T(128)S(1)} %pad_add_fusion.place, bf16[16,512]{1,0:T(8,128)(2,1)S(1)} %get-tuple-element.25.m0, bf16[16,512]{1,0:T(8,128)(2,1)S(1)} %collective-permute-done.12.m1, ...), custom_call_target="tpu_custom_call" | custom-call | tf_op jit(solution)/shard_map/pallas_call | solution.py:358
  81.3 28.1 %all_to_all.21 = bf16[128,16,256]{2,1,0:T(8,128)(2,1)S(1)} all-to-all(bf16[128,16,256]{2,1,0:T(8,128)(2,1)S(1)} %bitcast.17), channel_id=1, replica_groups=mesh['ep'=128] {'ep'}, dimensions={0} | all-to-all | bytes 2097152 | tf_op jit(solution)/shard_map/all_to_all | solution.py:364
  109.4 5.0 %expert.1 = bf16[2048,256]{1,0:T(8,128)(2,1)} custom-call(bf16[2048,256]{1,0:T(8,128)(2,1)S(1)} %bitcast.16, bf16[1,2048,512]{2,1,0:T(8,128)(2,1)S(1)} %copy-done, bf16[1,2048,512]{2,1,0:T(8,128)(2,1)} %up.1, bf16[1,512,2048]{2,1,0:T(8,128)(2,1)} %down.1), custom_call_target="tpu_custom_call" | custom-call | tf_op jit(solution)/shard_map/expert/pallas_call | solution.py:365
  114.4 0.0 copy-start.9
  114.4 4.4 %all-to-all-start.3 = ((bf16[128,16,256]{2,1,0:T(8,128)(2,1)}), bf16[128,16,256]{2,1,0:T(8,128)(2,1)S(1)}, u32[]{:S(2)}, u32[]{:S(2)}) async-start(bf16[128,16,256]{2,1,0:T(8,128)(2,1)} %bitcast.11), calls=%async_computation.3 | async-start | bytes 2097152 | tf_op jit(solution)/shard_map/all_to_all | solution.py:381
  118.9 0.1 tile.21.weights
  119.0 3.9 %shared.1 = (f32[16,2048]{1,0:T(8,128)S(1)}, bf16[16,128]{1,0:T(8,128)(2,1)}, bf16[16,128]{1,0:T(8,128)(2,1)}) custom-call(bf16[16,2048]{1,0:T(8,128)(2,1)S(1)} %get-tuple-element.31.x, bf16[16,2048]{1,0:T(8,128)(2,1)S(1)} %copy-done.1, f32[1,2048]{1,0:T(1,128)} %bitcast.18, bf16[2048,128]{1,0:T(8,128)(2,1)} %refs_0_.1, bf16[2048,128]{1,0:T(8,128)(2,1)} %refs_1_.1, ...), custom_call_target="tpu_custom_call" | custom-call | tf_op jit(solution)/shard_map/shared/pallas_call | solution.py:382
  122.8 15.4 %all-to-all-done.3 = bf16[128,16,256]{2,1,0:T(8,128)(2,1)S(1)} async-done(((bf16[128,16,256]{2,1,0:T(8,128)(2,1)}), bf16[128,16,256]{2,1,0:T(8,128)(2,1)S(1)}, u32[]{:S(2)}, u32[]{:S(2)}) %all-to-all-start.3) | async-done | bytes 1048608 | tf_op jit(solution)/shard_map/all_to_all | solution.py:381
  138.2 1.5 %shard_map.225 = bf16[16,2048]{1,0:T(8,128)(2,1)} custom-call(bf16[2048,256]{1,0:T(8,128)(2,1)S(1)} %bitcast.15, s32[6,128]{1,0:T(8,128)S(1)} %tile.9.routes, f32[6,128]{1,0:T(8,128)S(1)} %tile.21.weights, f32[16,2048]{1,0:T(8,128)S(1)} %get-tuple-element.30.resid1, f32[16,2048]{1,0:T(8,128)S(1)} %get-tuple-element.32.shared, f32[1,2048]{1,0:T(1,128)S(1)} %bitcast.20), custom_call_target="tpu_custom_call" | custom-call | tf_op jit(solution)/shard_map/pallas_call | solution.py:403
  (12 shorter events, 0.0 us)
Async XLA Ops:
  0.6 25.4 %copy-start.7 = (bf16[2048,16]{0,1:T(8,128)(2,1)S(1)}, bf16[2048,16]{0,1:T(8,128)(2,1)}, u32[]{:S(2)}) copy-start(bf16[2048,16]{0,1:T(8,128)(2,1)} %param.29) | copy-start | bytes 196612
  26.1 6.9 %copy-start.1 = (bf16[16,2048]{1,0:T(8,128)(2,1)S(1)}, bf16[16,2048]{1,0:T(8,128)(2,1)}, u32[]{:S(2)}) copy-start(bf16[16,2048]{1,0:T(8,128)(2,1)} %tokens.3) | copy-start | bytes 196612
  26.1 18.0 %copy-start.2 = (f32[2048]{0:T(1024)S(1)}, f32[2048]{0:T(1024)}, u32[]{:S(2)}) copy-start(f32[2048]{0:T(1024)} %param.25) | copy-start | bytes 24580
  27.2 18.7 %all-to-all-start = ((bf16[16,16,2048]{2,1,0:T(8,128)(2,1)}), bf16[16,16,2048]{2,1,0:T(8,128)(2,1)S(1)}, u32[]{:S(2)}, u32[]{:S(2)}) async-start(bf16[16,16,2048]{2,1,0:T(8,128)(2,1)} %broadcast_in_dim.29), calls=%async_computation | async-start | bytes 2097152 | tf_op jit(solution)/shard_map/all_to_all | solution.py:326
  30.8 23.7 %copy-start.10 = (f32[32]{0:T(128)S(1)}, f32[32]{0:T(128)}, u32[]{:S(2)}) copy-start(f32[32]{0:T(128)} %param.32) | copy-start | bytes 388
  30.8 27.2 %copy-start.6 = (s32[16]{0:T(128)S(1)}, s32[16]{0:T(128)}, u32[]{:S(2)}) copy-start(s32[16]{0:T(128)} %lens.1) | copy-start | bytes 196
  30.9 40.6 %collective-permute-start.11 = (bf16[16,16,2048]{2,1,0:T(8,128)(2,1)S(1)}, bf16[16,16,2048]{2,1,0:T(8,128)(2,1)}, u32[]{:S(2)}, u32[]{:S(2)}) collective-permute-start(bf16[16,16,2048]{2,1,0:T(8,128)(2,1)S(1)} %all_to_all.20.own), channel_id=1, source_target_pairs={{0,1},{1,0},{2,3},{3,2},{4,5},{5,4},{6,7},{7,6},{8,9},{9,8},{10,11... | collective-permute-start | bytes 3145736 | tf_op jit(solution)/shard_map/ppermute | solution.py:311
  33.0 3.9 %collective-permute-start = (bf16[16,2048]{1,0:T(8,128)(2,1)S(1)}, bf16[16,2048]{1,0:T(8,128)(2,1)S(1)}, u32[]{:S(2)}, u32[]{:S(2)}) collective-permute-start(bf16[16,2048]{1,0:T(8,128)(2,1)S(1)} %copy-done.1), channel_id=1, source_target_pairs={{0,2},{1,3},{2,0},{3,1},{4,6},{5,7},{6,4},{7,5},{8,10},{9,11},{10,... | collective-permute-start | bytes 196616 | tf_op jit(solution)/shard_map/ppermute | solution.py:311
  34.2 5.9 %collective-permute-start.1 = (bf16[16,2048]{1,0:T(8,128)(2,1)S(1)}, bf16[16,2048]{1,0:T(8,128)(2,1)S(1)}, u32[]{:S(2)}, u32[]{:S(2)}) collective-permute-start(bf16[16,2048]{1,0:T(8,128)(2,1)S(1)} %copy-done.1), channel_id=1, source_target_pairs={{0,4},{1,5},{2,6},{3,7},{4,0},{5,1},{6,2},{7,3},{8,12},{9,13},{10,... | collective-permute-start | bytes 196616 | tf_op jit(solution)/shard_map/ppermute | solution.py:311
  36.7 4.8 %collective-permute-start.2 = (bf16[16,2048]{1,0:T(8,128)(2,1)S(1)}, bf16[16,2048]{1,0:T(8,128)(2,1)S(1)}, u32[]{:S(2)}, u32[]{:S(2)}) collective-permute-start(bf16[16,2048]{1,0:T(8,128)(2,1)S(1)} %copy-done.1), channel_id=1, source_target_pairs={{0,6},{1,7},{2,4},{3,5},{4,2},{5,3},{6,0},{7,1},{8,14},{9,15},{10,... | collective-permute-start | bytes 196616 | tf_op jit(solution)/shard_map/ppermute | solution.py:311
  41.4 2.6 %collective-permute-start.3 = (bf16[64,2048]{1,0:T(8,128)(2,1)S(1)}, bf16[64,2048]{1,0:T(8,128)(2,1)S(1)}, u32[]{:S(2)}, u32[]{:S(2)}) collective-permute-start(bf16[64,2048]{1,0:T(8,128)(2,1)S(1)} %pad_maximum_fusion), channel_id=1, source_target_pairs={{0,1},{1,0},{2,3},{3,2},{4,5},{5,4},{6,7},{7,6},{8,9},{9,8},{10,11... | collective-permute-start | bytes 786440 | tf_op jit(solution)/shard_map/ppermute | solution.py:311
  46.3 4.3 %collective-permute-start.4 = (bf16[64,256]{1,0:T(8,128)(2,1)S(1)}, bf16[64,256]{1,0:T(8,128)(2,1)S(1)}, u32[]{:S(2)}, u32[]{:S(2)}) collective-permute-start(bf16[64,256]{1,0:T(8,128)(2,1)S(1)} %get-tuple-element.20), channel_id=1, source_target_pairs={{0,1},{1,0},{2,3},{3,2},{4,5},{5,4},{6,7},{7,6},{8,9},{9,8},{10,11... | collective-permute-start | bytes 98312 | tf_op jit(solution)/shard_map/ppermute | solution.py:311
  50.6 4.0 %collective-permute-start.5 = (bf16[16,512]{1,0:T(8,128)(2,1)S(1)}, bf16[16,512]{1,0:T(8,128)(2,1)S(1)}, u32[]{:S(2)}, u32[]{:S(2)}) collective-permute-start(bf16[16,512]{1,0:T(8,128)(2,1)S(1)} %get-tuple-element.22), channel_id=1, source_target_pairs={{0,2},{1,3},{2,0},{3,1},{4,6},{5,7},{6,4},{7,5},{8,10},{9,11},{10,... | collective-permute-start | bytes 49160 | tf_op jit(solution)/shard_map/ppermute | solution.py:311
  51.8 4.1 %collective-permute-start.6 = (bf16[16,512]{1,0:T(8,128)(2,1)S(1)}, bf16[16,512]{1,0:T(8,128)(2,1)S(1)}, u32[]{:S(2)}, u32[]{:S(2)}) collective-permute-start(bf16[16,512]{1,0:T(8,128)(2,1)S(1)} %get-tuple-element.23), channel_id=1, source_target_pairs={{0,4},{1,5},{2,6},{3,7},{4,0},{5,1},{6,2},{7,3},{8,12},{9,13},{10,... | collective-permute-start | bytes 49160 | tf_op jit(solution)/shard_map/ppermute | solution.py:311
  54.3 3.8 %collective-permute-start.7 = (bf16[16,512]{1,0:T(8,128)(2,1)S(1)}, bf16[16,512]{1,0:T(8,128)(2,1)S(1)}, u32[]{:S(2)}, u32[]{:S(2)}) collective-permute-start(bf16[16,512]{1,0:T(8,128)(2,1)S(1)} %get-tuple-element.24), channel_id=1, source_target_pairs={{0,6},{1,7},{2,4},{3,5},{4,2},{5,3},{6,0},{7,1},{8,14},{9,15},{10,... | collective-permute-start | bytes 49160 | tf_op jit(solution)/shard_map/ppermute | solution.py:311
  65.1 12.3 %copy-start.8 = (s32[16,6]{0,1:T(8,128)S(1)}, s32[16,6]{0,1:T(8,128)}, u32[]{:S(2)}) copy-start(s32[16,6]{0,1:T(8,128)} %param.34) | copy-start | bytes 1156
  65.1 14.6 %copy-start.4 = (f32[2048]{0:T(1024)S(1)}, f32[2048]{0:T(1024)}, u32[]{:S(2)}) copy-start(f32[2048]{0:T(1024)} %param.26) | copy-start | bytes 24580
  65.1 14.6 %copy-start.5 = (f32[2048]{0:T(1024)S(1)}, f32[2048]{0:T(1024)}, u32[]{:S(2)}) copy-start(f32[2048]{0:T(1024)} %param.27) | copy-start | bytes 24580
  65.1 44.3 %copy-start = (bf16[1,2048,512]{2,1,0:T(8,128)(2,1)S(1)}, bf16[1,2048,512]{2,1,0:T(8,128)(2,1)}, u32[]{:S(2)}) copy-start(bf16[1,2048,512]{2,1,0:T(8,128)(2,1)} %gate.1) | copy-start | bytes 6291460
  65.1 4.4 %collective-permute-start.10 = (bf16[16,2048]{1,0:T(8,128)(2,1)S(1)}, bf16[16,2048]{1,0:T(8,128)(2,1)S(1)}, u32[]{:S(2)}, u32[]{:S(2)}) collective-permute-start(bf16[16,2048]{1,0:T(8,128)(2,1)S(1)} %attend.1.a0), channel_id=1, source_target_pairs={{0,6},{1,7},{2,4},{3,5},{4,2},{5,3},{6,0},{7,1},{8,14},{9,15},{10,... | collective-permute-start | bytes 196616 | tf_op jit(solution)/shard_map/ppermute | solution.py:311
  65.4 4.1 %collective-permute-start.8 = (bf16[16,2048]{1,0:T(8,128)(2,1)S(1)}, bf16[16,2048]{1,0:T(8,128)(2,1)S(1)}, u32[]{:S(2)}, u32[]{:S(2)}) collective-permute-start(bf16[16,2048]{1,0:T(8,128)(2,1)S(1)} %attend.1.a0), channel_id=1, source_target_pairs={{0,2},{1,3},{2,0},{3,1},{4,6},{5,7},{6,4},{7,5},{8,10},{9,11},{10,... | collective-permute-start | bytes 196616 | tf_op jit(solution)/shard_map/ppermute | solution.py:311
  65.4 6.0 %collective-permute-start.9 = (bf16[16,2048]{1,0:T(8,128)(2,1)S(1)}, bf16[16,2048]{1,0:T(8,128)(2,1)S(1)}, u32[]{:S(2)}, u32[]{:S(2)}) collective-permute-start(bf16[16,2048]{1,0:T(8,128)(2,1)S(1)} %attend.1.a0), channel_id=1, source_target_pairs={{0,4},{1,5},{2,6},{3,7},{4,0},{5,1},{6,2},{7,3},{8,12},{9,13},{10,... | collective-permute-start | bytes 196616 | tf_op jit(solution)/shard_map/ppermute | solution.py:311
  73.4 4.0 %collective-permute-start.12 = (bf16[16,512]{1,0:T(8,128)(2,1)S(1)}, bf16[16,512]{1,0:T(8,128)(2,1)S(1)}, u32[]{:S(2)}, u32[]{:S(2)}) collective-permute-start(bf16[16,512]{1,0:T(8,128)(2,1)S(1)} %get-tuple-element.26), channel_id=1, source_target_pairs={{0,2},{1,3},{2,0},{3,1},{4,6},{5,7},{6,4},{7,5},{8,10},{9,11},{10,... | collective-permute-start | bytes 49160 | tf_op jit(solution)/shard_map/ppermute | solution.py:311
  73.6 4.1 %collective-permute-start.13 = (bf16[16,512]{1,0:T(8,128)(2,1)S(1)}, bf16[16,512]{1,0:T(8,128)(2,1)S(1)}, u32[]{:S(2)}, u32[]{:S(2)}) collective-permute-start(bf16[16,512]{1,0:T(8,128)(2,1)S(1)} %get-tuple-element.27), channel_id=1, source_target_pairs={{0,4},{1,5},{2,6},{3,7},{4,0},{5,1},{6,2},{7,3},{8,12},{9,13},{10,... | collective-permute-start | bytes 49160 | tf_op jit(solution)/shard_map/ppermute | solution.py:311
  75.9 3.8 %collective-permute-start.14 = (bf16[16,512]{1,0:T(8,128)(2,1)S(1)}, bf16[16,512]{1,0:T(8,128)(2,1)S(1)}, u32[]{:S(2)}, u32[]{:S(2)}) collective-permute-start(bf16[16,512]{1,0:T(8,128)(2,1)S(1)} %get-tuple-element.28), channel_id=1, source_target_pairs={{0,6},{1,7},{2,4},{3,5},{4,2},{5,3},{6,0},{7,1},{8,14},{9,15},{10,... | collective-permute-start | bytes 49160 | tf_op jit(solution)/shard_map/ppermute | solution.py:311
  114.4 4.5 %copy-start.9 = (f32[16,6]{0,1:T(8,128)S(1)}, f32[16,6]{0,1:T(8,128)}, u32[]{:S(2)}) copy-start(f32[16,6]{0,1:T(8,128)} %param.35) | copy-start | bytes 1156
  114.4 23.8 %all-to-all-start.3 = ((bf16[128,16,256]{2,1,0:T(8,128)(2,1)}), bf16[128,16,256]{2,1,0:T(8,128)(2,1)S(1)}, u32[]{:S(2)}, u32[]{:S(2)}) async-start(bf16[128,16,256]{2,1,0:T(8,128)(2,1)} %bitcast.11), calls=%async_computation.3 | async-start | bytes 2097152 | tf_op jit(solution)/shard_map/all_to_all | solution.py:381
  119.0 19.2 %copy-start.3 = (f32[2048]{0:T(1024)S(1)}, f32[2048]{0:T(1024)}, u32[]{:S(2)}) copy-start(f32[2048]{0:T(1024)} %param.28) | copy-start | bytes 24580

commit v4 on v3

--- a/solution.py
+++ b/solution.py
@@ -99,8 +99,8 @@
                 pltpu.make_async_copy(values.at[part], vbuf.at[part], sems.at[1, g]),
             ]
         )
-        for c in copies[g]:
-            c.start()
+    for c in copies[0]:
+        c.start()
 
     upper[...] = (iota((BLK, BLK), 0) > iota((BLK, BLK), 1)).astype(F32).astype(BF16)
     for i, q in enumerate((q0, q1, q2, q3)):
@@ -124,6 +124,8 @@
     count = LEN // BLK
     for g in range(SEQ // SUB):
         copies[g][0].wait()
+        for c in copies[g + 1] if g + 1 < SEQ // SUB else ():
+            c.start()
         valid, beta, keep, stacked = [], [], [], []
         for u in range(SUB):
             s = g * SUB + u
@@ -209,36 +211,38 @@
     return (x[:, None, :] * block[None, :, :]).reshape(EP * CAP * NJ, NJ * SEQ)
 
 
-def mix_kernel(place, m0, m1, m2, m3, tokens, mix_gain, ffn_gain, routes, resid1, ffn_in, outgoing, pieces):
+def route_kernel(routes, up_far, send, order, up, sem):
+    load = pltpu.make_async_copy(up_far.at[0], up, sem)
+    load.start()
+    send[...] = expand(places(routes, None)).astype(BF16)
+    n = GRP * 128
+    col = iota((n, n), 1)
+    source = ((col >> 5) & 3) * 128 + (col >> 7) * 32 + (col & 31)
+    order[...] = (iota((n, n), 0) == source).astype(F32).astype(BF16)
+    load.wait()
+
+
+def mix_kernel(place, m0, m1, m2, m3, tokens, mix_gain, ffn_gain, send, order, resid1, ffn_in, outgoing, pieces):
     for i, m in enumerate((m0, m1, m2, m3)):
         pieces[i] = m[...]
     own = place[0]
     got = [pieces[own ^ m] for m in range(GRP)]
-    n = GRP * 128
-    col = iota((n, n), 1)
-    source = ((col >> 5) & 3) * 128 + (col >> 7) * 32 + (col & 31)
-    order = (iota((n, n), 0) == source).astype(F32).astype(BF16)
     parts = []
     for i in range(COLS // 128):
         block = jnp.concatenate([g[:, i * 128 : (i + 1) * 128] for g in got], axis=1)
-        parts.append(dot(block, order))
+        parts.append(dot(block, order[...]))
     mixed = jnp.concatenate(parts, axis=1)
     r1 = tokens[...].astype(F32) + rms(mixed, mix_gain[...])
     resid1[...] = r1
     x = rms(r1, ffn_gain[...]).astype(BF16)
     ffn_in[...] = x
     blocks = jnp.concatenate([x[:, j * CH : (j + 1) * CH] for j in range(NJ)], axis=0)
-    send = expand(places(routes, None)).astype(BF16)
-    outgoing[...] = dot(send, blocks).astype(BF16)
-
-
-def expert_kernel(incoming, gate, up, down, outgoing, rows, result, wu, wd, back_rows, sems):
-    copies = [
-        pltpu.make_async_copy(w.at[0], v, sems.at[i])
-        for i, (w, v) in enumerate(((up, wu), (down, wd)))
-    ]
-    for c in copies:
-        c.start()
+    outgoing[...] = dot(send[...], blocks).astype(BF16)
+
+
+def expert_kernel(incoming, gate, up, down, outgoing, rows, result, wd, back_rows, sems):
+    copies = [pltpu.make_async_copy(down.at[0], wd, sems.at[0])]
+    copies[0].start()
     n = 256
     a, b = iota((n, n), 0), iota((n, n), 1)
     order = (b == (a & 31) * NJ + (a >> 5)).astype(F32).astype(BF16)
@@ -248,10 +252,8 @@
         for j in range(NJ):
             rows[g * 32 : (g + 1) * 32, j * CH : (j + 1) * CH] = block[j * 32 : (j + 1) * 32]
     x = rows[...]
-    gated = jax.nn.silu(dot(x, gate[0]))
+    hidden = (jax.nn.silu(dot(x, gate[0])) * dot(x, up[...])).astype(BF16)
     copies[0].wait()
-    hidden = (gated * dot(x, wu[...])).astype(BF16)
-    copies[1].wait()
     result[...] = dot(hidden, wd[...]).astype(BF16)
     for g in range(EP * 16 // n):
         block = jnp.concatenate(
@@ -259,15 +261,15 @@
         )
         span = pl.ds(g * n, n)
         back_rows[span, :] = dot(back, block).astype(BF16)
-        out = pltpu.make_async_copy(back_rows.at[span], outgoing.at[span], sems.at[2 + g])
+        out = pltpu.make_async_copy(back_rows.at[span], outgoing.at[span], sems.at[1 + g])
         out.start()
         copies.append(out)
-    for c in copies[2:]:
+    for c in copies[1:]:
         c.wait()
 
 
-def shared_kernel(x, tokens, mix_far, *refs):
-    far, (out, nk, nv), (gain, wk, wv, gate, up, down, sems) = refs[:5], refs[5:8], refs[8:]
+def shared_kernel(x, tokens, routes, weights, mix_far, *refs):
+    far, (out, high, low, nk, nv), (gain, wk, wv, gate, up, down, sems) = refs[:5], refs[5:10], refs[10:]
     copies = fetch((mix_far, *far), (gain, wk, wv, gate, up, down), sems)
     for c in copies[:3]:
         c.wait()
@@ -280,14 +282,15 @@
     hidden = (gated * dot(x[...], up[...])).astype(BF16)
     copies[5].wait()
     out[...] = dot(hidden, down[...])
-
-
-def final_kernel(returned, routes, weights, resid1, shared, gain, out):
     scaled = expand(places(routes, weights))
     top = scaled.astype(BF16)
-    rest = (scaled - top.astype(F32)).astype(BF16)
+    high[...] = top.T
+    low[...] = (scaled - top.astype(F32)).astype(BF16).T
+
+
+def final_kernel(returned, high, low, resid1, shared, gain, out):
     got = returned[...]
-    total = dot(top.T, got) + dot(rest.T, got)
+    total = dot(high[...], got) + dot(low[...], got)
     routed = jnp.concatenate([total[j * SEQ : (j + 1) * SEQ] for j in range(NJ)], axis=1)
     out[...] = (resid1[...] + rms(routed + shared[...], gain[...])).astype(BF16)
 
@@ -352,38 +355,43 @@
     )
     other_o = swap(own_o, 1)
 
-    mixed = trade(
-        call(output_kernel, 7, [piece] * GRP, smem=1)(place, *share(attended), own_o, other_o)
-    )
+    attended = share(attended)
+    mixed = call(output_kernel, 7, [piece] * GRP, smem=1)(place, *attended, own_o, other_o)
+    send, order, up = call(
+        route_kernel, 2,
+        [((EP * 16, NJ * SEQ), BF16), ((COLS, COLS), BF16), ((D, FF), BF16)],
+        hbm=1, scratch=[pltpu.SemaphoreType.DMA],
+    )(route_rows, in_hbm(expert_up))
+    mixed = trade(mixed)
     resid1, ffn_in, outgoing = call(
-        mix_kernel, 9,
+        mix_kernel, 10,
         [((SEQ, D), F32), ((SEQ, D), BF16), ((EP * 16, CH), BF16)],
         smem=1, scratch=[pltpu.VMEM((GRP, SEQ, COLS), BF16)],
-    )(place, *mixed, tokens, mix_out_gain[None], ffn_gain[None], route_rows)
+    )(place, *mixed, tokens, mix_out_gain[None], ffn_gain[None], send, order)
 
     incoming = lax.all_to_all(outgoing.reshape(EP, 16, CH), "ep", 0, 0, tiled=True)
     result = pl.pallas_call(
         expert_kernel,
-        in_specs=[VMEM, VMEM, HBM, HBM],
+        in_specs=[VMEM, VMEM, VMEM, HBM],
         out_specs=HBM,
         out_shape=jax.ShapeDtypeStruct((EP * 16, CH), BF16),
         scratch_shapes=[
             pltpu.VMEM((EP * CAP, D), BF16),
             pltpu.VMEM((EP * CAP, D), BF16),
-            pltpu.VMEM((D, FF), BF16),
             pltpu.VMEM((FF, D), BF16),
             pltpu.VMEM((EP * 16, CH), BF16),
-            pltpu.SemaphoreType.DMA((10,)),
+            pltpu.SemaphoreType.DMA((9,)),
         ],
         compiler_params=PARAMS,
         name="expert",
-    )(incoming.reshape(EP * 16, CH), expert_gate, in_hbm(expert_up), in_hbm(expert_down))
+    )(incoming.reshape(EP * 16, CH), expert_gate, up, in_hbm(expert_down))
     returned = lax.all_to_all(result.reshape(EP, 16, CH), "ep", 0, 0, tiled=True)
-    shared_out, new_keys, new_values = pl.pallas_call(
+    shared_out, high, low, new_keys, new_values = pl.pallas_call(
         shared_kernel,
-        in_specs=[VMEM, VMEM] + [HBM] * 6,
-        out_specs=[VMEM] * 3,
+        in_specs=[VMEM] * 4 + [HBM] * 6,
+        out_specs=[VMEM] * 5,
         out_shape=[jax.ShapeDtypeStruct((SEQ, D), F32)]
+        + [jax.ShapeDtypeStruct((NJ * SEQ, EP * 16), BF16)] * 2
         + [jax.ShapeDtypeStruct((SEQ, 2 * HD), BF16)] * 2,
         scratch_shapes=[
             pltpu.VMEM((1, D), F32),
@@ -397,11 +405,11 @@
         compiler_params=PARAMS,
         name="shared",
     )(
-        ffn_in, tokens, in_hbm(mix_gain[None]), in_hbm(key_weight), in_hbm(value_weight),
+        ffn_in, tokens, route_rows, weight_rows, in_hbm(mix_gain[None]), in_hbm(key_weight), in_hbm(value_weight),
         in_hbm(shared_gate), in_hbm(shared_up), in_hbm(shared_down),
     )
     (layer_out,) = call(final_kernel, 6, [((SEQ, D), BF16)])(
-        returned.reshape(EP * 16, CH), route_rows, weight_rows, resid1, shared_out,
+        returned.reshape(EP * 16, CH), high, low, resid1, shared_out,
         ffn_out_gain[None],
     )
     return (layer_out, new_keys, new_values)

time: 140 us -> 140 us (level)
    pallas_call x3 -> x4, Pallas kernels: 10.5 us -> 12.1 us  [the longest x1 4.81 us: body(): pl.pallas_call(expert_kernel, in_specs=[VMEM, VMEM, VMEM, HBM], out_specs...]
  transfers between devices with their start and end apart: 17 -> 17, of which waited for: 12 -> 11; matrix products, arithmetic and copies ran while one was open for 0% -> 0% of each run, Pallas kernels for 8% -> 10%
where the time goes in v4:
time: 140 us
  blocking collectives  51.4 us (37%)
  starting transfers between devices  31.3 us (22%)
  waiting for transfers between devices  30.6 us (22%)
  Pallas kernels  23 us (16%)
  local copies, waits for them, and re-layouts  2.38 us (2%)
    all_to_all x1, blocking collectives, body(): lax.all_to_all(outgoing.reshape(EP, 16, CH), 'ep', 0, 0, tiled=True)  27 us
    all_to_all x1, blocking collectives, gather_columns(): lax.all_to_all(copies, 'ep', 0, 0, tiled=True, axis_index_groups=groups)  24.4 us
    ppermute x15, starting transfers between devices, swap(): return lax.ppermute(x, 'ep', [(i, i ^ d) for i in range(EP)])  23.2 us
    all_to_all x1, waiting for transfers between devices, body(): lax.all_to_all(result.reshape(EP, 16, CH), 'ep', 0, 0, tiled=True)  15.1 us
    ppermute x15, waiting for transfers between devices, swap(): return lax.ppermute(x, 'ep', [(i, i ^ d) for i in range(EP)])  13.9 us
    pallas_call x1, Pallas kernels, attend(): pl.pallas_call(attend_kernel, in_specs=[SMEM, SMEM] + [VMEM] * (GRP + 1)...  6.98 us
    pallas_call x1, Pallas kernels, body(): pl.pallas_call(expert_kernel, in_specs=[VMEM, VMEM, VMEM, HBM], out_specs...  4.81 us
    all_to_all x1, starting transfers between devices, body(): lax.all_to_all(result.reshape(EP, 16, CH), 'ep', 0, 0, tiled=True)  4.43 us
  transfers between devices with their start and end apart: 17, of which 11 were waited for; matrix products, arithmetic and copies ran while one was open for 0% of the time, Pallas kernels for 10%

profile of v4, /device:TPU:1, one launch (start us, length us, event | category | flops | bytes accessed | tf_op | source)
XLA Modules:
  0.0 139.6 jit_solution(8084860560765545849)
XLA Ops:
  0.6 0.0 copy-start.7
  0.6 1.0 broadcast_in_dim.31
  1.6 24.4 %all_to_all.20.own = bf16[16,16,2048]{2,1,0:T(8,128)(2,1)S(1)} all-to-all(bf16[16,16,2048]{2,1,0:T(8,128)(2,1)S(1)} %broadcast_in_dim.31), channel_id=1, replica_groups={{0,8,16,24,32,40,48,56,64,72,80,88,96,104,112,120},{1,9,17,25,33,41,49,..., dimensions={0} | all-to-all | bytes 2097152 | tf_op jit(solution)/shard_map/all_to_all | solution.py:329
  26.1 0.0 copy-done.7
  26.1 1.1 broadcast_in_dim.29
  27.2 3.7 %all-to-all-start = ((bf16[16,16,2048]{2,1,0:T(8,128)(2,1)}), bf16[16,16,2048]{2,1,0:T(8,128)(2,1)S(1)}, u32[]{:S(2)}, u32[]{:S(2)}) async-start(bf16[16,16,2048]{2,1,0:T(8,128)(2,1)} %broadcast_in_dim.29), calls=%async_computation | async-start | bytes 2097152 | tf_op jit(solution)/shard_map/all_to_all | solution.py:329
  30.8 0.0 copy-start.10
  30.8 0.0 copy-start.6
  30.8 2.1 %collective-permute-start.11 = (bf16[16,16,2048]{2,1,0:T(8,128)(2,1)S(1)}, bf16[16,16,2048]{2,1,0:T(8,128)(2,1)}, u32[]{:S(2)}, u32[]{:S(2)}) collective-permute-start(bf16[16,16,2048]{2,1,0:T(8,128)(2,1)S(1)} %all_to_all.20.own), channel_id=1, source_target_pairs={{0,1},{1,0},{2,3},{3,2},{4,5},{5,4},{6,7},{7,6},{8,9},{9,8},{10,11... | collective-permute-start | bytes 3145736 | tf_op jit(solution)/shard_map/ppermute | solution.py:314
  33.0 0.0 copy-done.1
  33.0 1.2 collective-permute-start
  34.2 2.5 %collective-permute-start.1 = (bf16[16,2048]{1,0:T(8,128)(2,1)S(1)}, bf16[16,2048]{1,0:T(8,128)(2,1)S(1)}, u32[]{:S(2)}, u32[]{:S(2)}) collective-permute-start(bf16[16,2048]{1,0:T(8,128)(2,1)S(1)} %copy-done.1), channel_id=1, source_target_pairs={{0,4},{1,5},{2,6},{3,7},{4,0},{5,1},{6,2},{7,3},{8,12},{9,13},{10,... | collective-permute-start | bytes 196616 | tf_op jit(solution)/shard_map/ppermute | solution.py:314
  36.7 0.2 collective-permute-start.2
  36.9 0.0 collective-permute-done.t1
  36.9 3.3 %collective-permute-done.1.t2 = bf16[16,2048]{1,0:T(8,128)(2,1)S(1)} collective-permute-done((bf16[16,2048]{1,0:T(8,128)(2,1)S(1)}, bf16[16,2048]{1,0:T(8,128)(2,1)S(1)}, u32[]{:S(2)}, u32[]{:S(2)}) %collective-permute-start.1) | collective-permute-done | bytes 65568 | tf_op jit(solution)/shard_map/ppermute | solution.py:314
  40.1 1.3 collective-permute-done.2.t3
  41.4 1.5 %collective-permute-start.3 = (bf16[64,2048]{1,0:T(8,128)(2,1)S(1)}, bf16[64,2048]{1,0:T(8,128)(2,1)S(1)}, u32[]{:S(2)}, u32[]{:S(2)}) collective-permute-start(bf16[64,2048]{1,0:T(8,128)(2,1)S(1)} %pad_maximum_fusion), channel_id=1, source_target_pairs={{0,1},{1,0},{2,3},{3,2},{4,5},{5,4},{6,7},{7,6},{8,9},{9,8},{10,11... | collective-permute-start | bytes 786440 | tf_op jit(solution)/shard_map/ppermute | solution.py:314
  42.9 1.2 collective-permute-done.3.others
  44.1 0.0 copy-done.2
  44.1 0.2 shard_map.220.rows
  44.3 1.6 %all-to-all-done.own = bf16[16,16,2048]{2,1,0:T(8,128)(2,1)S(1)} async-done(((bf16[16,16,2048]{2,1,0:T(8,128)(2,1)}), bf16[16,16,2048]{2,1,0:T(8,128)(2,1)S(1)}, u32[]{:S(2)}, u32[]{:S(2)}) %all-to-all-start) | async-done | bytes 1048608 | tf_op jit(solution)/shard_map/all_to_all | solution.py:329
  45.9 0.5 shard_map.221
  46.3 3.4 %collective-permute-start.4 = (bf16[64,256]{1,0:T(8,128)(2,1)S(1)}, bf16[64,256]{1,0:T(8,128)(2,1)S(1)}, u32[]{:S(2)}, u32[]{:S(2)}) collective-permute-start(bf16[64,256]{1,0:T(8,128)(2,1)S(1)} %get-tuple-element.25), channel_id=1, source_target_pairs={{0,1},{1,0},{2,3},{3,2},{4,5},{5,4},{6,7},{7,6},{8,9},{9,8},{10,11... | collective-permute-start | bytes 98312 | tf_op jit(solution)/shard_map/ppermute | solution.py:314
  49.7 0.9 collective-permute-done.4.got
  50.6 1.2 collective-permute-start.5
  51.8 2.4 %collective-permute-start.6 = (bf16[16,512]{1,0:T(8,128)(2,1)S(1)}, bf16[16,512]{1,0:T(8,128)(2,1)S(1)}, u32[]{:S(2)}, u32[]{:S(2)}) collective-permute-start(bf16[16,512]{1,0:T(8,128)(2,1)S(1)} %get-tuple-element.28), channel_id=1, source_target_pairs={{0,4},{1,5},{2,6},{3,7},{4,0},{5,1},{6,2},{7,3},{8,12},{9,13},{10,... | collective-permute-start | bytes 49160 | tf_op jit(solution)/shard_map/ppermute | solution.py:314
  54.3 0.2 collective-permute-start.7
  54.5 0.1 pad_add_fusion.place
  54.5 0.1 copy.24.bias
  54.6 0.0 collective-permute-done.5.q1
  54.6 1.3 collective-permute-done.6.q2
  55.9 2.1 %collective-permute-done.7.q3 = bf16[16,512]{1,0:T(8,128)(2,1)S(1)} collective-permute-done((bf16[16,512]{1,0:T(8,128)(2,1)S(1)}, bf16[16,512]{1,0:T(8,128)(2,1)S(1)}, u32[]{:S(2)}, u32[]{:S(2)}) %collective-permute-start.7) | collective-permute-done | bytes 16416 | tf_op jit(solution)/shard_map/ppermute | solution.py:314
  58.1 7.0 %attend.1.a0 = bf16[16,2048]{1,0:T(8,128)(2,1)S(1)} custom-call(s32[2]{0:T(128)S(1)} %pad_add_fusion.place, s32[16]{0:T(128)S(1)} %copy-done.6, bf16[16,512]{1,0:T(8,128)(2,1)S(1)} %get-tuple-element.26.q0, bf16[16,512]{1,0:T(8,128)(2,1)S(1)} %collective-permute-done.5.q1, bf16[16,512]{1,0:T(8,128)(2,1)S(1)} %collective-permute-done.6.q2, ...), custom_call_target="tpu_custom_call" | custom-call | tf_op jit(solution)/shard_map/attend/pallas_call | solution.py:168
  65.1 0.0 copy-start.8
  65.1 0.0 copy-start.3
  65.1 0.0 copy-start.4
  65.1 0.1 collective-permute-start.8
  65.2 1.4 collective-permute-start.9
  66.6 2.5 %collective-permute-start.10 = (bf16[16,2048]{1,0:T(8,128)(2,1)S(1)}, bf16[16,2048]{1,0:T(8,128)(2,1)S(1)}, u32[]{:S(2)}, u32[]{:S(2)}) collective-permute-start(bf16[16,2048]{1,0:T(8,128)(2,1)S(1)} %attend.1.a0), channel_id=1, source_target_pairs={{0,6},{1,7},{2,4},{3,5},{4,2},{5,3},{6,0},{7,1},{8,14},{9,15},{10,... | collective-permute-start | bytes 196616 | tf_op jit(solution)/shard_map/ppermute | solution.py:314
  69.0 0.0 collective-permute-done.8.a1
  69.0 0.9 collective-permute-done.9.a2
  69.9 1.0 collective-permute-done.10.a3
  70.9 0.0 collective-permute-done.11.other
  70.9 2.0 %shard_map.223 = (bf16[16,512]{1,0:T(8,128)(2,1)S(1)}, bf16[16,512]{1,0:T(8,128)(2,1)S(1)}, bf16[16,512]{1,0:T(8,128)(2,1)S(1)}, bf16[16,512]{1,0:T(8,128)(2,1)S(1)}) custom-call(s32[2]{0:T(128)S(1)} %pad_add_fusion.place, bf16[16,2048]{1,0:T(8,128)(2,1)S(1)} %attend.1.a0, bf16[16,2048]{1,0:T(8,128)(2,1)S(1)} %collective-permute-done.8.a1, ...), custom_call_target="tpu_custom_call" | custom-call | tf_op jit(solution)/shard_map/pallas_call | solution.py:359
  72.9 0.5 collective-permute-start.12
  73.3 4.1 %collective-permute-start.13 = (bf16[16,512]{1,0:T(8,128)(2,1)S(1)}, bf16[16,512]{1,0:T(8,128)(2,1)S(1)}, u32[]{:S(2)}, u32[]{:S(2)}) collective-permute-start(bf16[16,512]{1,0:T(8,128)(2,1)S(1)} %get-tuple-element.32), channel_id=1, source_target_pairs={{0,4},{1,5},{2,6},{3,7},{4,0},{5,1},{6,2},{7,3},{8,12},{9,13},{10,... | collective-permute-start | bytes 49160 | tf_op jit(solution)/shard_map/ppermute | solution.py:314
  77.5 0.0 collective-permute-start.14
  77.5 0.1 tile.9.routes
  77.6 1.6 %shard_map.224 = (bf16[2048,128]{1,0:T(8,128)(2,1)S(1)}, bf16[512,512]{1,0:T(8,128)(2,1)S(1)}, bf16[2048,512]{1,0:T(8,128)(2,1)S(1)}) custom-call(s32[6,128]{1,0:T(8,128)S(1)} %tile.9.routes, bf16[1,2048,512]{2,1,0:T(8,128)(2,1)} %up_far.1), custom_call_target="tpu_custom_call" | custom-call | tf_op jit(solution)/shard_map/pallas_call | solution.py:360
  79.2 0.0 copy-start
  79.2 0.0 collective-permute-done.12.m1
  79.2 0.0 collective-permute-done.13.m2
  79.2 2.1 %collective-permute-done.14.m3 = bf16[16,512]{1,0:T(8,128)(2,1)S(1)} collective-permute-done((bf16[16,512]{1,0:T(8,128)(2,1)S(1)}, bf16[16,512]{1,0:T(8,128)(2,1)S(1)}, u32[]{:S(2)}, u32[]{:S(2)}) %collective-permute-start.14) | collective-permute-done | bytes 16416 | tf_op jit(solution)/shard_map/ppermute | solution.py:314
  81.3 0.0 copy-done.3
  81.3 1.6 %shard_map.225 = (f32[16,2048]{1,0:T(8,128)S(1)}, bf16[16,2048]{1,0:T(8,128)(2,1)S(1)}, bf16[2048,256]{1,0:T(8,128)(2,1)S(1)}) custom-call(s32[2]{0:T(128)S(1)} %pad_add_fusion.place, bf16[16,512]{1,0:T(8,128)(2,1)S(1)} %get-tuple-element.30.m0, bf16[16,512]{1,0:T(8,128)(2,1)S(1)} %collective-permute-done.12.m1, ...), custom_call_target="tpu_custom_call" | custom-call | tf_op jit(solution)/shard_map/pallas_call | solution.py:366
  82.8 27.0 %all_to_all.21 = bf16[128,16,256]{2,1,0:T(8,128)(2,1)S(1)} all-to-all(bf16[128,16,256]{2,1,0:T(8,128)(2,1)S(1)} %bitcast.17), channel_id=1, replica_groups=mesh['ep'=128] {'ep'}, dimensions={0} | all-to-all | bytes 2097152 | tf_op jit(solution)/shard_map/all_to_all | solution.py:372
  109.8 4.8 %expert.1 = bf16[2048,256]{1,0:T(8,128)(2,1)} custom-call(bf16[2048,256]{1,0:T(8,128)(2,1)S(1)} %bitcast.16, bf16[1,2048,512]{2,1,0:T(8,128)(2,1)S(1)} %copy-done, bf16[2048,512]{1,0:T(8,128)(2,1)S(1)} %get-tuple-element.37.up, bf16[1,512,2048]{2,1,0:T(8,128)(2,1)} %down.1), custom_call_target="tpu_custom_call" | custom-call | tf_op jit(solution)/shard_map/expert/pallas_call | solution.py:373
  114.6 0.0 copy-start.9
  114.6 4.4 %all-to-all-start.3 = ((bf16[128,16,256]{2,1,0:T(8,128)(2,1)}), bf16[128,16,256]{2,1,0:T(8,128)(2,1)S(1)}, u32[]{:S(2)}, u32[]{:S(2)}) async-start(bf16[128,16,256]{2,1,0:T(8,128)(2,1)} %bitcast.11), calls=%async_computation.3 | async-start | bytes 2097152 | tf_op jit(solution)/shard_map/all_to_all | solution.py:388
  119.1 0.1 tile.21.weights
  119.2 4.1 %shared.1 = (f32[16,2048]{1,0:T(8,128)S(1)}, bf16[128,2048]{1,0:T(8,128)(2,1)S(1)}, bf16[128,2048]{1,0:T(8,128)(2,1)S(1)}, bf16[16,128]{1,0:T(8,128)(2,1)}, bf16[16,128]{1,0:T(8,128)(2,1)}) custom-call(bf16[16,2048]{1,0:T(8,128)(2,1)S(1)} %get-tuple-element.38.x, bf16[16,2048]{1,0:T(8,128)(2,1)S(1)} %copy-done.1, s32[6,128]{1,0:T(8,128)S(1)} %tile.9.routes, ...), custom_call_target="tpu_custom_call" | custom-call | tf_op jit(solution)/shard_map/shared/pallas_call | solution.py:389
  123.3 15.1 %all-to-all-done.3 = bf16[128,16,256]{2,1,0:T(8,128)(2,1)S(1)} async-done(((bf16[128,16,256]{2,1,0:T(8,128)(2,1)}), bf16[128,16,256]{2,1,0:T(8,128)(2,1)S(1)}, u32[]{:S(2)}, u32[]{:S(2)}) %all-to-all-start.3) | async-done | bytes 1048608 | tf_op jit(solution)/shard_map/all_to_all | solution.py:388
  138.4 0.0 copy-done.5
  138.4 1.2 shard_map.226
  (13 shorter events, 0.0 us)
Async XLA Ops:
  0.6 25.4 %copy-start.7 = (bf16[2048,16]{0,1:T(8,128)(2,1)S(1)}, bf16[2048,16]{0,1:T(8,128)(2,1)}, u32[]{:S(2)}) copy-start(bf16[2048,16]{0,1:T(8,128)(2,1)} %param.29) | copy-start | bytes 196612
  26.1 6.9 %copy-start.1 = (bf16[16,2048]{1,0:T(8,128)(2,1)S(1)}, bf16[16,2048]{1,0:T(8,128)(2,1)}, u32[]{:S(2)}) copy-start(bf16[16,2048]{1,0:T(8,128)(2,1)} %tokens.3) | copy-start | bytes 196612
  26.1 18.0 %copy-start.2 = (f32[2048]{0:T(1024)S(1)}, f32[2048]{0:T(1024)}, u32[]{:S(2)}) copy-start(f32[2048]{0:T(1024)} %param.25) | copy-start | bytes 24580
  27.2 18.7 %all-to-all-start = ((bf16[16,16,2048]{2,1,0:T(8,128)(2,1)}), bf16[16,16,2048]{2,1,0:T(8,128)(2,1)S(1)}, u32[]{:S(2)}, u32[]{:S(2)}) async-start(bf16[16,16,2048]{2,1,0:T(8,128)(2,1)} %broadcast_in_dim.29), calls=%async_computation | async-start | bytes 2097152 | tf_op jit(solution)/shard_map/all_to_all | solution.py:329
  30.8 23.7 %copy-start.10 = (f32[32]{0:T(128)S(1)}, f32[32]{0:T(128)}, u32[]{:S(2)}) copy-start(f32[32]{0:T(128)} %param.32) | copy-start | bytes 388
  30.8 27.2 %copy-start.6 = (s32[16]{0:T(128)S(1)}, s32[16]{0:T(128)}, u32[]{:S(2)}) copy-start(s32[16]{0:T(128)} %lens.1) | copy-start | bytes 196
  30.8 40.0 %collective-permute-start.11 = (bf16[16,16,2048]{2,1,0:T(8,128)(2,1)S(1)}, bf16[16,16,2048]{2,1,0:T(8,128)(2,1)}, u32[]{:S(2)}, u32[]{:S(2)}) collective-permute-start(bf16[16,16,2048]{2,1,0:T(8,128)(2,1)S(1)} %all_to_all.20.own), channel_id=1, source_target_pairs={{0,1},{1,0},{2,3},{3,2},{4,5},{5,4},{6,7},{7,6},{8,9},{9,8},{10,11... | collective-permute-start | bytes 3145736 | tf_op jit(solution)/shard_map/ppermute | solution.py:314
  33.0 3.9 %collective-permute-start = (bf16[16,2048]{1,0:T(8,128)(2,1)S(1)}, bf16[16,2048]{1,0:T(8,128)(2,1)S(1)}, u32[]{:S(2)}, u32[]{:S(2)}) collective-permute-start(bf16[16,2048]{1,0:T(8,128)(2,1)S(1)} %copy-done.1), channel_id=1, source_target_pairs={{0,2},{1,3},{2,0},{3,1},{4,6},{5,7},{6,4},{7,5},{8,10},{9,11},{10,... | collective-permute-start | bytes 196616 | tf_op jit(solution)/shard_map/ppermute | solution.py:314
  34.2 5.9 %collective-permute-start.1 = (bf16[16,2048]{1,0:T(8,128)(2,1)S(1)}, bf16[16,2048]{1,0:T(8,128)(2,1)S(1)}, u32[]{:S(2)}, u32[]{:S(2)}) collective-permute-start(bf16[16,2048]{1,0:T(8,128)(2,1)S(1)} %copy-done.1), channel_id=1, source_target_pairs={{0,4},{1,5},{2,6},{3,7},{4,0},{5,1},{6,2},{7,3},{8,12},{9,13},{10,... | collective-permute-start | bytes 196616 | tf_op jit(solution)/shard_map/ppermute | solution.py:314
  36.7 4.8 %collective-permute-start.2 = (bf16[16,2048]{1,0:T(8,128)(2,1)S(1)}, bf16[16,2048]{1,0:T(8,128)(2,1)S(1)}, u32[]{:S(2)}, u32[]{:S(2)}) collective-permute-start(bf16[16,2048]{1,0:T(8,128)(2,1)S(1)} %copy-done.1), channel_id=1, source_target_pairs={{0,6},{1,7},{2,4},{3,5},{4,2},{5,3},{6,0},{7,1},{8,14},{9,15},{10,... | collective-permute-start | bytes 196616 | tf_op jit(solution)/shard_map/ppermute | solution.py:314
  41.4 2.6 %collective-permute-start.3 = (bf16[64,2048]{1,0:T(8,128)(2,1)S(1)}, bf16[64,2048]{1,0:T(8,128)(2,1)S(1)}, u32[]{:S(2)}, u32[]{:S(2)}) collective-permute-start(bf16[64,2048]{1,0:T(8,128)(2,1)S(1)} %pad_maximum_fusion), channel_id=1, source_target_pairs={{0,1},{1,0},{2,3},{3,2},{4,5},{5,4},{6,7},{7,6},{8,9},{9,8},{10,11... | collective-permute-start | bytes 786440 | tf_op jit(solution)/shard_map/ppermute | solution.py:314
  46.3 4.3 %collective-permute-start.4 = (bf16[64,256]{1,0:T(8,128)(2,1)S(1)}, bf16[64,256]{1,0:T(8,128)(2,1)S(1)}, u32[]{:S(2)}, u32[]{:S(2)}) collective-permute-start(bf16[64,256]{1,0:T(8,128)(2,1)S(1)} %get-tuple-element.25), channel_id=1, source_target_pairs={{0,1},{1,0},{2,3},{3,2},{4,5},{5,4},{6,7},{7,6},{8,9},{9,8},{10,11... | collective-permute-start | bytes 98312 | tf_op jit(solution)/shard_map/ppermute | solution.py:314
  50.6 4.0 %collective-permute-start.5 = (bf16[16,512]{1,0:T(8,128)(2,1)S(1)}, bf16[16,512]{1,0:T(8,128)(2,1)S(1)}, u32[]{:S(2)}, u32[]{:S(2)}) collective-permute-start(bf16[16,512]{1,0:T(8,128)(2,1)S(1)} %get-tuple-element.27), channel_id=1, source_target_pairs={{0,2},{1,3},{2,0},{3,1},{4,6},{5,7},{6,4},{7,5},{8,10},{9,11},{10,... | collective-permute-start | bytes 49160 | tf_op jit(solution)/shard_map/ppermute | solution.py:314
  51.8 4.1 %collective-permute-start.6 = (bf16[16,512]{1,0:T(8,128)(2,1)S(1)}, bf16[16,512]{1,0:T(8,128)(2,1)S(1)}, u32[]{:S(2)}, u32[]{:S(2)}) collective-permute-start(bf16[16,512]{1,0:T(8,128)(2,1)S(1)} %get-tuple-element.28), channel_id=1, source_target_pairs={{0,4},{1,5},{2,6},{3,7},{4,0},{5,1},{6,2},{7,3},{8,12},{9,13},{10,... | collective-permute-start | bytes 49160 | tf_op jit(solution)/shard_map/ppermute | solution.py:314
  54.3 3.8 %collective-permute-start.7 = (bf16[16,512]{1,0:T(8,128)(2,1)S(1)}, bf16[16,512]{1,0:T(8,128)(2,1)S(1)}, u32[]{:S(2)}, u32[]{:S(2)}) collective-permute-start(bf16[16,512]{1,0:T(8,128)(2,1)S(1)} %get-tuple-element.29), channel_id=1, source_target_pairs={{0,6},{1,7},{2,4},{3,5},{4,2},{5,3},{6,0},{7,1},{8,14},{9,15},{10,... | collective-permute-start | bytes 49160 | tf_op jit(solution)/shard_map/ppermute | solution.py:314
  65.1 12.4 %copy-start.8 = (s32[16,6]{0,1:T(8,128)S(1)}, s32[16,6]{0,1:T(8,128)}, u32[]{:S(2)}) copy-start(s32[16,6]{0,1:T(8,128)} %param.34) | copy-start | bytes 1156
  65.1 16.2 %copy-start.3 = (f32[2048]{0:T(1024)S(1)}, f32[2048]{0:T(1024)}, u32[]{:S(2)}) copy-start(f32[2048]{0:T(1024)} %param.26) | copy-start | bytes 24580
  65.1 16.2 %copy-start.4 = (f32[2048]{0:T(1024)S(1)}, f32[2048]{0:T(1024)}, u32[]{:S(2)}) copy-start(f32[2048]{0:T(1024)} %param.27) | copy-start | bytes 24580
  65.1 3.9 %collective-permute-start.8 = (bf16[16,2048]{1,0:T(8,128)(2,1)S(1)}, bf16[16,2048]{1,0:T(8,128)(2,1)S(1)}, u32[]{:S(2)}, u32[]{:S(2)}) collective-permute-start(bf16[16,2048]{1,0:T(8,128)(2,1)S(1)} %attend.1.a0), channel_id=1, source_target_pairs={{0,2},{1,3},{2,0},{3,1},{4,6},{5,7},{6,4},{7,5},{8,10},{9,11},{10,... | collective-permute-start | bytes 196616 | tf_op jit(solution)/shard_map/ppermute | solution.py:314
  65.2 4.7 %collective-permute-start.9 = (bf16[16,2048]{1,0:T(8,128)(2,1)S(1)}, bf16[16,2048]{1,0:T(8,128)(2,1)S(1)}, u32[]{:S(2)}, u32[]{:S(2)}) collective-permute-start(bf16[16,2048]{1,0:T(8,128)(2,1)S(1)} %attend.1.a0), channel_id=1, source_target_pairs={{0,4},{1,5},{2,6},{3,7},{4,0},{5,1},{6,2},{7,3},{8,12},{9,13},{10,... | collective-permute-start | bytes 196616 | tf_op jit(solution)/shard_map/ppermute | solution.py:314
  66.6 4.3 %collective-permute-start.10 = (bf16[16,2048]{1,0:T(8,128)(2,1)S(1)}, bf16[16,2048]{1,0:T(8,128)(2,1)S(1)}, u32[]{:S(2)}, u32[]{:S(2)}) collective-permute-start(bf16[16,2048]{1,0:T(8,128)(2,1)S(1)} %attend.1.a0), channel_id=1, source_target_pairs={{0,6},{1,7},{2,4},{3,5},{4,2},{5,3},{6,0},{7,1},{8,14},{9,15},{10,... | collective-permute-start | bytes 196616 | tf_op jit(solution)/shard_map/ppermute | solution.py:314
  72.9 6.3 %collective-permute-start.12 = (bf16[16,512]{1,0:T(8,128)(2,1)S(1)}, bf16[16,512]{1,0:T(8,128)(2,1)S(1)}, u32[]{:S(2)}, u32[]{:S(2)}) collective-permute-start(bf16[16,512]{1,0:T(8,128)(2,1)S(1)} %get-tuple-element.31), channel_id=1, source_target_pairs={{0,2},{1,3},{2,0},{3,1},{4,6},{5,7},{6,4},{7,5},{8,10},{9,11},{10,... | collective-permute-start | bytes 49160 | tf_op jit(solution)/shard_map/ppermute | solution.py:314
  73.3 5.8 %collective-permute-start.13 = (bf16[16,512]{1,0:T(8,128)(2,1)S(1)}, bf16[16,512]{1,0:T(8,128)(2,1)S(1)}, u32[]{:S(2)}, u32[]{:S(2)}) collective-permute-start(bf16[16,512]{1,0:T(8,128)(2,1)S(1)} %get-tuple-element.32), channel_id=1, source_target_pairs={{0,4},{1,5},{2,6},{3,7},{4,0},{5,1},{6,2},{7,3},{8,12},{9,13},{10,... | collective-permute-start | bytes 49160 | tf_op jit(solution)/shard_map/ppermute | solution.py:314
  77.5 3.8 %collective-permute-start.14 = (bf16[16,512]{1,0:T(8,128)(2,1)S(1)}, bf16[16,512]{1,0:T(8,128)(2,1)S(1)}, u32[]{:S(2)}, u32[]{:S(2)}) collective-permute-start(bf16[16,512]{1,0:T(8,128)(2,1)S(1)} %get-tuple-element.33), channel_id=1, source_target_pairs={{0,6},{1,7},{2,4},{3,5},{4,2},{5,3},{6,0},{7,1},{8,14},{9,15},{10,... | collective-permute-start | bytes 49160 | tf_op jit(solution)/shard_map/ppermute | solution.py:314
  79.2 30.6 %copy-start = (bf16[1,2048,512]{2,1,0:T(8,128)(2,1)S(1)}, bf16[1,2048,512]{2,1,0:T(8,128)(2,1)}, u32[]{:S(2)}) copy-start(bf16[1,2048,512]{2,1,0:T(8,128)(2,1)} %gate.1) | copy-start | bytes 6291460
  114.6 4.5 %copy-start.9 = (f32[16,6]{0,1:T(8,128)S(1)}, f32[16,6]{0,1:T(8,128)}, u32[]{:S(2)}) copy-start(f32[16,6]{0,1:T(8,128)} %param.35) | copy-start | bytes 1156
  114.6 23.8 %all-to-all-start.3 = ((bf16[128,16,256]{2,1,0:T(8,128)(2,1)}), bf16[128,16,256]{2,1,0:T(8,128)(2,1)S(1)}, u32[]{:S(2)}, u32[]{:S(2)}) async-start(bf16[128,16,256]{2,1,0:T(8,128)(2,1)} %bitcast.11), calls=%async_computation.3 | async-start | bytes 2097152 | tf_op jit(solution)/shard_map/all_to_all | solution.py:388
  119.2 19.2 %copy-start.5 = (f32[2048]{0:T(1024)S(1)}, f32[2048]{0:T(1024)}, u32[]{:S(2)}) copy-start(f32[2048]{0:T(1024)} %param.28) | copy-start | bytes 24580

commit v5 on v4

--- a/solution.py
+++ b/solution.py
@@ -114,7 +114,7 @@
         target = (plane >> 3) * HD + (m & 1) * 32 + shard
         select.append((col == target).astype(F32).astype(BF16))
         mask = head + (m >> 1) == iota((H, COLS), 0)
-        part = qf[place[0] ^ m]
+        part = qf[(m - place[0]) & (GRP - 1)]
         for u in range(SEQ):
             rows = jnp.broadcast_to(part[u : u + 1], (H, COLS))
             spread[u].append(jnp.where(mask, rows, 0.0).astype(BF16))
@@ -226,7 +226,7 @@
     for i, m in enumerate((m0, m1, m2, m3)):
         pieces[i] = m[...]
     own = place[0]
-    got = [pieces[own ^ m] for m in range(GRP)]
+    got = [pieces[(m - own) & (GRP - 1)] for m in range(GRP)]
     parts = []
     for i in range(COLS // 128):
         block = jnp.concatenate([g[:, i * 128 : (i + 1) * 128] for g in got], axis=1)
@@ -314,12 +314,18 @@
     return lax.ppermute(x, "ep", [(i, i ^ d) for i in range(EP)])
 
 
+def shift(x, d):
+    return lax.ppermute(
+        x, "ep", [(i, i // 8 * 8 + (i // XS + d) % GRP * XS + i % 2) for i in range(EP)]
+    )
+
+
 def share(x):
-    return [x] + [swap(x, XS * d) for d in range(1, GRP)]
+    return [x] + [shift(x, d) for d in range(1, GRP)]
 
 
 def trade(parts):
-    return [parts[0]] + [swap(parts[d], XS * d) for d in range(1, GRP)]
+    return [parts[0]] + [shift(parts[d], -d) for d in range(1, GRP)]
 
 
 def gather_columns(weight):

time: 140 us -> 139 us (level)
  waiting for transfers between devices: 30.6 us -> 29.2 us
    ppermute x15 -> x3, starting transfers between devices: 23.2 us -> 7.04 us  [swap(): return lax.ppermute(x, 'ep', [(i, i ^ d) for i in range(EP)])]
    ppermute x0 -> x12, starting transfers between devices: none -> 15.2 us  [shift(): lax.ppermute(x, 'ep', [(i, i // 8 * 8 + (i // XS + d) % GRP * XS + i % 2)...]
    ppermute x15 -> x3, waiting for transfers between devices: 13.9 us -> 2.02 us  [swap(): return lax.ppermute(x, 'ep', [(i, i ^ d) for i in range(EP)])]
    ppermute x0 -> x12, waiting for transfers between devices: none -> 9.25 us  [shift(): lax.ppermute(x, 'ep', [(i, i // 8 * 8 + (i // XS + d) % GRP * XS + i % 2)...]
where the time goes in v5:
time: 139 us; the launch traced here: 138 us
  blocking collectives  52.4 us (38%)
  starting transfers between devices  30.3 us (22%)
  waiting for transfers between devices  29.2 us (21%)
  Pallas kernels  23.2 us (17%)
  local copies, waits for them, and re-layouts  2.39 us (2%)
    all_to_all x1, blocking collectives, body(): lax.all_to_all(outgoing.reshape(EP, 16, CH), 'ep', 0, 0, tiled=True)  27.9 us
    all_to_all x1, blocking collectives, gather_columns(): lax.all_to_all(copies, 'ep', 0, 0, tiled=True, axis_index_groups=groups)  24.4 us
    ppermute x12, starting transfers between devices, shift(): lax.ppermute(x, 'ep', [(i, i // 8 * 8 + (i // XS + d) % GRP * XS + i % 2)...  15.2 us
    all_to_all x1, waiting for transfers between devices, body(): lax.all_to_all(result.reshape(EP, 16, CH), 'ep', 0, 0, tiled=True)  15.1 us
    ppermute x12, waiting for transfers between devices, shift(): lax.ppermute(x, 'ep', [(i, i // 8 * 8 + (i // XS + d) % GRP * XS + i % 2)...  9.25 us
    pallas_call x1, Pallas kernels, attend(): pl.pallas_call(attend_kernel, in_specs=[SMEM, SMEM] + [VMEM] * (GRP + 1)...  7.21 us
    ppermute x3, starting transfers between devices, swap(): return lax.ppermute(x, 'ep', [(i, i ^ d) for i in range(EP)])  7.04 us
    pallas_call x1, Pallas kernels, body(): pl.pallas_call(expert_kernel, in_specs=[VMEM, VMEM, VMEM, HBM], out_specs...  4.82 us
  transfers between devices with their start and end apart: 17, of which 11 were waited for; matrix products, arithmetic and copies ran while one was open for 0% of the time, Pallas kernels for 10%

profile of v5, /device:TPU:1, one launch (start us, length us, event | category | flops | bytes accessed | tf_op | source)
XLA Modules:
  0.0 138.4 jit_solution(2088017641097186581)
XLA Ops:
  0.6 0.0 copy-start.7
  0.6 1.0 broadcast_in_dim.31
  1.6 24.4 %all_to_all.20.own = bf16[16,16,2048]{2,1,0:T(8,128)(2,1)S(1)} all-to-all(bf16[16,16,2048]{2,1,0:T(8,128)(2,1)S(1)} %broadcast_in_dim.31), channel_id=1, replica_groups={{0,8,16,24,32,40,48,56,64,72,80,88,96,104,112,120},{1,9,17,25,33,41,49,..., dimensions={0} | all-to-all | bytes 2097152 | tf_op jit(solution)/shard_map/all_to_all | solution.py:335
  26.1 0.0 copy-done.7
  26.1 1.1 broadcast_in_dim.29
  27.2 3.7 %all-to-all-start = ((bf16[16,16,2048]{2,1,0:T(8,128)(2,1)}), bf16[16,16,2048]{2,1,0:T(8,128)(2,1)S(1)}, u32[]{:S(2)}, u32[]{:S(2)}) async-start(bf16[16,16,2048]{2,1,0:T(8,128)(2,1)} %broadcast_in_dim.29), calls=%async_computation | async-start | bytes 2097152 | tf_op jit(solution)/shard_map/all_to_all | solution.py:335
  30.8 0.0 copy-start.10
  30.8 0.0 copy-start.6
  30.8 2.1 %collective-permute-start.11 = (bf16[16,16,2048]{2,1,0:T(8,128)(2,1)S(1)}, bf16[16,16,2048]{2,1,0:T(8,128)(2,1)}, u32[]{:S(2)}, u32[]{:S(2)}) collective-permute-start(bf16[16,16,2048]{2,1,0:T(8,128)(2,1)S(1)} %all_to_all.20.own), channel_id=1, source_target_pairs={{0,1},{1,0},{2,3},{3,2},{4,5},{5,4},{6,7},{7,6},{8,9},{9,8},{10,11... | collective-permute-start | bytes 3145736 | tf_op jit(solution)/shard_map/ppermute | solution.py:314
  33.0 0.0 copy-done.1
  33.0 1.2 collective-permute-start
  34.2 2.5 %collective-permute-start.1 = (bf16[16,2048]{1,0:T(8,128)(2,1)S(1)}, bf16[16,2048]{1,0:T(8,128)(2,1)S(1)}, u32[]{:S(2)}, u32[]{:S(2)}) collective-permute-start(bf16[16,2048]{1,0:T(8,128)(2,1)S(1)} %copy-done.1), channel_id=1, source_target_pairs={{0,4},{1,5},{2,6},{3,7},{4,0},{5,1},{6,2},{7,3},{8,12},{9,13},{10,... | collective-permute-start | bytes 196616 | tf_op jit(solution)/shard_map/ppermute | solution.py:318
  36.7 1.2 collective-permute-start.2
  37.8 0.0 collective-permute-done.t1
  37.8 2.3 %collective-permute-done.1.t2 = bf16[16,2048]{1,0:T(8,128)(2,1)S(1)} collective-permute-done((bf16[16,2048]{1,0:T(8,128)(2,1)S(1)}, bf16[16,2048]{1,0:T(8,128)(2,1)S(1)}, u32[]{:S(2)}, u32[]{:S(2)}) %collective-permute-start.1) | collective-permute-done | bytes 65568 | tf_op jit(solution)/shard_map/ppermute | solution.py:318
  40.2 0.0 collective-permute-done.2.t3
  40.2 1.5 %collective-permute-start.3 = (bf16[64,2048]{1,0:T(8,128)(2,1)S(1)}, bf16[64,2048]{1,0:T(8,128)(2,1)S(1)}, u32[]{:S(2)}, u32[]{:S(2)}) collective-permute-start(bf16[64,2048]{1,0:T(8,128)(2,1)S(1)} %pad_maximum_fusion), channel_id=1, source_target_pairs={{0,1},{1,0},{2,3},{3,2},{4,5},{5,4},{6,7},{7,6},{8,9},{9,8},{10,11... | collective-permute-start | bytes 786440 | tf_op jit(solution)/shard_map/ppermute | solution.py:314
  41.7 1.2 collective-permute-done.3.others
  42.8 0.0 copy-done.2
  42.8 0.2 shard_map.220.rows
  43.1 2.8 %all-to-all-done.own = bf16[16,16,2048]{2,1,0:T(8,128)(2,1)S(1)} async-done(((bf16[16,16,2048]{2,1,0:T(8,128)(2,1)}), bf16[16,16,2048]{2,1,0:T(8,128)(2,1)S(1)}, u32[]{:S(2)}, u32[]{:S(2)}) %all-to-all-start) | async-done | bytes 1048608 | tf_op jit(solution)/shard_map/all_to_all | solution.py:335
  45.9 0.5 shard_map.221
  46.3 3.4 %collective-permute-start.4 = (bf16[64,256]{1,0:T(8,128)(2,1)S(1)}, bf16[64,256]{1,0:T(8,128)(2,1)S(1)}, u32[]{:S(2)}, u32[]{:S(2)}) collective-permute-start(bf16[64,256]{1,0:T(8,128)(2,1)S(1)} %get-tuple-element.25), channel_id=1, source_target_pairs={{0,1},{1,0},{2,3},{3,2},{4,5},{5,4},{6,7},{7,6},{8,9},{9,8},{10,11... | collective-permute-start | bytes 98312 | tf_op jit(solution)/shard_map/ppermute | solution.py:314
  49.7 0.9 collective-permute-done.4.got
  50.6 2.5 %collective-permute-start.5 = (bf16[16,512]{1,0:T(8,128)(2,1)S(1)}, bf16[16,512]{1,0:T(8,128)(2,1)S(1)}, u32[]{:S(2)}, u32[]{:S(2)}) collective-permute-start(bf16[16,512]{1,0:T(8,128)(2,1)S(1)} %get-tuple-element.27), channel_id=1, source_target_pairs={{0,6},{1,7},{2,0},{3,1},{4,2},{5,3},{6,4},{7,5},{8,14},{9,15},{10,... | collective-permute-start | bytes 49160 | tf_op jit(solution)/shard_map/ppermute | solution.py:318
  53.1 0.5 collective-permute-start.6
  53.6 0.6 collective-permute-start.7
  54.2 0.1 pad_add_fusion.place
  54.3 0.1 copy.24.bias
  54.4 0.0 collective-permute-done.5.q1
  54.4 2.8 %collective-permute-done.6.q2 = bf16[16,512]{1,0:T(8,128)(2,1)S(1)} collective-permute-done((bf16[16,512]{1,0:T(8,128)(2,1)S(1)}, bf16[16,512]{1,0:T(8,128)(2,1)S(1)}, u32[]{:S(2)}, u32[]{:S(2)}) %collective-permute-start.6) | collective-permute-done | bytes 16416 | tf_op jit(solution)/shard_map/ppermute | solution.py:318
  57.2 0.2 collective-permute-done.7.q3
  57.4 7.2 %attend.1.a0 = bf16[16,2048]{1,0:T(8,128)(2,1)S(1)} custom-call(s32[2]{0:T(128)S(1)} %pad_add_fusion.place, s32[16]{0:T(128)S(1)} %copy-done.6, bf16[16,512]{1,0:T(8,128)(2,1)S(1)} %get-tuple-element.26.q0, bf16[16,512]{1,0:T(8,128)(2,1)S(1)} %collective-permute-done.5.q1, bf16[16,512]{1,0:T(8,128)(2,1)S(1)} %collective-permute-done.6.q2, ...), custom_call_target="tpu_custom_call" | custom-call | tf_op jit(solution)/shard_map/attend/pallas_call | solution.py:168
  64.6 0.0 copy-start.8
  64.6 0.0 copy-start.3
  64.6 0.0 copy-start.4
  64.7 0.1 collective-permute-start.8
  64.7 1.7 %collective-permute-start.9 = (bf16[16,2048]{1,0:T(8,128)(2,1)S(1)}, bf16[16,2048]{1,0:T(8,128)(2,1)S(1)}, u32[]{:S(2)}, u32[]{:S(2)}) collective-permute-start(bf16[16,2048]{1,0:T(8,128)(2,1)S(1)} %attend.1.a0), channel_id=1, source_target_pairs={{0,4},{1,5},{2,6},{3,7},{4,0},{5,1},{6,2},{7,3},{8,12},{9,13},{10,... | collective-permute-start | bytes 196616 | tf_op jit(solution)/shard_map/ppermute | solution.py:318
  66.4 1.9 %collective-permute-start.10 = (bf16[16,2048]{1,0:T(8,128)(2,1)S(1)}, bf16[16,2048]{1,0:T(8,128)(2,1)S(1)}, u32[]{:S(2)}, u32[]{:S(2)}) collective-permute-start(bf16[16,2048]{1,0:T(8,128)(2,1)S(1)} %attend.1.a0), channel_id=1, source_target_pairs={{0,6},{1,7},{2,0},{3,1},{4,2},{5,3},{6,4},{7,5},{8,14},{9,15},{10,... | collective-permute-start | bytes 196616 | tf_op jit(solution)/shard_map/ppermute | solution.py:318
  68.3 1.4 %collective-permute-done.8.a1 = bf16[16,2048]{1,0:T(8,128)(2,1)S(1)} collective-permute-done((bf16[16,2048]{1,0:T(8,128)(2,1)S(1)}, bf16[16,2048]{1,0:T(8,128)(2,1)S(1)}, u32[]{:S(2)}, u32[]{:S(2)}) %collective-permute-start.8) | collective-permute-done | bytes 65568 | tf_op jit(solution)/shard_map/ppermute | solution.py:318
  69.8 0.0 collective-permute-done.9.a2
  69.8 0.6 collective-permute-done.10.a3
  70.3 0.0 collective-permute-done.11.other
  70.3 2.0 %shard_map.223 = (bf16[16,512]{1,0:T(8,128)(2,1)S(1)}, bf16[16,512]{1,0:T(8,128)(2,1)S(1)}, bf16[16,512]{1,0:T(8,128)(2,1)S(1)}, bf16[16,512]{1,0:T(8,128)(2,1)S(1)}) custom-call(s32[2]{0:T(128)S(1)} %pad_add_fusion.place, bf16[16,2048]{1,0:T(8,128)(2,1)S(1)} %attend.1.a0, bf16[16,2048]{1,0:T(8,128)(2,1)S(1)} %collective-permute-done.8.a1, ...), custom_call_target="tpu_custom_call" | custom-call | tf_op jit(solution)/shard_map/pallas_call | solution.py:365
  72.3 2.5 %collective-permute-start.12 = (bf16[16,512]{1,0:T(8,128)(2,1)S(1)}, bf16[16,512]{1,0:T(8,128)(2,1)S(1)}, u32[]{:S(2)}, u32[]{:S(2)}) collective-permute-start(bf16[16,512]{1,0:T(8,128)(2,1)S(1)} %get-tuple-element.31), channel_id=1, source_target_pairs={{0,6},{1,7},{2,0},{3,1},{4,2},{5,3},{6,4},{7,5},{8,14},{9,15},{10,... | collective-permute-start | bytes 49160 | tf_op jit(solution)/shard_map/ppermute | solution.py:318
  74.8 0.3 collective-permute-start.13
  75.1 0.3 collective-permute-start.14
  75.5 0.1 tile.9.routes
  75.6 1.6 %shard_map.224 = (bf16[2048,128]{1,0:T(8,128)(2,1)S(1)}, bf16[512,512]{1,0:T(8,128)(2,1)S(1)}, bf16[2048,512]{1,0:T(8,128)(2,1)S(1)}) custom-call(s32[6,128]{1,0:T(8,128)S(1)} %tile.9.routes, bf16[1,2048,512]{2,1,0:T(8,128)(2,1)} %up_far.1), custom_call_target="tpu_custom_call" | custom-call | tf_op jit(solution)/shard_map/pallas_call | solution.py:366
  77.2 0.0 copy-start
  77.2 0.0 collective-permute-done.12.m1
  77.2 1.7 %collective-permute-done.13.m2 = bf16[16,512]{1,0:T(8,128)(2,1)S(1)} collective-permute-done((bf16[16,512]{1,0:T(8,128)(2,1)S(1)}, bf16[16,512]{1,0:T(8,128)(2,1)S(1)}, u32[]{:S(2)}, u32[]{:S(2)}) %collective-permute-start.13) | collective-permute-done | bytes 16416 | tf_op jit(solution)/shard_map/ppermute | solution.py:318
  78.9 0.2 collective-permute-done.14.m3
  79.1 0.0 copy-done.4
  79.1 1.5 %shard_map.225 = (f32[16,2048]{1,0:T(8,128)S(1)}, bf16[16,2048]{1,0:T(8,128)(2,1)S(1)}, bf16[2048,256]{1,0:T(8,128)(2,1)S(1)}) custom-call(s32[2]{0:T(128)S(1)} %pad_add_fusion.place, bf16[16,512]{1,0:T(8,128)(2,1)S(1)} %get-tuple-element.30.m0, bf16[16,512]{1,0:T(8,128)(2,1)S(1)} %collective-permute-done.12.m1, ...), custom_call_target="tpu_custom_call" | custom-call | tf_op jit(solution)/shard_map/pallas_call | solution.py:372
  80.6 27.9 %all_to_all.21 = bf16[128,16,256]{2,1,0:T(8,128)(2,1)S(1)} all-to-all(bf16[128,16,256]{2,1,0:T(8,128)(2,1)S(1)} %bitcast.17), channel_id=1, replica_groups=mesh['ep'=128] {'ep'}, dimensions={0} | all-to-all | bytes 2097152 | tf_op jit(solution)/shard_map/all_to_all | solution.py:378
  108.6 0.0 copy-done
  108.6 4.8 %expert.1 = bf16[2048,256]{1,0:T(8,128)(2,1)} custom-call(bf16[2048,256]{1,0:T(8,128)(2,1)S(1)} %bitcast.16, bf16[1,2048,512]{2,1,0:T(8,128)(2,1)S(1)} %copy-done, bf16[2048,512]{1,0:T(8,128)(2,1)S(1)} %get-tuple-element.37.up, bf16[1,512,2048]{2,1,0:T(8,128)(2,1)} %down.1), custom_call_target="tpu_custom_call" | custom-call | tf_op jit(solution)/shard_map/expert/pallas_call | solution.py:379
  113.4 0.0 copy-start.9
  113.4 4.4 %all-to-all-start.3 = ((bf16[128,16,256]{2,1,0:T(8,128)(2,1)}), bf16[128,16,256]{2,1,0:T(8,128)(2,1)S(1)}, u32[]{:S(2)}, u32[]{:S(2)}) async-start(bf16[128,16,256]{2,1,0:T(8,128)(2,1)} %bitcast.11), calls=%async_computation.3 | async-start | bytes 2097152 | tf_op jit(solution)/shard_map/all_to_all | solution.py:394
  117.9 0.1 tile.21.weights
  117.9 4.1 %shared.1 = (f32[16,2048]{1,0:T(8,128)S(1)}, bf16[128,2048]{1,0:T(8,128)(2,1)S(1)}, bf16[128,2048]{1,0:T(8,128)(2,1)S(1)}, bf16[16,128]{1,0:T(8,128)(2,1)}, bf16[16,128]{1,0:T(8,128)(2,1)}) custom-call(bf16[16,2048]{1,0:T(8,128)(2,1)S(1)} %get-tuple-element.38.x, bf16[16,2048]{1,0:T(8,128)(2,1)S(1)} %copy-done.1, s32[6,128]{1,0:T(8,128)S(1)} %tile.9.routes, ...), custom_call_target="tpu_custom_call" | custom-call | tf_op jit(solution)/shard_map/shared/pallas_call | solution.py:395
  122.0 15.1 %all-to-all-done.3 = bf16[128,16,256]{2,1,0:T(8,128)(2,1)S(1)} async-done(((bf16[128,16,256]{2,1,0:T(8,128)(2,1)}), bf16[128,16,256]{2,1,0:T(8,128)(2,1)S(1)}, u32[]{:S(2)}, u32[]{:S(2)}) %all-to-all-start.3) | async-done | bytes 1048608 | tf_op jit(solution)/shard_map/all_to_all | solution.py:394
  137.2 1.2 shard_map.226
  (13 shorter events, 0.0 us)
Async XLA Ops:
  0.6 25.4 %copy-start.7 = (bf16[2048,16]{0,1:T(8,128)(2,1)S(1)}, bf16[2048,16]{0,1:T(8,128)(2,1)}, u32[]{:S(2)}) copy-start(bf16[2048,16]{0,1:T(8,128)(2,1)} %param.29) | copy-start | bytes 196612
  26.1 6.9 %copy-start.1 = (bf16[16,2048]{1,0:T(8,128)(2,1)S(1)}, bf16[16,2048]{1,0:T(8,128)(2,1)}, u32[]{:S(2)}) copy-start(bf16[16,2048]{1,0:T(8,128)(2,1)} %tokens.3) | copy-start | bytes 196612
  26.1 16.8 %copy-start.2 = (f32[2048]{0:T(1024)S(1)}, f32[2048]{0:T(1024)}, u32[]{:S(2)}) copy-start(f32[2048]{0:T(1024)} %param.25) | copy-start | bytes 24580
  27.2 18.7 %all-to-all-start = ((bf16[16,16,2048]{2,1,0:T(8,128)(2,1)}), bf16[16,16,2048]{2,1,0:T(8,128)(2,1)S(1)}, u32[]{:S(2)}, u32[]{:S(2)}) async-start(bf16[16,16,2048]{2,1,0:T(8,128)(2,1)} %broadcast_in_dim.29), calls=%async_computation | async-start | bytes 2097152 | tf_op jit(solution)/shard_map/all_to_all | solution.py:335
  30.8 23.5 %copy-start.10 = (f32[32]{0:T(128)S(1)}, f32[32]{0:T(128)}, u32[]{:S(2)}) copy-start(f32[32]{0:T(128)} %param.32) | copy-start | bytes 388
  30.8 26.6 %copy-start.6 = (s32[16]{0:T(128)S(1)}, s32[16]{0:T(128)}, u32[]{:S(2)}) copy-start(s32[16]{0:T(128)} %lens.1) | copy-start | bytes 196
  30.8 39.5 %collective-permute-start.11 = (bf16[16,16,2048]{2,1,0:T(8,128)(2,1)S(1)}, bf16[16,16,2048]{2,1,0:T(8,128)(2,1)}, u32[]{:S(2)}, u32[]{:S(2)}) collective-permute-start(bf16[16,16,2048]{2,1,0:T(8,128)(2,1)S(1)} %all_to_all.20.own), channel_id=1, source_target_pairs={{0,1},{1,0},{2,3},{3,2},{4,5},{5,4},{6,7},{7,6},{8,9},{9,8},{10,11... | collective-permute-start | bytes 3145736 | tf_op jit(solution)/shard_map/ppermute | solution.py:314
  33.0 4.8 %collective-permute-start = (bf16[16,2048]{1,0:T(8,128)(2,1)S(1)}, bf16[16,2048]{1,0:T(8,128)(2,1)S(1)}, u32[]{:S(2)}, u32[]{:S(2)}) collective-permute-start(bf16[16,2048]{1,0:T(8,128)(2,1)S(1)} %copy-done.1), channel_id=1, source_target_pairs={{0,2},{1,3},{2,4},{3,5},{4,6},{5,7},{6,0},{7,1},{8,10},{9,11},{10,... | collective-permute-start | bytes 196616 | tf_op jit(solution)/shard_map/ppermute | solution.py:318
  34.2 5.9 %collective-permute-start.1 = (bf16[16,2048]{1,0:T(8,128)(2,1)S(1)}, bf16[16,2048]{1,0:T(8,128)(2,1)S(1)}, u32[]{:S(2)}, u32[]{:S(2)}) collective-permute-start(bf16[16,2048]{1,0:T(8,128)(2,1)S(1)} %copy-done.1), channel_id=1, source_target_pairs={{0,4},{1,5},{2,6},{3,7},{4,0},{5,1},{6,2},{7,3},{8,12},{9,13},{10,... | collective-permute-start | bytes 196616 | tf_op jit(solution)/shard_map/ppermute | solution.py:318
  36.7 3.5 %collective-permute-start.2 = (bf16[16,2048]{1,0:T(8,128)(2,1)S(1)}, bf16[16,2048]{1,0:T(8,128)(2,1)S(1)}, u32[]{:S(2)}, u32[]{:S(2)}) collective-permute-start(bf16[16,2048]{1,0:T(8,128)(2,1)S(1)} %copy-done.1), channel_id=1, source_target_pairs={{0,6},{1,7},{2,0},{3,1},{4,2},{5,3},{6,4},{7,5},{8,14},{9,15},{10,... | collective-permute-start | bytes 196616 | tf_op jit(solution)/shard_map/ppermute | solution.py:318
  40.2 2.7 %collective-permute-start.3 = (bf16[64,2048]{1,0:T(8,128)(2,1)S(1)}, bf16[64,2048]{1,0:T(8,128)(2,1)S(1)}, u32[]{:S(2)}, u32[]{:S(2)}) collective-permute-start(bf16[64,2048]{1,0:T(8,128)(2,1)S(1)} %pad_maximum_fusion), channel_id=1, source_target_pairs={{0,1},{1,0},{2,3},{3,2},{4,5},{5,4},{6,7},{7,6},{8,9},{9,8},{10,11... | collective-permute-start | bytes 786440 | tf_op jit(solution)/shard_map/ppermute | solution.py:314
  46.3 4.3 %collective-permute-start.4 = (bf16[64,256]{1,0:T(8,128)(2,1)S(1)}, bf16[64,256]{1,0:T(8,128)(2,1)S(1)}, u32[]{:S(2)}, u32[]{:S(2)}) collective-permute-start(bf16[64,256]{1,0:T(8,128)(2,1)S(1)} %get-tuple-element.25), channel_id=1, source_target_pairs={{0,1},{1,0},{2,3},{3,2},{4,5},{5,4},{6,7},{7,6},{8,9},{9,8},{10,11... | collective-permute-start | bytes 98312 | tf_op jit(solution)/shard_map/ppermute | solution.py:314
  50.6 3.8 %collective-permute-start.5 = (bf16[16,512]{1,0:T(8,128)(2,1)S(1)}, bf16[16,512]{1,0:T(8,128)(2,1)S(1)}, u32[]{:S(2)}, u32[]{:S(2)}) collective-permute-start(bf16[16,512]{1,0:T(8,128)(2,1)S(1)} %get-tuple-element.27), channel_id=1, source_target_pairs={{0,6},{1,7},{2,0},{3,1},{4,2},{5,3},{6,4},{7,5},{8,14},{9,15},{10,... | collective-permute-start | bytes 49160 | tf_op jit(solution)/shard_map/ppermute | solution.py:318
  53.1 4.1 %collective-permute-start.6 = (bf16[16,512]{1,0:T(8,128)(2,1)S(1)}, bf16[16,512]{1,0:T(8,128)(2,1)S(1)}, u32[]{:S(2)}, u32[]{:S(2)}) collective-permute-start(bf16[16,512]{1,0:T(8,128)(2,1)S(1)} %get-tuple-element.28), channel_id=1, source_target_pairs={{0,4},{1,5},{2,6},{3,7},{4,0},{5,1},{6,2},{7,3},{8,12},{9,13},{10,... | collective-permute-start | bytes 49160 | tf_op jit(solution)/shard_map/ppermute | solution.py:318
  53.6 3.8 %collective-permute-start.7 = (bf16[16,512]{1,0:T(8,128)(2,1)S(1)}, bf16[16,512]{1,0:T(8,128)(2,1)S(1)}, u32[]{:S(2)}, u32[]{:S(2)}) collective-permute-start(bf16[16,512]{1,0:T(8,128)(2,1)S(1)} %get-tuple-element.29), channel_id=1, source_target_pairs={{0,2},{1,3},{2,4},{3,5},{4,6},{5,7},{6,0},{7,1},{8,10},{9,11},{10,... | collective-permute-start | bytes 49160 | tf_op jit(solution)/shard_map/ppermute | solution.py:318
  64.6 10.9 %copy-start.8 = (s32[16,6]{0,1:T(8,128)S(1)}, s32[16,6]{0,1:T(8,128)}, u32[]{:S(2)}) copy-start(s32[16,6]{0,1:T(8,128)} %param.34) | copy-start | bytes 1156
  64.6 14.4 %copy-start.3 = (f32[2048]{0:T(1024)S(1)}, f32[2048]{0:T(1024)}, u32[]{:S(2)}) copy-start(f32[2048]{0:T(1024)} %param.26) | copy-start | bytes 24580
  64.6 14.4 %copy-start.4 = (f32[2048]{0:T(1024)S(1)}, f32[2048]{0:T(1024)}, u32[]{:S(2)}) copy-start(f32[2048]{0:T(1024)} %param.27) | copy-start | bytes 24580
  64.7 5.1 %collective-permute-start.8 = (bf16[16,2048]{1,0:T(8,128)(2,1)S(1)}, bf16[16,2048]{1,0:T(8,128)(2,1)S(1)}, u32[]{:S(2)}, u32[]{:S(2)}) collective-permute-start(bf16[16,2048]{1,0:T(8,128)(2,1)S(1)} %attend.1.a0), channel_id=1, source_target_pairs={{0,2},{1,3},{2,4},{3,5},{4,6},{5,7},{6,0},{7,1},{8,10},{9,11},{10,... | collective-permute-start | bytes 196616 | tf_op jit(solution)/shard_map/ppermute | solution.py:318
  64.7 5.0 %collective-permute-start.9 = (bf16[16,2048]{1,0:T(8,128)(2,1)S(1)}, bf16[16,2048]{1,0:T(8,128)(2,1)S(1)}, u32[]{:S(2)}, u32[]{:S(2)}) collective-permute-start(bf16[16,2048]{1,0:T(8,128)(2,1)S(1)} %attend.1.a0), channel_id=1, source_target_pairs={{0,4},{1,5},{2,6},{3,7},{4,0},{5,1},{6,2},{7,3},{8,12},{9,13},{10,... | collective-permute-start | bytes 196616 | tf_op jit(solution)/shard_map/ppermute | solution.py:318
  66.4 3.9 %collective-permute-start.10 = (bf16[16,2048]{1,0:T(8,128)(2,1)S(1)}, bf16[16,2048]{1,0:T(8,128)(2,1)S(1)}, u32[]{:S(2)}, u32[]{:S(2)}) collective-permute-start(bf16[16,2048]{1,0:T(8,128)(2,1)S(1)} %attend.1.a0), channel_id=1, source_target_pairs={{0,6},{1,7},{2,0},{3,1},{4,2},{5,3},{6,4},{7,5},{8,14},{9,15},{10,... | collective-permute-start | bytes 196616 | tf_op jit(solution)/shard_map/ppermute | solution.py:318
  72.3 4.8 %collective-permute-start.12 = (bf16[16,512]{1,0:T(8,128)(2,1)S(1)}, bf16[16,512]{1,0:T(8,128)(2,1)S(1)}, u32[]{:S(2)}, u32[]{:S(2)}) collective-permute-start(bf16[16,512]{1,0:T(8,128)(2,1)S(1)} %get-tuple-element.31), channel_id=1, source_target_pairs={{0,6},{1,7},{2,0},{3,1},{4,2},{5,3},{6,4},{7,5},{8,14},{9,15},{10,... | collective-permute-start | bytes 49160 | tf_op jit(solution)/shard_map/ppermute | solution.py:318
  74.8 4.1 %collective-permute-start.13 = (bf16[16,512]{1,0:T(8,128)(2,1)S(1)}, bf16[16,512]{1,0:T(8,128)(2,1)S(1)}, u32[]{:S(2)}, u32[]{:S(2)}) collective-permute-start(bf16[16,512]{1,0:T(8,128)(2,1)S(1)} %get-tuple-element.32), channel_id=1, source_target_pairs={{0,4},{1,5},{2,6},{3,7},{4,0},{5,1},{6,2},{7,3},{8,12},{9,13},{10,... | collective-permute-start | bytes 49160 | tf_op jit(solution)/shard_map/ppermute | solution.py:318
  75.1 3.9 %collective-permute-start.14 = (bf16[16,512]{1,0:T(8,128)(2,1)S(1)}, bf16[16,512]{1,0:T(8,128)(2,1)S(1)}, u32[]{:S(2)}, u32[]{:S(2)}) collective-permute-start(bf16[16,512]{1,0:T(8,128)(2,1)S(1)} %get-tuple-element.33), channel_id=1, source_target_pairs={{0,2},{1,3},{2,4},{3,5},{4,6},{5,7},{6,0},{7,1},{8,10},{9,11},{10,... | collective-permute-start | bytes 49160 | tf_op jit(solution)/shard_map/ppermute | solution.py:318
  77.2 31.4 %copy-start = (bf16[1,2048,512]{2,1,0:T(8,128)(2,1)S(1)}, bf16[1,2048,512]{2,1,0:T(8,128)(2,1)}, u32[]{:S(2)}) copy-start(bf16[1,2048,512]{2,1,0:T(8,128)(2,1)} %gate.1) | copy-start | bytes 6291460
  113.4 4.5 %copy-start.9 = (f32[16,6]{0,1:T(8,128)S(1)}, f32[16,6]{0,1:T(8,128)}, u32[]{:S(2)}) copy-start(f32[16,6]{0,1:T(8,128)} %param.35) | copy-start | bytes 1156
  113.4 23.8 %all-to-all-start.3 = ((bf16[128,16,256]{2,1,0:T(8,128)(2,1)}), bf16[128,16,256]{2,1,0:T(8,128)(2,1)S(1)}, u32[]{:S(2)}, u32[]{:S(2)}) async-start(bf16[128,16,256]{2,1,0:T(8,128)(2,1)} %bitcast.11), calls=%async_computation.3 | async-start | bytes 2097152 | tf_op jit(solution)/shard_map/all_to_all | solution.py:394
  117.9 19.2 %copy-start.5 = (f32[2048]{0:T(1024)S(1)}, f32[2048]{0:T(1024)}, u32[]{:S(2)}) copy-start(f32[2048]{0:T(1024)} %param.28) | copy-start | bytes 24580

commit v6 on v5

--- a/solution.py
+++ b/solution.py
@@ -315,17 +315,20 @@
 
 
 def shift(x, d):
-    return lax.ppermute(
-        x, "ep", [(i, i // 8 * 8 + (i // XS + d) % GRP * XS + i % 2) for i in range(EP)]
-    )
+    return lax.ppermute(x, "ep", [(i, i // 8 * 8 + (i // XS + d) % GRP * XS + i % 2) for i in range(EP)])
+
+
+FAR_FIRST = (2, 1, 3)
 
 
 def share(x):
-    return [x] + [shift(x, d) for d in range(1, GRP)]
+    got = {d: shift(x, d) for d in FAR_FIRST}
+    return [x] + [got[d] for d in range(1, GRP)]
 
 
 def trade(parts):
-    return [parts[0]] + [shift(parts[d], -d) for d in range(1, GRP)]
+    got = {d: shift(parts[d], -d) for d in FAR_FIRST}
+    return [parts[0]] + [got[d] for d in range(1, GRP)]
 
 
 def gather_columns(weight):

time: 139 us -> 139 us (level)
  no operation moved by 1% of the time
where the time goes in v6:
time: 139 us; the launch traced here: 138 us
  blocking collectives  52.4 us (38%)
  starting transfers between devices  30.3 us (22%)
  waiting for transfers between devices  29.2 us (21%)
  Pallas kernels  23.2 us (17%)
  local copies, waits for them, and re-layouts  2.39 us (2%)
    all_to_all x1, blocking collectives, body(): lax.all_to_all(outgoing.reshape(EP, 16, CH), 'ep', 0, 0, tiled=True)  27.9 us
    all_to_all x1, blocking collectives, gather_columns(): lax.all_to_all(copies, 'ep', 0, 0, tiled=True, axis_index_groups=groups)  24.4 us
    ppermute x12, starting transfers between devices, shift(): lax.ppermute(x, 'ep', [(i, i // 8 * 8 + (i // XS + d) % GRP * XS + i % 2)...  15.2 us
    all_to_all x1, waiting for transfers between devices, body(): lax.all_to_all(result.reshape(EP, 16, CH), 'ep', 0, 0, tiled=True)  15.1 us
    ppermute x12, waiting for transfers between devices, shift(): lax.ppermute(x, 'ep', [(i, i // 8 * 8 + (i // XS + d) % GRP * XS + i % 2)...  9.25 us
    pallas_call x1, Pallas kernels, attend(): pl.pallas_call(attend_kernel, in_specs=[SMEM, SMEM] + [VMEM] * (GRP + 1)...  7.21 us
    ppermute x3, starting transfers between devices, swap(): return lax.ppermute(x, 'ep', [(i, i ^ d) for i in range(EP)])  7.04 us
    pallas_call x1, Pallas kernels, body(): pl.pallas_call(expert_kernel, in_specs=[VMEM, VMEM, VMEM, HBM], out_specs...  4.82 us
  transfers between devices with their start and end apart: 17, of which 11 were waited for; matrix products, arithmetic and copies ran while one was open for 0% of the time, Pallas kernels for 10%

profile of v6, /device:TPU:1, one launch (start us, length us, event | category | flops | bytes accessed | tf_op | source)
XLA Modules:
  0.0 138.4 jit_solution(2088017641097186581)
XLA Ops:
  0.6 0.0 copy-start.7
  0.6 1.0 broadcast_in_dim.31
  1.6 24.4 %all_to_all.20.own = bf16[16,16,2048]{2,1,0:T(8,128)(2,1)S(1)} all-to-all(bf16[16,16,2048]{2,1,0:T(8,128)(2,1)S(1)} %broadcast_in_dim.31), channel_id=1, replica_groups={{0,8,16,24,32,40,48,56,64,72,80,88,96,104,112,120},{1,9,17,25,33,41,49,..., dimensions={0} | all-to-all | bytes 2097152 | tf_op jit(solution)/shard_map/all_to_all | solution.py:338
  26.1 0.0 copy-done.7
  26.1 1.1 broadcast_in_dim.29
  27.2 3.7 %all-to-all-start = ((bf16[16,16,2048]{2,1,0:T(8,128)(2,1)}), bf16[16,16,2048]{2,1,0:T(8,128)(2,1)S(1)}, u32[]{:S(2)}, u32[]{:S(2)}) async-start(bf16[16,16,2048]{2,1,0:T(8,128)(2,1)} %broadcast_in_dim.29), calls=%async_computation | async-start | bytes 2097152 | tf_op jit(solution)/shard_map/all_to_all | solution.py:338
  30.8 0.0 copy-start.10
  30.8 0.0 copy-start.6
  30.8 2.1 %collective-permute-start.11 = (bf16[16,16,2048]{2,1,0:T(8,128)(2,1)S(1)}, bf16[16,16,2048]{2,1,0:T(8,128)(2,1)}, u32[]{:S(2)}, u32[]{:S(2)}) collective-permute-start(bf16[16,16,2048]{2,1,0:T(8,128)(2,1)S(1)} %all_to_all.20.own), channel_id=1, source_target_pairs={{0,1},{1,0},{2,3},{3,2},{4,5},{5,4},{6,7},{7,6},{8,9},{9,8},{10,11... | collective-permute-start | bytes 3145736 | tf_op jit(solution)/shard_map/ppermute | solution.py:314
  33.0 0.0 copy-done.1
  33.0 1.2 collective-permute-start
  34.2 2.5 %collective-permute-start.1 = (bf16[16,2048]{1,0:T(8,128)(2,1)S(1)}, bf16[16,2048]{1,0:T(8,128)(2,1)S(1)}, u32[]{:S(2)}, u32[]{:S(2)}) collective-permute-start(bf16[16,2048]{1,0:T(8,128)(2,1)S(1)} %copy-done.1), channel_id=1, source_target_pairs={{0,4},{1,5},{2,6},{3,7},{4,0},{5,1},{6,2},{7,3},{8,12},{9,13},{10,... | collective-permute-start | bytes 196616 | tf_op jit(solution)/shard_map/ppermute | solution.py:318
  36.7 1.2 collective-permute-start.2
  37.8 0.0 collective-permute-done.t1
  37.8 2.3 %collective-permute-done.1.t2 = bf16[16,2048]{1,0:T(8,128)(2,1)S(1)} collective-permute-done((bf16[16,2048]{1,0:T(8,128)(2,1)S(1)}, bf16[16,2048]{1,0:T(8,128)(2,1)S(1)}, u32[]{:S(2)}, u32[]{:S(2)}) %collective-permute-start.1) | collective-permute-done | bytes 65568 | tf_op jit(solution)/shard_map/ppermute | solution.py:318
  40.2 0.0 collective-permute-done.2.t3
  40.2 1.5 %collective-permute-start.3 = (bf16[64,2048]{1,0:T(8,128)(2,1)S(1)}, bf16[64,2048]{1,0:T(8,128)(2,1)S(1)}, u32[]{:S(2)}, u32[]{:S(2)}) collective-permute-start(bf16[64,2048]{1,0:T(8,128)(2,1)S(1)} %pad_maximum_fusion), channel_id=1, source_target_pairs={{0,1},{1,0},{2,3},{3,2},{4,5},{5,4},{6,7},{7,6},{8,9},{9,8},{10,11... | collective-permute-start | bytes 786440 | tf_op jit(solution)/shard_map/ppermute | solution.py:314
  41.7 1.2 collective-permute-done.3.others
  42.8 0.0 copy-done.2
  42.8 0.2 shard_map.220.rows
  43.1 2.8 %all-to-all-done.own = bf16[16,16,2048]{2,1,0:T(8,128)(2,1)S(1)} async-done(((bf16[16,16,2048]{2,1,0:T(8,128)(2,1)}), bf16[16,16,2048]{2,1,0:T(8,128)(2,1)S(1)}, u32[]{:S(2)}, u32[]{:S(2)}) %all-to-all-start) | async-done | bytes 1048608 | tf_op jit(solution)/shard_map/all_to_all | solution.py:338
  45.9 0.5 shard_map.221
  46.3 3.4 %collective-permute-start.4 = (bf16[64,256]{1,0:T(8,128)(2,1)S(1)}, bf16[64,256]{1,0:T(8,128)(2,1)S(1)}, u32[]{:S(2)}, u32[]{:S(2)}) collective-permute-start(bf16[64,256]{1,0:T(8,128)(2,1)S(1)} %get-tuple-element.25), channel_id=1, source_target_pairs={{0,1},{1,0},{2,3},{3,2},{4,5},{5,4},{6,7},{7,6},{8,9},{9,8},{10,11... | collective-permute-start | bytes 98312 | tf_op jit(solution)/shard_map/ppermute | solution.py:314
  49.7 0.9 collective-permute-done.4.got
  50.6 2.5 %collective-permute-start.5 = (bf16[16,512]{1,0:T(8,128)(2,1)S(1)}, bf16[16,512]{1,0:T(8,128)(2,1)S(1)}, u32[]{:S(2)}, u32[]{:S(2)}) collective-permute-start(bf16[16,512]{1,0:T(8,128)(2,1)S(1)} %get-tuple-element.27), channel_id=1, source_target_pairs={{0,6},{1,7},{2,0},{3,1},{4,2},{5,3},{6,4},{7,5},{8,14},{9,15},{10,... | collective-permute-start | bytes 49160 | tf_op jit(solution)/shard_map/ppermute | solution.py:318
  53.1 0.5 collective-permute-start.6
  53.6 0.6 collective-permute-start.7
  54.2 0.1 pad_add_fusion.place
  54.3 0.1 copy.24.bias
  54.4 0.0 collective-permute-done.5.q1
  54.4 2.8 %collective-permute-done.6.q2 = bf16[16,512]{1,0:T(8,128)(2,1)S(1)} collective-permute-done((bf16[16,512]{1,0:T(8,128)(2,1)S(1)}, bf16[16,512]{1,0:T(8,128)(2,1)S(1)}, u32[]{:S(2)}, u32[]{:S(2)}) %collective-permute-start.6) | collective-permute-done | bytes 16416 | tf_op jit(solution)/shard_map/ppermute | solution.py:318
  57.2 0.2 collective-permute-done.7.q3
  57.4 7.2 %attend.1.a0 = bf16[16,2048]{1,0:T(8,128)(2,1)S(1)} custom-call(s32[2]{0:T(128)S(1)} %pad_add_fusion.place, s32[16]{0:T(128)S(1)} %copy-done.6, bf16[16,512]{1,0:T(8,128)(2,1)S(1)} %get-tuple-element.26.q0, bf16[16,512]{1,0:T(8,128)(2,1)S(1)} %collective-permute-done.5.q1, bf16[16,512]{1,0:T(8,128)(2,1)S(1)} %collective-permute-done.6.q2, ...), custom_call_target="tpu_custom_call" | custom-call | tf_op jit(solution)/shard_map/attend/pallas_call | solution.py:168
  64.6 0.0 copy-start.8
  64.6 0.0 copy-start.3
  64.6 0.0 copy-start.4
  64.7 0.1 collective-permute-start.8
  64.7 1.7 %collective-permute-start.9 = (bf16[16,2048]{1,0:T(8,128)(2,1)S(1)}, bf16[16,2048]{1,0:T(8,128)(2,1)S(1)}, u32[]{:S(2)}, u32[]{:S(2)}) collective-permute-start(bf16[16,2048]{1,0:T(8,128)(2,1)S(1)} %attend.1.a0), channel_id=1, source_target_pairs={{0,4},{1,5},{2,6},{3,7},{4,0},{5,1},{6,2},{7,3},{8,12},{9,13},{10,... | collective-permute-start | bytes 196616 | tf_op jit(solution)/shard_map/ppermute | solution.py:318
  66.4 1.9 %collective-permute-start.10 = (bf16[16,2048]{1,0:T(8,128)(2,1)S(1)}, bf16[16,2048]{1,0:T(8,128)(2,1)S(1)}, u32[]{:S(2)}, u32[]{:S(2)}) collective-permute-start(bf16[16,2048]{1,0:T(8,128)(2,1)S(1)} %attend.1.a0), channel_id=1, source_target_pairs={{0,6},{1,7},{2,0},{3,1},{4,2},{5,3},{6,4},{7,5},{8,14},{9,15},{10,... | collective-permute-start | bytes 196616 | tf_op jit(solution)/shard_map/ppermute | solution.py:318
  68.3 1.4 %collective-permute-done.8.a1 = bf16[16,2048]{1,0:T(8,128)(2,1)S(1)} collective-permute-done((bf16[16,2048]{1,0:T(8,128)(2,1)S(1)}, bf16[16,2048]{1,0:T(8,128)(2,1)S(1)}, u32[]{:S(2)}, u32[]{:S(2)}) %collective-permute-start.8) | collective-permute-done | bytes 65568 | tf_op jit(solution)/shard_map/ppermute | solution.py:318
  69.8 0.0 collective-permute-done.9.a2
  69.8 0.6 collective-permute-done.10.a3
  70.3 0.0 collective-permute-done.11.other
  70.3 2.0 %shard_map.223 = (bf16[16,512]{1,0:T(8,128)(2,1)S(1)}, bf16[16,512]{1,0:T(8,128)(2,1)S(1)}, bf16[16,512]{1,0:T(8,128)(2,1)S(1)}, bf16[16,512]{1,0:T(8,128)(2,1)S(1)}) custom-call(s32[2]{0:T(128)S(1)} %pad_add_fusion.place, bf16[16,2048]{1,0:T(8,128)(2,1)S(1)} %attend.1.a0, bf16[16,2048]{1,0:T(8,128)(2,1)S(1)} %collective-permute-done.8.a1, ...), custom_call_target="tpu_custom_call" | custom-call | tf_op jit(solution)/shard_map/pallas_call | solution.py:368
  72.3 2.5 %collective-permute-start.12 = (bf16[16,512]{1,0:T(8,128)(2,1)S(1)}, bf16[16,512]{1,0:T(8,128)(2,1)S(1)}, u32[]{:S(2)}, u32[]{:S(2)}) collective-permute-start(bf16[16,512]{1,0:T(8,128)(2,1)S(1)} %get-tuple-element.31), channel_id=1, source_target_pairs={{0,6},{1,7},{2,0},{3,1},{4,2},{5,3},{6,4},{7,5},{8,14},{9,15},{10,... | collective-permute-start | bytes 49160 | tf_op jit(solution)/shard_map/ppermute | solution.py:318
  74.8 0.3 collective-permute-start.13
  75.1 0.3 collective-permute-start.14
  75.5 0.1 tile.9.routes
  75.6 1.6 %shard_map.224 = (bf16[2048,128]{1,0:T(8,128)(2,1)S(1)}, bf16[512,512]{1,0:T(8,128)(2,1)S(1)}, bf16[2048,512]{1,0:T(8,128)(2,1)S(1)}) custom-call(s32[6,128]{1,0:T(8,128)S(1)} %tile.9.routes, bf16[1,2048,512]{2,1,0:T(8,128)(2,1)} %up_far.1), custom_call_target="tpu_custom_call" | custom-call | tf_op jit(solution)/shard_map/pallas_call | solution.py:369
  77.2 0.0 copy-start
  77.2 0.0 collective-permute-done.12.m1
  77.2 1.7 %collective-permute-done.13.m2 = bf16[16,512]{1,0:T(8,128)(2,1)S(1)} collective-permute-done((bf16[16,512]{1,0:T(8,128)(2,1)S(1)}, bf16[16,512]{1,0:T(8,128)(2,1)S(1)}, u32[]{:S(2)}, u32[]{:S(2)}) %collective-permute-start.13) | collective-permute-done | bytes 16416 | tf_op jit(solution)/shard_map/ppermute | solution.py:318
  78.9 0.2 collective-permute-done.14.m3
  79.1 0.0 copy-done.4
  79.1 1.5 %shard_map.225 = (f32[16,2048]{1,0:T(8,128)S(1)}, bf16[16,2048]{1,0:T(8,128)(2,1)S(1)}, bf16[2048,256]{1,0:T(8,128)(2,1)S(1)}) custom-call(s32[2]{0:T(128)S(1)} %pad_add_fusion.place, bf16[16,512]{1,0:T(8,128)(2,1)S(1)} %get-tuple-element.30.m0, bf16[16,512]{1,0:T(8,128)(2,1)S(1)} %collective-permute-done.12.m1, ...), custom_call_target="tpu_custom_call" | custom-call | tf_op jit(solution)/shard_map/pallas_call | solution.py:375
  80.6 27.9 %all_to_all.21 = bf16[128,16,256]{2,1,0:T(8,128)(2,1)S(1)} all-to-all(bf16[128,16,256]{2,1,0:T(8,128)(2,1)S(1)} %bitcast.17), channel_id=1, replica_groups=mesh['ep'=128] {'ep'}, dimensions={0} | all-to-all | bytes 2097152 | tf_op jit(solution)/shard_map/all_to_all | solution.py:381
  108.6 0.0 copy-done
  108.6 4.8 %expert.1 = bf16[2048,256]{1,0:T(8,128)(2,1)} custom-call(bf16[2048,256]{1,0:T(8,128)(2,1)S(1)} %bitcast.16, bf16[1,2048,512]{2,1,0:T(8,128)(2,1)S(1)} %copy-done, bf16[2048,512]{1,0:T(8,128)(2,1)S(1)} %get-tuple-element.37.up, bf16[1,512,2048]{2,1,0:T(8,128)(2,1)} %down.1), custom_call_target="tpu_custom_call" | custom-call | tf_op jit(solution)/shard_map/expert/pallas_call | solution.py:382
  113.4 0.0 copy-start.9
  113.4 4.4 %all-to-all-start.3 = ((bf16[128,16,256]{2,1,0:T(8,128)(2,1)}), bf16[128,16,256]{2,1,0:T(8,128)(2,1)S(1)}, u32[]{:S(2)}, u32[]{:S(2)}) async-start(bf16[128,16,256]{2,1,0:T(8,128)(2,1)} %bitcast.11), calls=%async_computation.3 | async-start | bytes 2097152 | tf_op jit(solution)/shard_map/all_to_all | solution.py:397
  117.9 0.1 tile.21.weights
  117.9 4.1 %shared.1 = (f32[16,2048]{1,0:T(8,128)S(1)}, bf16[128,2048]{1,0:T(8,128)(2,1)S(1)}, bf16[128,2048]{1,0:T(8,128)(2,1)S(1)}, bf16[16,128]{1,0:T(8,128)(2,1)}, bf16[16,128]{1,0:T(8,128)(2,1)}) custom-call(bf16[16,2048]{1,0:T(8,128)(2,1)S(1)} %get-tuple-element.38.x, bf16[16,2048]{1,0:T(8,128)(2,1)S(1)} %copy-done.1, s32[6,128]{1,0:T(8,128)S(1)} %tile.9.routes, ...), custom_call_target="tpu_custom_call" | custom-call | tf_op jit(solution)/shard_map/shared/pallas_call | solution.py:398
  122.0 15.1 %all-to-all-done.3 = bf16[128,16,256]{2,1,0:T(8,128)(2,1)S(1)} async-done(((bf16[128,16,256]{2,1,0:T(8,128)(2,1)}), bf16[128,16,256]{2,1,0:T(8,128)(2,1)S(1)}, u32[]{:S(2)}, u32[]{:S(2)}) %all-to-all-start.3) | async-done | bytes 1048608 | tf_op jit(solution)/shard_map/all_to_all | solution.py:397
  137.2 1.2 shard_map.226
  (13 shorter events, 0.0 us)
Async XLA Ops:
  0.6 25.4 %copy-start.7 = (bf16[2048,16]{0,1:T(8,128)(2,1)S(1)}, bf16[2048,16]{0,1:T(8,128)(2,1)}, u32[]{:S(2)}) copy-start(bf16[2048,16]{0,1:T(8,128)(2,1)} %param.29) | copy-start | bytes 196612
  26.1 6.9 %copy-start.1 = (bf16[16,2048]{1,0:T(8,128)(2,1)S(1)}, bf16[16,2048]{1,0:T(8,128)(2,1)}, u32[]{:S(2)}) copy-start(bf16[16,2048]{1,0:T(8,128)(2,1)} %tokens.3) | copy-start | bytes 196612
  26.1 16.8 %copy-start.2 = (f32[2048]{0:T(1024)S(1)}, f32[2048]{0:T(1024)}, u32[]{:S(2)}) copy-start(f32[2048]{0:T(1024)} %param.25) | copy-start | bytes 24580
  27.2 18.7 %all-to-all-start = ((bf16[16,16,2048]{2,1,0:T(8,128)(2,1)}), bf16[16,16,2048]{2,1,0:T(8,128)(2,1)S(1)}, u32[]{:S(2)}, u32[]{:S(2)}) async-start(bf16[16,16,2048]{2,1,0:T(8,128)(2,1)} %broadcast_in_dim.29), calls=%async_computation | async-start | bytes 2097152 | tf_op jit(solution)/shard_map/all_to_all | solution.py:338
  30.8 23.5 %copy-start.10 = (f32[32]{0:T(128)S(1)}, f32[32]{0:T(128)}, u32[]{:S(2)}) copy-start(f32[32]{0:T(128)} %param.32) | copy-start | bytes 388
  30.8 26.6 %copy-start.6 = (s32[16]{0:T(128)S(1)}, s32[16]{0:T(128)}, u32[]{:S(2)}) copy-start(s32[16]{0:T(128)} %lens.1) | copy-start | bytes 196
  30.8 39.5 %collective-permute-start.11 = (bf16[16,16,2048]{2,1,0:T(8,128)(2,1)S(1)}, bf16[16,16,2048]{2,1,0:T(8,128)(2,1)}, u32[]{:S(2)}, u32[]{:S(2)}) collective-permute-start(bf16[16,16,2048]{2,1,0:T(8,128)(2,1)S(1)} %all_to_all.20.own), channel_id=1, source_target_pairs={{0,1},{1,0},{2,3},{3,2},{4,5},{5,4},{6,7},{7,6},{8,9},{9,8},{10,11... | collective-permute-start | bytes 3145736 | tf_op jit(solution)/shard_map/ppermute | solution.py:314
  33.0 4.8 %collective-permute-start = (bf16[16,2048]{1,0:T(8,128)(2,1)S(1)}, bf16[16,2048]{1,0:T(8,128)(2,1)S(1)}, u32[]{:S(2)}, u32[]{:S(2)}) collective-permute-start(bf16[16,2048]{1,0:T(8,128)(2,1)S(1)} %copy-done.1), channel_id=1, source_target_pairs={{0,2},{1,3},{2,4},{3,5},{4,6},{5,7},{6,0},{7,1},{8,10},{9,11},{10,... | collective-permute-start | bytes 196616 | tf_op jit(solution)/shard_map/ppermute | solution.py:318
  34.2 5.9 %collective-permute-start.1 = (bf16[16,2048]{1,0:T(8,128)(2,1)S(1)}, bf16[16,2048]{1,0:T(8,128)(2,1)S(1)}, u32[]{:S(2)}, u32[]{:S(2)}) collective-permute-start(bf16[16,2048]{1,0:T(8,128)(2,1)S(1)} %copy-done.1), channel_id=1, source_target_pairs={{0,4},{1,5},{2,6},{3,7},{4,0},{5,1},{6,2},{7,3},{8,12},{9,13},{10,... | collective-permute-start | bytes 196616 | tf_op jit(solution)/shard_map/ppermute | solution.py:318
  36.7 3.5 %collective-permute-start.2 = (bf16[16,2048]{1,0:T(8,128)(2,1)S(1)}, bf16[16,2048]{1,0:T(8,128)(2,1)S(1)}, u32[]{:S(2)}, u32[]{:S(2)}) collective-permute-start(bf16[16,2048]{1,0:T(8,128)(2,1)S(1)} %copy-done.1), channel_id=1, source_target_pairs={{0,6},{1,7},{2,0},{3,1},{4,2},{5,3},{6,4},{7,5},{8,14},{9,15},{10,... | collective-permute-start | bytes 196616 | tf_op jit(solution)/shard_map/ppermute | solution.py:318
  40.2 2.7 %collective-permute-start.3 = (bf16[64,2048]{1,0:T(8,128)(2,1)S(1)}, bf16[64,2048]{1,0:T(8,128)(2,1)S(1)}, u32[]{:S(2)}, u32[]{:S(2)}) collective-permute-start(bf16[64,2048]{1,0:T(8,128)(2,1)S(1)} %pad_maximum_fusion), channel_id=1, source_target_pairs={{0,1},{1,0},{2,3},{3,2},{4,5},{5,4},{6,7},{7,6},{8,9},{9,8},{10,11... | collective-permute-start | bytes 786440 | tf_op jit(solution)/shard_map/ppermute | solution.py:314
  46.3 4.3 %collective-permute-start.4 = (bf16[64,256]{1,0:T(8,128)(2,1)S(1)}, bf16[64,256]{1,0:T(8,128)(2,1)S(1)}, u32[]{:S(2)}, u32[]{:S(2)}) collective-permute-start(bf16[64,256]{1,0:T(8,128)(2,1)S(1)} %get-tuple-element.25), channel_id=1, source_target_pairs={{0,1},{1,0},{2,3},{3,2},{4,5},{5,4},{6,7},{7,6},{8,9},{9,8},{10,11... | collective-permute-start | bytes 98312 | tf_op jit(solution)/shard_map/ppermute | solution.py:314
  50.6 3.8 %collective-permute-start.5 = (bf16[16,512]{1,0:T(8,128)(2,1)S(1)}, bf16[16,512]{1,0:T(8,128)(2,1)S(1)}, u32[]{:S(2)}, u32[]{:S(2)}) collective-permute-start(bf16[16,512]{1,0:T(8,128)(2,1)S(1)} %get-tuple-element.27), channel_id=1, source_target_pairs={{0,6},{1,7},{2,0},{3,1},{4,2},{5,3},{6,4},{7,5},{8,14},{9,15},{10,... | collective-permute-start | bytes 49160 | tf_op jit(solution)/shard_map/ppermute | solution.py:318
  53.1 4.1 %collective-permute-start.6 = (bf16[16,512]{1,0:T(8,128)(2,1)S(1)}, bf16[16,512]{1,0:T(8,128)(2,1)S(1)}, u32[]{:S(2)}, u32[]{:S(2)}) collective-permute-start(bf16[16,512]{1,0:T(8,128)(2,1)S(1)} %get-tuple-element.28), channel_id=1, source_target_pairs={{0,4},{1,5},{2,6},{3,7},{4,0},{5,1},{6,2},{7,3},{8,12},{9,13},{10,... | collective-permute-start | bytes 49160 | tf_op jit(solution)/shard_map/ppermute | solution.py:318
  53.6 3.8 %collective-permute-start.7 = (bf16[16,512]{1,0:T(8,128)(2,1)S(1)}, bf16[16,512]{1,0:T(8,128)(2,1)S(1)}, u32[]{:S(2)}, u32[]{:S(2)}) collective-permute-start(bf16[16,512]{1,0:T(8,128)(2,1)S(1)} %get-tuple-element.29), channel_id=1, source_target_pairs={{0,2},{1,3},{2,4},{3,5},{4,6},{5,7},{6,0},{7,1},{8,10},{9,11},{10,... | collective-permute-start | bytes 49160 | tf_op jit(solution)/shard_map/ppermute | solution.py:318
  64.6 10.9 %copy-start.8 = (s32[16,6]{0,1:T(8,128)S(1)}, s32[16,6]{0,1:T(8,128)}, u32[]{:S(2)}) copy-start(s32[16,6]{0,1:T(8,128)} %param.34) | copy-start | bytes 1156
  64.6 14.4 %copy-start.3 = (f32[2048]{0:T(1024)S(1)}, f32[2048]{0:T(1024)}, u32[]{:S(2)}) copy-start(f32[2048]{0:T(1024)} %param.26) | copy-start | bytes 24580
  64.6 14.4 %copy-start.4 = (f32[2048]{0:T(1024)S(1)}, f32[2048]{0:T(1024)}, u32[]{:S(2)}) copy-start(f32[2048]{0:T(1024)} %param.27) | copy-start | bytes 24580
  64.7 5.1 %collective-permute-start.8 = (bf16[16,2048]{1,0:T(8,128)(2,1)S(1)}, bf16[16,2048]{1,0:T(8,128)(2,1)S(1)}, u32[]{:S(2)}, u32[]{:S(2)}) collective-permute-start(bf16[16,2048]{1,0:T(8,128)(2,1)S(1)} %attend.1.a0), channel_id=1, source_target_pairs={{0,2},{1,3},{2,4},{3,5},{4,6},{5,7},{6,0},{7,1},{8,10},{9,11},{10,... | collective-permute-start | bytes 196616 | tf_op jit(solution)/shard_map/ppermute | solution.py:318
  64.7 5.0 %collective-permute-start.9 = (bf16[16,2048]{1,0:T(8,128)(2,1)S(1)}, bf16[16,2048]{1,0:T(8,128)(2,1)S(1)}, u32[]{:S(2)}, u32[]{:S(2)}) collective-permute-start(bf16[16,2048]{1,0:T(8,128)(2,1)S(1)} %attend.1.a0), channel_id=1, source_target_pairs={{0,4},{1,5},{2,6},{3,7},{4,0},{5,1},{6,2},{7,3},{8,12},{9,13},{10,... | collective-permute-start | bytes 196616 | tf_op jit(solution)/shard_map/ppermute | solution.py:318
  66.4 3.9 %collective-permute-start.10 = (bf16[16,2048]{1,0:T(8,128)(2,1)S(1)}, bf16[16,2048]{1,0:T(8,128)(2,1)S(1)}, u32[]{:S(2)}, u32[]{:S(2)}) collective-permute-start(bf16[16,2048]{1,0:T(8,128)(2,1)S(1)} %attend.1.a0), channel_id=1, source_target_pairs={{0,6},{1,7},{2,0},{3,1},{4,2},{5,3},{6,4},{7,5},{8,14},{9,15},{10,... | collective-permute-start | bytes 196616 | tf_op jit(solution)/shard_map/ppermute | solution.py:318
  72.3 4.8 %collective-permute-start.12 = (bf16[16,512]{1,0:T(8,128)(2,1)S(1)}, bf16[16,512]{1,0:T(8,128)(2,1)S(1)}, u32[]{:S(2)}, u32[]{:S(2)}) collective-permute-start(bf16[16,512]{1,0:T(8,128)(2,1)S(1)} %get-tuple-element.31), channel_id=1, source_target_pairs={{0,6},{1,7},{2,0},{3,1},{4,2},{5,3},{6,4},{7,5},{8,14},{9,15},{10,... | collective-permute-start | bytes 49160 | tf_op jit(solution)/shard_map/ppermute | solution.py:318
  74.8 4.1 %collective-permute-start.13 = (bf16[16,512]{1,0:T(8,128)(2,1)S(1)}, bf16[16,512]{1,0:T(8,128)(2,1)S(1)}, u32[]{:S(2)}, u32[]{:S(2)}) collective-permute-start(bf16[16,512]{1,0:T(8,128)(2,1)S(1)} %get-tuple-element.32), channel_id=1, source_target_pairs={{0,4},{1,5},{2,6},{3,7},{4,0},{5,1},{6,2},{7,3},{8,12},{9,13},{10,... | collective-permute-start | bytes 49160 | tf_op jit(solution)/shard_map/ppermute | solution.py:318
  75.1 3.9 %collective-permute-start.14 = (bf16[16,512]{1,0:T(8,128)(2,1)S(1)}, bf16[16,512]{1,0:T(8,128)(2,1)S(1)}, u32[]{:S(2)}, u32[]{:S(2)}) collective-permute-start(bf16[16,512]{1,0:T(8,128)(2,1)S(1)} %get-tuple-element.33), channel_id=1, source_target_pairs={{0,2},{1,3},{2,4},{3,5},{4,6},{5,7},{6,0},{7,1},{8,10},{9,11},{10,... | collective-permute-start | bytes 49160 | tf_op jit(solution)/shard_map/ppermute | solution.py:318
  77.2 31.4 %copy-start = (bf16[1,2048,512]{2,1,0:T(8,128)(2,1)S(1)}, bf16[1,2048,512]{2,1,0:T(8,128)(2,1)}, u32[]{:S(2)}) copy-start(bf16[1,2048,512]{2,1,0:T(8,128)(2,1)} %gate.1) | copy-start | bytes 6291460
  113.4 4.5 %copy-start.9 = (f32[16,6]{0,1:T(8,128)S(1)}, f32[16,6]{0,1:T(8,128)}, u32[]{:S(2)}) copy-start(f32[16,6]{0,1:T(8,128)} %param.35) | copy-start | bytes 1156
  113.4 23.8 %all-to-all-start.3 = ((bf16[128,16,256]{2,1,0:T(8,128)(2,1)}), bf16[128,16,256]{2,1,0:T(8,128)(2,1)S(1)}, u32[]{:S(2)}, u32[]{:S(2)}) async-start(bf16[128,16,256]{2,1,0:T(8,128)(2,1)} %bitcast.11), calls=%async_computation.3 | async-start | bytes 2097152 | tf_op jit(solution)/shard_map/all_to_all | solution.py:397
  117.9 19.2 %copy-start.5 = (f32[2048]{0:T(1024)S(1)}, f32[2048]{0:T(1024)}, u32[]{:S(2)}) copy-start(f32[2048]{0:T(1024)} %param.28) | copy-start | bytes 24580
